TPU v7x, 32 devices: a whole 2x2x4 slice. The times are simulated.
32 devices in a mesh: sp: 4 (over z), tp: 8 (over y, x, core).
Axes of the slice: x: 2, y: 2, z: 4, core: 2. Of those that a mesh axis runs over, the one named last changes fastest.
Arguments:
- activations: bfloat16 [1024, 2048], P('sp', 'tp'), may hold values from -170 to 170
- norm_gain: float32 [2048], replicated, may hold values from 0.1 to 1.9
- query_weight: bfloat16 [2048, 1536], P(None, 'tp'), may hold values from -0.125 to 0.125
- latent_weight: bfloat16 [2048, 512], P(None, 'tp'), may hold values from -0.125 to 0.125
- rope_key_weight: bfloat16 [2048, 64], replicated, may hold values from -0.125 to 0.125
- latent_gain: float32 [512], replicated, may hold values from 1.5 to 64
- expand_weight: bfloat16 [512, 2048], P(None, 'tp'), may hold values from -0.25 to 0.25
- gate_weight: bfloat16 [2048, 1024], P(None, 'tp'), may hold values from -0.125 to 0.125
- pre_weight: bfloat16 [2048, 1024], P(None, 'tp'), may hold values from -0.125 to 0.125
- value_weight: bfloat16 [2048, 1024], P(None, 'tp'), may hold values from -0.125 to 0.125
- conv_kernel: bfloat16 [3, 1024], P(None, 'tp'), may hold values from -3.5 to 3.5
- output_attend: bfloat16 [1024, 2048], P('tp'), may hold values from -0.1875 to 0.1875
- output_conv: bfloat16 [1024, 2048], P('tp'), may hold values from -0.125 to 0.125
Outputs:
- mixed: bfloat16 [1024, 2048], P(('sp', 'tp'))
- log_weight_sum: float32 [8, 1024], P('tp', 'sp')
All inputs are finite; a program needn't handle non-finite values.
Results may differ from a plain program's by a relative error of at most 0.035.
The roundings to bfloat16 on the way count: a program that leaves them out, or rounds other values in their place, can miss the bound.
Values may be sent and summed in bfloat16 or wider, within the bound.
No kernel may reach another device: no remote copies, remote signals or barrier semaphores. Data moves between devices by JAX's collectives and lax.ppermute only.
A program may use at most 128 MiB of HBM per device.

v0:
```python
import functools
import math

import jax
import jax.numpy as jnp
from jax import lax
from jax.experimental import pallas as pl
from jax.experimental.pallas import tpu as pltpu
from jax.sharding import PartitionSpec as P


NOPE = 128
ROPE = 64
VDIM = 128
GRID_W = 64
EPSILON = 1e-06
ROPE_BASE = 10000.0
LANES = 128
HALO = 8
F32 = jnp.float32
BF16 = jnp.bfloat16


def swap(array, axis, mask):
    peers = lax.axis_size(axis)
    return lax.ppermute(array, axis, [(i, i ^ mask) for i in range(peers)])


def exchange(array, axis, stride, peers):
    pieces = []
    for i in reversed(range(1, peers)):
        pieces.append(swap(array, axis, stride * i))
    return pieces[::-1]


def kernel_call(body, outs, limit, scratch=(), flops=0, nbytes=0, space=pltpu.VMEM):
    whole = pl.BlockSpec(memory_space=pltpu.VMEM)

    def call(*operands):
        if space is not pltpu.VMEM:
            operands = [pltpu.with_memory_space_constraint(operand, space) for operand in operands]
        return pl.pallas_call(
            body,
            out_shape=[jax.ShapeDtypeStruct(shape, dtype) for shape, dtype in outs],
            in_specs=[pl.BlockSpec(memory_space=space)] * len(operands),
            out_specs=[whole] * len(outs),
            scratch_shapes=list(scratch),
            compiler_params=pltpu.CompilerParams(vmem_limit_bytes=limit),
            cost_estimate=pl.CostEstimate(flops=flops, bytes_accessed=nbytes, transcendentals=0),
        )(*operands)

    return call


def rotate(values, cosines, sines):
    quarter = ROPE // 4
    lane = lax.broadcasted_iota(jnp.int32, values.shape, 1)
    first = (lane // quarter) % 2 == 0
    ahead = pltpu.roll(values, LANES - quarter, 1)
    behind = pltpu.roll(values, quarter, 1)
    return values * cosines + jnp.where(first, ahead, behind) * sines


def low_lanes(shape):
    return lax.broadcasted_iota(jnp.int32, shape, 1) < ROPE


def prepare(
    latent_ref, rope_ref, query_ref, pre_ref, value_ref, expand_ref, gain_ref, attend_ref, conv_ref, taps_ref,
    key_w_ref, query_w_ref, mix_w_ref, expand_k_ref, expand_v_ref, lat_gain_ref, own_w_ref, cos_ref, sin_ref,
    taps_out_ref, expand_in, gain_in, taps_in, sems,
):
    moves = [
        (expand_ref, expand_in),
        (gain_ref, gain_in),
        (taps_ref, taps_in),
        (latent_ref, key_w_ref.at[:ROPE]),
        (latent_ref, key_w_ref.at[ROPE : 2 * ROPE]),
        (rope_ref, key_w_ref.at[2 * ROPE : 3 * ROPE]),
        (rope_ref, key_w_ref.at[3 * ROPE :]),
        (pre_ref, mix_w_ref.at[:, :LANES]),
        (value_ref, mix_w_ref.at[:, LANES:]),
        (query_ref, query_w_ref.at[: NOPE + ROPE]),
        (query_ref.at[NOPE:], query_w_ref.at[NOPE + ROPE :]),
        (attend_ref, own_w_ref.at[:VDIM]),
        (conv_ref, own_w_ref.at[VDIM:]),
    ]
    copies = [pltpu.make_async_copy(source, target, sems.at[i]) for i, (source, target) in enumerate(moves)]
    for copy in copies:
        copy.start()
    quarter = ROPE // 4
    groups = cos_ref.shape[0] // GRID_W
    first_row = lax.axis_index("sp") * groups

    def angles(rows, start):
        lane = lax.broadcasted_iota(jnp.int32, (rows, LANES), 1) % ROPE
        place = (lax.broadcasted_iota(jnp.int32, (rows, LANES), 0) + start).astype(F32)
        inverse = jnp.exp((lane % quarter).astype(F32) * (-math.log(ROPE_BASE) / quarter))
        angle = place * inverse
        sign = jnp.where((lane // quarter) % 2 == 0, -1.0, 1.0)
        return lane < 2 * quarter, jnp.cos(angle), jnp.sin(angle) * sign

    _, row_cos, row_sin = angles(groups, first_row)
    by_row, col_cos, col_sin = angles(GRID_W, 0)
    for g in range(groups):
        rows = slice(g * GRID_W, (g + 1) * GRID_W)
        cos_ref[rows, :] = jnp.where(by_row, row_cos[g : g + 1], col_cos)
        sin_ref[rows, :] = jnp.where(by_row, row_sin[g : g + 1], col_sin)
    for copy in copies[:3]:
        copy.wait()
    taps_out_ref[...] = taps_in[...].astype(F32)
    ranks = lat_gain_ref.shape[0]
    low = low_lanes((1, LANES))
    zeros = jnp.zeros((ROPE, LANES), BF16)
    for k in range(ranks):
        part = expand_in[k * ROPE : (k + 1) * ROPE, :]
        upper = slice(k * LANES, k * LANES + ROPE)
        lower = slice(k * LANES + ROPE, (k + 1) * LANES)
        for ref, piece in ((expand_k_ref, part[:, :NOPE]), (expand_v_ref, part[:, NOPE:])):
            ref[upper, :LANES] = piece
            ref[upper, LANES:] = zeros
            ref[lower, :LANES] = zeros
            ref[lower, LANES:] = piece
        pair = gain_in[:, (k // 2) * LANES : (k // 2 + 1) * LANES]
        turned = pltpu.roll(pair, ROPE, 1)
        chosen = (pair, turned) if k % 2 == 0 else (turned, pair)
        lat_gain_ref[k : k + 1, :] = jnp.where(low, *chosen)
    for copy in copies[3:]:
        copy.wait()


def dot_nt(left, right):
    return lax.dot_general(left, right, (((1,), (1,)), ((), ())), preferred_element_type=F32)


def project_first(pairs, *refs):
    pieces, refs = refs[: 2 * pairs], refs[2 * pairs :]
    gain_ref, key_w_ref, mix_w_ref, cos_ref, sin_ref = refs[:5]
    scaled_ref, inv_ref, message_ref, mix_ref, key_ref = refs[5:]
    rank = lax.axis_index("tp")
    tokens, width = pieces[0].shape
    half = tokens // 2
    total = jnp.zeros((tokens, LANES), F32)
    for i, ref in enumerate(pieces):
        owner = rank ^ (2 * (i % pairs) + i // pairs)
        piece = ref[...].astype(F32)
        squares = piece * piece
        for j in range(width // LANES):
            total = total + squares[:, j * LANES : (j + 1) * LANES]
        columns = pl.ds(pl.multiple_of(owner * width, width), width)
        scaled_ref[:, columns] = (piece * gain_ref[:, columns]).astype(BF16)
    features = 2 * pairs * width
    inv = lax.rsqrt(jnp.sum(total, axis=1, keepdims=True) / features + EPSILON)
    inv_ref[...] = jnp.broadcast_to(inv, inv_ref.shape)
    scaled = scaled_ref[...]
    keys = dot_nt(scaled, key_w_ref[...]) * inv
    mixes = jnp.dot(scaled, mix_w_ref[...], preferred_element_type=F32) * inv
    mix = (mixes[:, :LANES] * mixes[:, LANES:]).astype(BF16)
    mix_ref[...] = mix
    latent = keys[:, :LANES]
    low = low_lanes((half, LANES))
    message_ref[:half, :] = jnp.where(low, latent[:half], latent[half:]).astype(BF16)
    key_ref[...] = keys[:, LANES:]
    share = half // (2 * pairs)
    start = pl.multiple_of(rank * share, share)
    turned = []
    for base in (0, half):
        rows = pl.ds(start + base, share)
        turned.append(rotate(key_ref[rows, :], cos_ref[rows, :], sin_ref[rows, :]))
    low = low_lanes((share, LANES))
    message_ref[half : half + share, :] = jnp.where(low, turned[0], turned[1]).astype(BF16)
    row = lax.broadcasted_iota(jnp.int32, (HALO, LANES), 0)
    first = jnp.broadcast_to(mix[:1].astype(F32), (HALO, LANES))
    last = jnp.broadcast_to(mix[tokens - 1 :].astype(F32), (HALO, LANES))
    message_ref[half + share :, :] = jnp.where(row == 0, first, last).astype(BF16)


def project_second(
    scaled_ref, inv_ref, query_w_ref, gate_w_ref, cos_ref, sin_ref, query_ref, gate_ref
):
    scaled = scaled_ref[...]
    inv = inv_ref[...]
    scale = (NOPE + ROPE) ** (-0.5)
    query = dot_nt(scaled, query_w_ref[...])
    gate_ref[...] = jnp.dot(scaled, gate_w_ref[...], preferred_element_type=F32) * inv
    nope = (query[:, :NOPE] * inv * scale).astype(BF16)
    rope = rotate(query[:, NOPE:] * inv, cos_ref[...], sin_ref[...]) * scale
    low = low_lanes(rope.shape)
    query_ref[0, :, :NOPE] = nope
    query_ref[1, :, :NOPE] = nope
    query_ref[0, :, NOPE:] = jnp.where(low, rope, 0.0).astype(BF16)
    query_ref[1, :, NOPE:] = jnp.where(low, 0.0, rope).astype(BF16)


def attend(pairs, chunk, natural, *refs):
    pieces, halos, refs = refs[: 2 * pairs], refs[2 * pairs : -13], refs[-13:]
    gain_ref, expand_k_ref, expand_v_ref, query_ref, gate_ref, mix_ref, taps_ref = refs[:7]
    keep_ref, send_ref, log_ref, latent_ref, rope_ref, both_ref = refs[7:]
    rank = lax.axis_index("tp")
    place = lax.axis_index("sp")
    blocks = pieces[0].shape[0]
    ranks = 2 * pairs
    tokens = query_ref.shape[1]
    half = tokens // 2
    share = half // ranks
    entries = ranks * ROPE
    low = low_lanes((half, LANES))
    owned = [(rank ^ (2 * (i % pairs) + i // pairs), ref) for i, ref in enumerate(pieces)]

    def one_chunk(first, state):
        for slot in range(chunk):
            block = first + slot
            base = slot * half
            total = jnp.zeros((half, LANES), F32)
            for owner, ref in owned:
                piece = ref[block, :half, :].astype(F32)
                total = total + piece * piece
                start = pl.multiple_of(base + owner * share, share)
                rope_ref[pl.ds(start, share), :] = ref[block, half : half + share, :]
            sum_low = jnp.sum(jnp.where(low, total, 0.0), axis=1, keepdims=True)
            sum_high = jnp.sum(jnp.where(low, 0.0, total), axis=1, keepdims=True)
            inv = lax.rsqrt(jnp.where(low, sum_low, sum_high) / entries + EPSILON)
            for owner, ref in owned:
                piece = ref[block, :half, :].astype(F32)
                start = pl.multiple_of(owner * LANES, LANES)
                scaled = piece * inv * gain_ref[pl.ds(owner, 1), :]
                latent_ref[base : base + half, pl.ds(start, LANES)] = scaled.astype(BF16)
        latent = latent_ref[...]
        keys = jnp.dot(latent, expand_k_ref[...], preferred_element_type=F32).astype(BF16)
        values = lax.dot_general(
            expand_v_ref[...], latent, (((0,), (1,)), ((), ())), preferred_element_type=F32
        ).astype(BF16)
        rope = rope_ref[...]
        scores = [
            dot_nt(jnp.concatenate([keys[:, i * NOPE : (i + 1) * NOPE], rope], axis=1), query_ref[i])
            for i in range(2)
        ]
        peak = jnp.max(jnp.maximum(*scores), axis=0, keepdims=True)
        if state is not None:
            peak = jnp.maximum(peak, state[0])
        weights = [jnp.exp(piece - peak) for piece in scores]
        total = jnp.sum(weights[0] + weights[1], axis=0, keepdims=True)
        out = sum(
            jnp.dot(values[i * VDIM : (i + 1) * VDIM], weights[i].astype(BF16), preferred_element_type=F32)
            for i in range(2)
        )
        if state is not None:
            rescale = jnp.exp(state[0] - peak)
            total = total + state[1] * rescale
            out = out + state[2] * rescale
        return peak, total, out

    if blocks == chunk:
        peak, total, out = one_chunk(0, None)
    else:
        start = (
            jnp.full((1, tokens), -jnp.inf, F32),
            jnp.zeros((1, tokens), F32),
            jnp.zeros((VDIM, tokens), F32),
        )
        peak, total, out = lax.fori_loop(0, blocks // chunk, lambda i, state: one_chunk(i * chunk, state), start)
    both_ref[:, :VDIM] = jnp.transpose(out / total)
    log_ref[...] = peak + jnp.log(total)

    mix = mix_ref[...].astype(F32)

    def edge_of(other, at):
        inside = (other >= 0) & (other < blocks)
        other = jnp.clip(other, 0, blocks - 1)
        if natural:
            edges = halos[0][other].astype(F32)
        else:
            edges = jnp.zeros((HALO, LANES), F32)
            for i, ref in enumerate(halos):
                edges = jnp.where((other ^ place) == i, ref[half + share :, :].astype(F32), edges)
        return jnp.where(inside, edges[at : at + 1, :], 0.0)

    before = edge_of(place - 1, 1)
    after = edge_of(place + 1, 0)
    row = lax.broadcasted_iota(jnp.int32, mix.shape, 0)
    earlier = jnp.where(row == 0, before, pltpu.roll(mix, 1, 0))
    later = jnp.where(row == tokens - 1, after, pltpu.roll(mix, tokens - 1, 0))
    taps = taps_ref[...]
    convolved = taps[0:1] * earlier + taps[1:2] * mix + taps[2:3] * later
    both_ref[:, VDIM:] = gate_ref[...] * convolved

    chip, core = rank // 2, rank % 2
    rows = tokens // ranks
    for i in range(pairs):
        base = 2 * (chip ^ i)
        mine = pl.multiple_of((base + core) * rows, rows)
        other = pl.multiple_of((base + 1 - core) * rows, rows)
        keep_ref[i * rows : (i + 1) * rows, :] = both_ref[pl.ds(mine, rows), :].astype(BF16)
        send_ref[i * rows : (i + 1) * rows, :] = both_ref[pl.ds(other, rows), :].astype(BF16)


def output(keep_ref, got_ref, own_w_ref, other_w_ref, first_ref, *rest_refs):
    out = jnp.dot(keep_ref[...], own_w_ref[...], preferred_element_type=F32)
    out = out + jnp.dot(got_ref[...], other_w_ref[...], preferred_element_type=F32)
    rows = first_ref.shape[0]
    first_ref[...] = out[:rows]
    for i, ref in enumerate(rest_refs):
        ref[...] = out[(i + 1) * rows : (i + 2) * rows].astype(BF16)


def body(
    activations,
    norm_gain,
    query_weight,
    latent_weight,
    rope_key_weight,
    latent_gain,
    expand_weight,
    gate_weight,
    pre_weight,
    value_weight,
    conv_kernel,
    output_attend,
    output_conv,
):
    ranks = lax.axis_size("tp")
    places = lax.axis_size("sp")
    pairs = ranks // 2
    tokens, width = activations.shape
    features = ranks * width
    half = tokens // 2
    share = half // ranks
    rows = tokens // ranks
    channels = gate_weight.shape[1]

    even = [activations] + exchange(activations, "tp", 2, pairs)
    odd = [swap(piece, "tp", 1) for piece in even]

    key_w, query_w, mix_w, expand_k, expand_v, lat_gain, own_w, cosines, sines, taps = kernel_call(
        prepare,
        [
            ((4 * ROPE, features), BF16),
            ((NOPE + 2 * ROPE, features), BF16),
            ((features, 2 * LANES), BF16),
            ((ranks * LANES, 2 * NOPE), BF16),
            ((ranks * LANES, 2 * VDIM), BF16),
            ((ranks, LANES), F32),
            ((VDIM + channels, features), BF16),
            ((tokens, LANES), F32),
            ((tokens, LANES), F32),
            (conv_kernel.shape, F32),
        ],
        16 << 20,
        scratch=[
            pltpu.VMEM(expand_weight.shape, BF16),
            pltpu.VMEM((1, latent_gain.shape[0]), F32),
            pltpu.VMEM(conv_kernel.shape, BF16),
            pltpu.SemaphoreType.DMA((13,)),
        ],
        space=pltpu.HBM,
        flops=1 << 28,
        nbytes=1 << 23,
    )(
        latent_weight.T, rope_key_weight.T, query_weight.T, pre_weight, value_weight, expand_weight,
        latent_gain.reshape(1, -1), output_attend, output_conv, conv_kernel,
    )
    other_w = swap(own_w, "tp", 1)

    scaled, inv, message, mix = kernel_call(
        functools.partial(project_first, pairs),
        [
            ((tokens, features), BF16),
            ((tokens, LANES), F32),
            ((half + share + HALO, LANES), BF16),
            ((tokens, channels), BF16),
        ],
        12 << 20,
        scratch=[pltpu.VMEM((tokens, LANES), F32)],
        flops=2 * tokens * features * 4 * LANES,
        nbytes=4 * tokens * features,
    )(*even, *odd, norm_gain.reshape(1, -1), key_w, mix_w, cosines, sines)

    small = places <= 8 and places & (places - 1) == 0
    if small:
        halos = [message] + exchange(message, "sp", 1, places)
        around = jnp.stack([piece[: half + share] for piece in halos])
    else:
        around = lax.all_gather(message, "sp", axis=0)
        around, halos = around[:, : half + share], [around[:, half + share :]]
    query, gate = kernel_call(
        project_second,
        [((2, tokens, NOPE + LANES), BF16), ((tokens, channels), F32)],
        12 << 20,
        flops=2 * tokens * features * 3 * LANES,
        nbytes=4 * tokens * features,
    )(scaled, inv, query_w, gate_weight, cosines, sines)
    chip_even = [around] + exchange(around, "tp", 2, pairs)
    chip_odd = [swap(piece, "tp", 1) for piece in chip_even]

    chunk = places if small else 4
    keep, send, logs = kernel_call(
        functools.partial(attend, pairs, chunk, not small),
        [((half, VDIM + channels), BF16), ((half, VDIM + channels), BF16), ((1, tokens), F32)],
        (16 << 20) if small else (60 << 20),
        scratch=[
            pltpu.VMEM((chunk * half, ranks * LANES), BF16),
            pltpu.VMEM((chunk * half, LANES), BF16),
            pltpu.VMEM((tokens, VDIM + channels), F32),
        ],
        flops=1 << 30,
        nbytes=1 << 22,
    )(*chip_even, *chip_odd, *halos, lat_gain, expand_k, expand_v, query, gate, mix, taps)

    got = swap(send, "tp", 1)
    outs = kernel_call(
        output,
        [((rows, features), F32)] + [((rows, features), BF16)] * (pairs - 1),
        12 << 20,
        flops=1 << 28,
        nbytes=1 << 22,
    )(keep, got, own_w, other_w)
    arrived = [swap(outs[i], "tp", 2 * i) for i in reversed(range(1, pairs))]
    total = outs[0]
    for piece in arrived:
        total = total + piece.astype(F32)
    return total.astype(BF16), logs


def solution(mesh):
    return jax.shard_map(
        body,
        mesh=mesh,
        in_specs=(
            P("sp", "tp"),
            P(),
            P(None, "tp"),
            P(None, "tp"),
            P(),
            P(),
            P(None, "tp"),
            P(None, "tp"),
            P(None, "tp"),
            P(None, "tp"),
            P(None, "tp"),
            P("tp", None),
            P("tp", None),
        ),
        out_specs=(P(("sp", "tp"), None), P("tp", "sp")),
        check_vma=False,
    )
```

profile of v0, /device:TPU:0, one launch (start us, length us, event | category | flops | bytes accessed | tf_op | source)
XLA Modules:
  0.0 49.6 jit_solution(12498551670109985877)
XLA Ops:
  0.6 4.0 %collective-permute-start.2 = (bf16[256,256]{1,0:T(8,128)(2,1)}, bf16[256,256]{1,0:T(8,128)(2,1)S(1)}, u32[]{:S(2)}, u32[]{:S(2)}) collective-permute-start(bf16[256,256]{1,0:T(8,128)(2,1)} %refs_0_.1), channel_id=1, source_target_pairs={{0,6},{1,7},{2,4},{3,5},{4,2},{5,3},{6,0},{7,1},{8,14},{9,15},{10,... | collective-permute-start | bytes 393224 | tf_op jit(solution)/shard_map/ppermute | solution.py:26
  4.6 0.5 %collective-permute-start.1 = (bf16[256,256]{1,0:T(8,128)(2,1)}, bf16[256,256]{1,0:T(8,128)(2,1)S(1)}, u32[]{:S(2)}, u32[]{:S(2)}) collective-permute-start(bf16[256,256]{1,0:T(8,128)(2,1)} %refs_0_.1), channel_id=1, source_target_pairs={{0,4},{1,5},{2,6},{3,7},{4,0},{5,1},{6,2},{7,3},{8,12},{9,13},{10,... | collective-permute-start | bytes 393224 | tf_op jit(solution)/shard_map/ppermute | solution.py:26
  5.3 3.6 %collective-permute-done.2.refs_3_ = bf16[256,256]{1,0:T(8,128)(2,1)S(1)} collective-permute-done((bf16[256,256]{1,0:T(8,128)(2,1)}, bf16[256,256]{1,0:T(8,128)(2,1)S(1)}, u32[]{:S(2)}, u32[]{:S(2)}) %collective-permute-start.2) | collective-permute-done | bytes 131104 | tf_op jit(solution)/shard_map/ppermute | solution.py:26
  8.8 2.3 %collective-permute-done.1.refs_2_ = bf16[256,256]{1,0:T(8,128)(2,1)S(1)} collective-permute-done((bf16[256,256]{1,0:T(8,128)(2,1)}, bf16[256,256]{1,0:T(8,128)(2,1)S(1)}, u32[]{:S(2)}, u32[]{:S(2)}) %collective-permute-start.1) | collective-permute-done | bytes 131104 | tf_op jit(solution)/shard_map/ppermute | solution.py:26
  11.1 0.2 collective-permute-done.refs_1_
  11.4 0.3 collective-permute-start.4
  11.7 2.4 %shard_map.140 = (bf16[256,2048]{1,0:T(8,128)(2,1)S(1)}, bf16[256,2048]{1,0:T(8,128)(2,1)S(1)}, bf16[2048,256]{1,0:T(8,128)(2,1)S(1)}, bf16[1024,256]{1,0:T(8,12...) custom-call(bf16[64,2048]{1,0:T(8,128)(2,1)} %bitcast.15, ...), custom_call_target="tpu_custom_call" | custom-call | flops 268435456 | bytes 8388608 | tf_op jit(solution)/shard_map/pallas_call | solution.py:42
  14.1 0.3 collective-permute-start.18
  14.4 0.3 copy-done.2
  14.8 1.1 %shard_map.141 = (bf16[256,2048]{1,0:T(8,128)(2,1)S(1)}, f32[256,128]{1,0:T(8,128)S(1)}, bf16[152,128]{1,0:T(8,128)(2,1)S(1)}, bf16[256,128]{1,0:T(8,128)(2,1)S(1)}) custom-call(bf16[256,256]{1,0:T(8,128)(2,1)S(1)} %copy-done.1, bf16[256,256]{1,0:T(8,128)(2,1)S(1)} %collective-permute-done.refs_1_, bf16[256,256]{1,0:T(8,128)(2,1)S(1)} %collective-permute-done.1.refs_2_, ...), custom_call_target="tpu_custom_call" | custom-call | flops 536870912 | bytes 2097152 | tf_op jit(solution)/shard_map/pallas_call | solution.py:42
  15.9 3.9 %collective-permute-start.9 = (bf16[152,128]{1,0:T(8,128)(2,1)S(1)}, bf16[152,128]{1,0:T(8,128)(2,1)S(1)}, u32[]{:S(2)}, u32[]{:S(2)}) collective-permute-start(bf16[152,128]{1,0:T(8,128)(2,1)S(1)} %get-tuple-element.29.refs_8_), channel_id=1, source_target_pairs={{0,24},{8,16},{16,8},{24,0},{1,25},{9,17},{17,9},{25,1},{2,26},{10... | collective-permute-start | bytes 116744 | tf_op jit(solution)/shard_map/ppermute | solution.py:26
  19.8 0.6 %collective-permute-start.7 = (bf16[152,128]{1,0:T(8,128)(2,1)S(1)}, bf16[152,128]{1,0:T(8,128)(2,1)S(1)}, u32[]{:S(2)}, u32[]{:S(2)}) collective-permute-start(bf16[152,128]{1,0:T(8,128)(2,1)S(1)} %get-tuple-element.29.refs_8_), channel_id=1, source_target_pairs={{0,8},{8,0},{16,24},{24,16},{1,9},{9,1},{17,25},{25,17},{2,10},{10... | collective-permute-start | bytes 116744 | tf_op jit(solution)/shard_map/ppermute | solution.py:26
  20.4 1.3 %collective-permute-done.9.refs_11_ = bf16[152,128]{1,0:T(8,128)(2,1)S(1)} collective-permute-done((bf16[152,128]{1,0:T(8,128)(2,1)S(1)}, bf16[152,128]{1,0:T(8,128)(2,1)S(1)}, u32[]{:S(2)}, u32[]{:S(2)}) %collective-permute-start.9) | collective-permute-done | bytes 38944 | tf_op jit(solution)/shard_map/ppermute | solution.py:26
  21.8 2.9 %collective-permute-done.8.refs_10_ = bf16[152,128]{1,0:T(8,128)(2,1)S(1)} collective-permute-done((bf16[152,128]{1,0:T(8,128)(2,1)S(1)}, bf16[152,128]{1,0:T(8,128)(2,1)S(1)}, u32[]{:S(2)}, u32[]{:S(2)}) %collective-permute-start.8) | collective-permute-done | bytes 38944 | tf_op jit(solution)/shard_map/ppermute | solution.py:26
  24.7 1.8 %collective-permute-start.12 = (bf16[4,144,128]{2,1,0:T(8,128)(2,1)S(1)}, bf16[4,144,128]{2,1,0:T(8,128)(2,1)S(1)}, u32[]{:S(2)}, u32[]{:S(2)}) collective-permute-start(bf16[4,144,128]{2,1,0:T(8,128)(2,1)S(1)} %pad_maximum_fusion.refs_0_), channel_id=1, source_target_pairs={{0,6},{1,7},{2,4},{3,5},{4,2},{5,3},{6,0},{7,1},{8,14},{9,15},{10,... | collective-permute-start | bytes 442376 | tf_op jit(solution)/shard_map/ppermute | solution.py:26
  26.5 1.2 %collective-permute-start.11 = (bf16[4,144,128]{2,1,0:T(8,128)(2,1)S(1)}, bf16[4,144,128]{2,1,0:T(8,128)(2,1)S(1)}, u32[]{:S(2)}, u32[]{:S(2)}) collective-permute-start(bf16[4,144,128]{2,1,0:T(8,128)(2,1)S(1)} %pad_maximum_fusion.refs_0_), channel_id=1, source_target_pairs={{0,4},{1,5},{2,6},{3,7},{4,0},{5,1},{6,2},{7,3},{8,12},{9,13},{10,... | collective-permute-start | bytes 442376 | tf_op jit(solution)/shard_map/ppermute | solution.py:26
  27.7 0.5 %collective-permute-start.10 = (bf16[4,144,128]{2,1,0:T(8,128)(2,1)S(1)}, bf16[4,144,128]{2,1,0:T(8,128)(2,1)S(1)}, u32[]{:S(2)}, u32[]{:S(2)}) collective-permute-start(bf16[4,144,128]{2,1,0:T(8,128)(2,1)S(1)} %pad_maximum_fusion.refs_0_), channel_id=1, source_target_pairs={{0,2},{1,3},{2,0},{3,1},{4,6},{5,7},{6,4},{7,5},{8,10},{9,11},{10,... | collective-permute-start | bytes 442376 | tf_op jit(solution)/shard_map/ppermute | solution.py:26
  28.3 3.9 %collective-permute-done.12.refs_3_ = bf16[4,144,128]{2,1,0:T(8,128)(2,1)S(1)} collective-permute-done((bf16[4,144,128]{2,1,0:T(8,128)(2,1)S(1)}, bf16[4,144,128]{2,1,0:T(8,128)(2,1)S(1)}, u32[]{:S(2)}, u32[]{:S(2)}) %collective-permute-start.12) | collective-permute-done | bytes 147488 | tf_op jit(solution)/shard_map/ppermute | solution.py:26
  32.2 1.4 %collective-permute-done.11.refs_2_ = bf16[4,144,128]{2,1,0:T(8,128)(2,1)S(1)} collective-permute-done((bf16[4,144,128]{2,1,0:T(8,128)(2,1)S(1)}, bf16[4,144,128]{2,1,0:T(8,128)(2,1)S(1)}, u32[]{:S(2)}, u32[]{:S(2)}) %collective-permute-start.11) | collective-permute-done | bytes 147488 | tf_op jit(solution)/shard_map/ppermute | solution.py:26
  33.7 0.5 %collective-permute-start.14 = (bf16[4,144,128]{2,1,0:T(8,128)(2,1)S(1)}, bf16[4,144,128]{2,1,0:T(8,128)(2,1)S(1)}, u32[]{:S(2)}, u32[]{:S(2)}) collective-permute-start(bf16[4,144,128]{2,1,0:T(8,128)(2,1)S(1)} %collective-permute-done.10.refs_1_), channel_id=1, source_target_pairs={{0,1},{1,0},{2,3},{3,2},{4,5},{5,4},{6,7},{7,6},{8,9},{9,8},{10,11... | collective-permute-start | bytes 442376 | tf_op jit(solution)/shard_map/ppermute | solution.py:26
  34.2 0.8 %shard_map.142 = (bf16[2,256,256]{2,1,0:T(8,128)(2,1)S(1)}, f32[256,128]{1,0:T(8,128)S(1)}) custom-call(bf16[256,2048]{1,0:T(8,128)(2,1)S(1)} %get-tuple-element.33.scaled_ref, f32[256,128]{1,0:T(8,128)S(1)} %get-tuple-element.34.inv_ref, bf16[256,2048]{1,0:T(8,128)(2,1)S(1)} %get-tuple-element.35.query_w_ref, bf16[2048,128]{1,0:T(8,128)(2,1)S(1)} %copy-done, ...), custom_call_target="tpu_custom_call" | custom-call | flops 402653184 | bytes 2097152 | tf_op jit(solution)/shard_map/pallas_call | solution.py:42
  35.0 0.2 collective-permute-done.14.refs_5_
  35.2 2.4 %shard_map.143 = (bf16[128,256]{1,0:T(8,128)(2,1)S(1)}, bf16[128,256]{1,0:T(8,128)(2,1)S(1)}, f32[1,256]{1,0:T(1,128)}) custom-call(bf16[4,144,128]{2,1,0:T(8,128)(2,1)S(1)} %pad_maximum_fusion.refs_0_, bf16[4,144,128]{2,1,0:T(8,128)(2,1)S(1)} %collective-permute-done.10.refs_1_, bf16[4,144,128]{2,1,0:T(8,128)(2,1)S(1)} %collective-permute-done.11.refs_2_, ...), custom_call_target="tpu_custom_call" | custom-call | flops 1073741824 | bytes 4194304 | tf_op jit(solution)/shard_map/pallas_call | solution.py:42
  37.6 0.3 collective-permute-start.17
  37.9 1.0 %collective-permute-done.17.got_ref = bf16[128,256]{1,0:T(8,128)(2,1)S(1)} collective-permute-done((bf16[128,256]{1,0:T(8,128)(2,1)S(1)}, bf16[128,256]{1,0:T(8,128)(2,1)S(1)}, u32[]{:S(2)}, u32[]{:S(2)}) %collective-permute-start.17) | collective-permute-done | bytes 65568 | tf_op jit(solution)/shard_map/ppermute | solution.py:26
  38.9 0.5 shard_map.144
  39.4 1.8 %collective-permute-start.19 = (bf16[32,2048]{1,0:T(8,128)(2,1)S(1)}, bf16[32,2048]{1,0:T(8,128)(2,1)S(1)}, u32[]{:S(2)}, u32[]{:S(2)}) collective-permute-start(bf16[32,2048]{1,0:T(8,128)(2,1)S(1)} %get-tuple-element.44), channel_id=1, source_target_pairs={{0,6},{1,7},{2,4},{3,5},{4,2},{5,3},{6,0},{7,1},{8,14},{9,15},{10,... | collective-permute-start | bytes 393224 | tf_op jit(solution)/shard_map/ppermute | solution.py:26
  41.1 1.3 %collective-permute-start.20 = (bf16[32,2048]{1,0:T(8,128)(2,1)S(1)}, bf16[32,2048]{1,0:T(8,128)(2,1)S(1)}, u32[]{:S(2)}, u32[]{:S(2)}) collective-permute-start(bf16[32,2048]{1,0:T(8,128)(2,1)S(1)} %get-tuple-element.45), channel_id=1, source_target_pairs={{0,4},{1,5},{2,6},{3,7},{4,0},{5,1},{6,2},{7,3},{8,12},{9,13},{10,... | collective-permute-start | bytes 393224 | tf_op jit(solution)/shard_map/ppermute | solution.py:26
  42.4 0.5 collective-permute-start.21
  42.9 3.8 %collective-permute-done.19 = bf16[32,2048]{1,0:T(8,128)(2,1)S(1)} collective-permute-done((bf16[32,2048]{1,0:T(8,128)(2,1)S(1)}, bf16[32,2048]{1,0:T(8,128)(2,1)S(1)}, u32[]{:S(2)}, u32[]{:S(2)}) %collective-permute-start.19) | collective-permute-done | bytes 131104 | tf_op jit(solution)/shard_map/ppermute | solution.py:26
  46.7 2.1 %collective-permute-done.20 = bf16[32,2048]{1,0:T(8,128)(2,1)S(1)} collective-permute-done((bf16[32,2048]{1,0:T(8,128)(2,1)S(1)}, bf16[32,2048]{1,0:T(8,128)(2,1)S(1)}, u32[]{:S(2)}, u32[]{:S(2)}) %collective-permute-start.20) | collective-permute-done | bytes 131104 | tf_op jit(solution)/shard_map/ppermute | solution.py:26
  48.9 0.7 %add_convert_fusion = bf16[32,2048]{1,0:T(8,128)(2,1)} fusion(bf16[32,2048]{1,0:T(8,128)(2,1)S(1)} %collective-permute-done.21, bf16[32,2048]{1,0:T(8,128)(2,1)S(1)} %collective-permute-done.20, f32[32,2048]{1,0:T(8,128)S(1)} %get-tuple-element.43, bf16[32,2048]{1,0:T(8,128)(2,1)S(1)} %collective-permute-done.19), kind=kLoop, calls=%fused_computation | loop fusion | flops 458752 | bytes 786432 | tf_op jit(solution)/shard_map/convert_element_type | solution.py:421
  (29 shorter events, 0.3 us)
Async XLA Ops:
  0.6 8.2 %collective-permute-start.2 = (bf16[256,256]{1,0:T(8,128)(2,1)}, bf16[256,256]{1,0:T(8,128)(2,1)S(1)}, u32[]{:S(2)}, u32[]{:S(2)}) collective-permute-start(bf16[256,256]{1,0:T(8,128)(2,1)} %refs_0_.1), channel_id=1, source_target_pairs={{0,6},{1,7},{2,4},{3,5},{4,2},{5,3},{6,0},{7,1},{8,14},{9,15},{10,... | collective-permute-start | bytes 393224 | tf_op jit(solution)/shard_map/ppermute | solution.py:26
  4.6 6.5 %collective-permute-start.1 = (bf16[256,256]{1,0:T(8,128)(2,1)}, bf16[256,256]{1,0:T(8,128)(2,1)S(1)}, u32[]{:S(2)}, u32[]{:S(2)}) collective-permute-start(bf16[256,256]{1,0:T(8,128)(2,1)} %refs_0_.1), channel_id=1, source_target_pairs={{0,4},{1,5},{2,6},{3,7},{4,0},{5,1},{6,2},{7,3},{8,12},{9,13},{10,... | collective-permute-start | bytes 393224 | tf_op jit(solution)/shard_map/ppermute | solution.py:26
  5.1 6.3 %collective-permute-start = (bf16[256,256]{1,0:T(8,128)(2,1)}, bf16[256,256]{1,0:T(8,128)(2,1)S(1)}, u32[]{:S(2)}, u32[]{:S(2)}) collective-permute-start(bf16[256,256]{1,0:T(8,128)(2,1)} %refs_0_.1), channel_id=1, source_target_pairs={{0,2},{1,3},{2,0},{3,1},{4,6},{5,7},{6,4},{7,5},{8,10},{9,11},{10,... | collective-permute-start | bytes 393224 | tf_op jit(solution)/shard_map/ppermute | solution.py:26
  5.3 9.1 %collective-permute-start.3 = (bf16[256,256]{1,0:T(8,128)(2,1)}, bf16[256,256]{1,0:T(8,128)(2,1)S(1)}, u32[]{:S(2)}, u32[]{:S(2)}) collective-permute-start(bf16[256,256]{1,0:T(8,128)(2,1)} %refs_0_.1), channel_id=1, source_target_pairs={{0,1},{1,0},{2,3},{3,2},{4,5},{5,4},{6,7},{7,6},{8,9},{9,8},{10,11... | collective-permute-start | bytes 393224 | tf_op jit(solution)/shard_map/ppermute | solution.py:26
  8.8 5.6 %collective-permute-start.6 = (bf16[256,256]{1,0:T(8,128)(2,1)S(1)}, bf16[256,256]{1,0:T(8,128)(2,1)S(1)}, u32[]{:S(2)}, u32[]{:S(2)}) collective-permute-start(bf16[256,256]{1,0:T(8,128)(2,1)S(1)} %collective-permute-done.2.refs_3_), channel_id=1, source_target_pairs={{0,1},{1,0},{2,3},{3,2},{4,5},{5,4},{6,7},{7,6},{8,9},{9,8},{10,11... | collective-permute-start | bytes 393224 | tf_op jit(solution)/shard_map/ppermute | solution.py:26
  11.1 3.3 %collective-permute-start.5 = (bf16[256,256]{1,0:T(8,128)(2,1)S(1)}, bf16[256,256]{1,0:T(8,128)(2,1)S(1)}, u32[]{:S(2)}, u32[]{:S(2)}) collective-permute-start(bf16[256,256]{1,0:T(8,128)(2,1)S(1)} %collective-permute-done.1.refs_2_), channel_id=1, source_target_pairs={{0,1},{1,0},{2,3},{3,2},{4,5},{5,4},{6,7},{7,6},{8,9},{9,8},{10,11... | collective-permute-start | bytes 393224 | tf_op jit(solution)/shard_map/ppermute | solution.py:26
  11.4 3.0 %collective-permute-start.4 = (bf16[256,256]{1,0:T(8,128)(2,1)S(1)}, bf16[256,256]{1,0:T(8,128)(2,1)S(1)}, u32[]{:S(2)}, u32[]{:S(2)}) collective-permute-start(bf16[256,256]{1,0:T(8,128)(2,1)S(1)} %collective-permute-done.refs_1_), channel_id=1, source_target_pairs={{0,1},{1,0},{2,3},{3,2},{4,5},{5,4},{6,7},{7,6},{8,9},{9,8},{10,11... | collective-permute-start | bytes 393224 | tf_op jit(solution)/shard_map/ppermute | solution.py:26
  11.7 2.8 %copy-start.1 = (bf16[256,256]{1,0:T(8,128)(2,1)S(1)}, bf16[256,256]{1,0:T(8,128)(2,1)}, u32[]{:S(2)}) copy-start(bf16[256,256]{1,0:T(8,128)(2,1)} %refs_0_.1) | copy-start | bytes 393220
  14.1 0.7 %copy-start.2 = (f32[2048]{0:T(1024)S(1)}, f32[2048]{0:T(1024)}, u32[]{:S(2)}) copy-start(f32[2048]{0:T(1024)} %param.14) | copy-start | bytes 24580
  14.1 24.8 %collective-permute-start.18 = (bf16[256,2048]{1,0:T(8,128)(2,1)S(1)}, bf16[256,2048]{1,0:T(8,128)(2,1)S(1)}, u32[]{:S(2)}, u32[]{:S(2)}) collective-permute-start(bf16[256,2048]{1,0:T(8,128)(2,1)S(1)} %get-tuple-element.42.own_w_ref), channel_id=1, source_target_pairs={{0,1},{1,0},{2,3},{3,2},{4,5},{5,4},{6,7},{7,6},{8,9},{9,8},{10,11... | collective-permute-start | bytes 3145736 | tf_op jit(solution)/shard_map/ppermute | solution.py:26
  15.9 18.3 %copy-start = (bf16[2048,128]{1,0:T(8,128)(2,1)S(1)}, bf16[2048,128]{1,0:T(8,128)(2,1)}, u32[]{:S(2)}) copy-start(bf16[2048,128]{1,0:T(8,128)(2,1)} %gate_w_ref.1) | copy-start | bytes 1572868
  15.9 5.8 %collective-permute-start.9 = (bf16[152,128]{1,0:T(8,128)(2,1)S(1)}, bf16[152,128]{1,0:T(8,128)(2,1)S(1)}, u32[]{:S(2)}, u32[]{:S(2)}) collective-permute-start(bf16[152,128]{1,0:T(8,128)(2,1)S(1)} %get-tuple-element.29.refs_8_), channel_id=1, source_target_pairs={{0,24},{8,16},{16,8},{24,0},{1,25},{9,17},{17,9},{25,1},{2,26},{10... | collective-permute-start | bytes 116744 | tf_op jit(solution)/shard_map/ppermute | solution.py:26
  19.8 4.9 %collective-permute-start.8 = (bf16[152,128]{1,0:T(8,128)(2,1)S(1)}, bf16[152,128]{1,0:T(8,128)(2,1)S(1)}, u32[]{:S(2)}, u32[]{:S(2)}) collective-permute-start(bf16[152,128]{1,0:T(8,128)(2,1)S(1)} %get-tuple-element.29.refs_8_), channel_id=1, source_target_pairs={{0,16},{8,24},{16,0},{24,8},{1,17},{9,25},{17,1},{25,9},{2,18},{10... | collective-permute-start | bytes 116744 | tf_op jit(solution)/shard_map/ppermute | solution.py:26
  19.8 4.9 %collective-permute-start.7 = (bf16[152,128]{1,0:T(8,128)(2,1)S(1)}, bf16[152,128]{1,0:T(8,128)(2,1)S(1)}, u32[]{:S(2)}, u32[]{:S(2)}) collective-permute-start(bf16[152,128]{1,0:T(8,128)(2,1)S(1)} %get-tuple-element.29.refs_8_), channel_id=1, source_target_pairs={{0,8},{8,0},{16,24},{24,16},{1,9},{9,1},{17,25},{25,17},{2,10},{10... | collective-permute-start | bytes 116744 | tf_op jit(solution)/shard_map/ppermute | solution.py:26
  24.7 7.5 %collective-permute-start.12 = (bf16[4,144,128]{2,1,0:T(8,128)(2,1)S(1)}, bf16[4,144,128]{2,1,0:T(8,128)(2,1)S(1)}, u32[]{:S(2)}, u32[]{:S(2)}) collective-permute-start(bf16[4,144,128]{2,1,0:T(8,128)(2,1)S(1)} %pad_maximum_fusion.refs_0_), channel_id=1, source_target_pairs={{0,6},{1,7},{2,4},{3,5},{4,2},{5,3},{6,0},{7,1},{8,14},{9,15},{10,... | collective-permute-start | bytes 442376 | tf_op jit(solution)/shard_map/ppermute | solution.py:26
  26.5 7.1 %collective-permute-start.11 = (bf16[4,144,128]{2,1,0:T(8,128)(2,1)S(1)}, bf16[4,144,128]{2,1,0:T(8,128)(2,1)S(1)}, u32[]{:S(2)}, u32[]{:S(2)}) collective-permute-start(bf16[4,144,128]{2,1,0:T(8,128)(2,1)S(1)} %pad_maximum_fusion.refs_0_), channel_id=1, source_target_pairs={{0,4},{1,5},{2,6},{3,7},{4,0},{5,1},{6,2},{7,3},{8,12},{9,13},{10,... | collective-permute-start | bytes 442376 | tf_op jit(solution)/shard_map/ppermute | solution.py:26
  27.7 5.9 %collective-permute-start.10 = (bf16[4,144,128]{2,1,0:T(8,128)(2,1)S(1)}, bf16[4,144,128]{2,1,0:T(8,128)(2,1)S(1)}, u32[]{:S(2)}, u32[]{:S(2)}) collective-permute-start(bf16[4,144,128]{2,1,0:T(8,128)(2,1)S(1)} %pad_maximum_fusion.refs_0_), channel_id=1, source_target_pairs={{0,2},{1,3},{2,0},{3,1},{4,6},{5,7},{6,4},{7,5},{8,10},{9,11},{10,... | collective-permute-start | bytes 442376 | tf_op jit(solution)/shard_map/ppermute | solution.py:26
  28.3 6.7 %collective-permute-start.13 = (bf16[4,144,128]{2,1,0:T(8,128)(2,1)S(1)}, bf16[4,144,128]{2,1,0:T(8,128)(2,1)S(1)}, u32[]{:S(2)}, u32[]{:S(2)}) collective-permute-start(bf16[4,144,128]{2,1,0:T(8,128)(2,1)S(1)} %pad_maximum_fusion.refs_0_), channel_id=1, source_target_pairs={{0,1},{1,0},{2,3},{3,2},{4,5},{5,4},{6,7},{7,6},{8,9},{9,8},{10,11... | collective-permute-start | bytes 442376 | tf_op jit(solution)/shard_map/ppermute | solution.py:26
  32.2 2.8 %collective-permute-start.16 = (bf16[4,144,128]{2,1,0:T(8,128)(2,1)S(1)}, bf16[4,144,128]{2,1,0:T(8,128)(2,1)S(1)}, u32[]{:S(2)}, u32[]{:S(2)}) collective-permute-start(bf16[4,144,128]{2,1,0:T(8,128)(2,1)S(1)} %collective-permute-done.12.refs_3_), channel_id=1, source_target_pairs={{0,1},{1,0},{2,3},{3,2},{4,5},{5,4},{6,7},{7,6},{8,9},{9,8},{10,11... | collective-permute-start | bytes 442376 | tf_op jit(solution)/shard_map/ppermute | solution.py:26
  33.6 1.4 %collective-permute-start.15 = (bf16[4,144,128]{2,1,0:T(8,128)(2,1)S(1)}, bf16[4,144,128]{2,1,0:T(8,128)(2,1)S(1)}, u32[]{:S(2)}, u32[]{:S(2)}) collective-permute-start(bf16[4,144,128]{2,1,0:T(8,128)(2,1)S(1)} %collective-permute-done.11.refs_2_), channel_id=1, source_target_pairs={{0,1},{1,0},{2,3},{3,2},{4,5},{5,4},{6,7},{7,6},{8,9},{9,8},{10,11... | collective-permute-start | bytes 442376 | tf_op jit(solution)/shard_map/ppermute | solution.py:26
  33.7 1.6 %collective-permute-start.14 = (bf16[4,144,128]{2,1,0:T(8,128)(2,1)S(1)}, bf16[4,144,128]{2,1,0:T(8,128)(2,1)S(1)}, u32[]{:S(2)}, u32[]{:S(2)}) collective-permute-start(bf16[4,144,128]{2,1,0:T(8,128)(2,1)S(1)} %collective-permute-done.10.refs_1_), channel_id=1, source_target_pairs={{0,1},{1,0},{2,3},{3,2},{4,5},{5,4},{6,7},{7,6},{8,9},{9,8},{10,11... | collective-permute-start | bytes 442376 | tf_op jit(solution)/shard_map/ppermute | solution.py:26
  37.6 1.3 %collective-permute-start.17 = (bf16[128,256]{1,0:T(8,128)(2,1)S(1)}, bf16[128,256]{1,0:T(8,128)(2,1)S(1)}, u32[]{:S(2)}, u32[]{:S(2)}) collective-permute-start(bf16[128,256]{1,0:T(8,128)(2,1)S(1)} %get-tuple-element.41), channel_id=1, source_target_pairs={{0,1},{1,0},{2,3},{3,2},{4,5},{5,4},{6,7},{7,6},{8,9},{9,8},{10,11... | collective-permute-start | bytes 196616 | tf_op jit(solution)/shard_map/ppermute | solution.py:26
  39.4 7.4 %collective-permute-start.19 = (bf16[32,2048]{1,0:T(8,128)(2,1)S(1)}, bf16[32,2048]{1,0:T(8,128)(2,1)S(1)}, u32[]{:S(2)}, u32[]{:S(2)}) collective-permute-start(bf16[32,2048]{1,0:T(8,128)(2,1)S(1)} %get-tuple-element.44), channel_id=1, source_target_pairs={{0,6},{1,7},{2,4},{3,5},{4,2},{5,3},{6,0},{7,1},{8,14},{9,15},{10,... | collective-permute-start | bytes 393224 | tf_op jit(solution)/shard_map/ppermute | solution.py:26
  41.1 7.7 %collective-permute-start.20 = (bf16[32,2048]{1,0:T(8,128)(2,1)S(1)}, bf16[32,2048]{1,0:T(8,128)(2,1)S(1)}, u32[]{:S(2)}, u32[]{:S(2)}) collective-permute-start(bf16[32,2048]{1,0:T(8,128)(2,1)S(1)} %get-tuple-element.45), channel_id=1, source_target_pairs={{0,4},{1,5},{2,6},{3,7},{4,0},{5,1},{6,2},{7,3},{8,12},{9,13},{10,... | collective-permute-start | bytes 393224 | tf_op jit(solution)/shard_map/ppermute | solution.py:26
  42.4 6.5 %collective-permute-start.21 = (bf16[32,2048]{1,0:T(8,128)(2,1)S(1)}, bf16[32,2048]{1,0:T(8,128)(2,1)S(1)}, u32[]{:S(2)}, u32[]{:S(2)}) collective-permute-start(bf16[32,2048]{1,0:T(8,128)(2,1)S(1)} %get-tuple-element.46), channel_id=1, source_target_pairs={{0,2},{1,3},{2,0},{3,1},{4,6},{5,7},{6,4},{7,5},{8,10},{9,11},{10,... | collective-permute-start | bytes 393224 | tf_op jit(solution)/shard_map/ppermute | solution.py:26
where the time goes:
time: 49.8 us; the launch traced here: 49.6 us
  waiting for transfers between devices  22.9 us (46%)
  starting transfers between devices  17.6 us (35%)
  Pallas kernels  7.21 us (14%)
  between operations  0.75 us (2%)
  other arithmetic  0.74 us (1%)
    ppermute x22, waiting for transfers between devices, swap(): return lax.ppermute(array, axis, [(i, i ^ mask) for i in range(peers)])  22.9 us
    ppermute x22, starting transfers between devices, swap(): return lax.ppermute(array, axis, [(i, i ^ mask) for i in range(peers)])  17.6 us
    pallas_call x5, Pallas kernels, call(): pl.pallas_call(body, out_shape=[jax.ShapeDtypeStruct(shape, dtype) for sh...  7.21 us
  transfers between devices with their start and end apart: 22, of which 12 were waited for; matrix products, arithmetic and copies ran while one was open for 0% of the time, Pallas kernels for 14%

commit v1 on v0

v1 whole, which is shorter than its diff:
```python
import functools
import math

import jax
import jax.numpy as jnp
from jax import lax
from jax.experimental import pallas as pl
from jax.experimental.pallas import tpu as pltpu
from jax.sharding import PartitionSpec as P


NOPE = 128
ROPE = 64
VDIM = 128
GRID_W = 64
EPSILON = 1e-06
ROPE_BASE = 10000.0
LANES = 128
HALO = 8
F32 = jnp.float32
BF16 = jnp.bfloat16


def swap(array, axis, mask):
    peers = lax.axis_size(axis)
    return lax.ppermute(array, axis, [(i, i ^ mask) for i in range(peers)])


def exchange(array, axis, stride, peers):
    pieces = []
    for i in reversed(range(1, peers)):
        pieces.append(swap(array, axis, stride * i))
    return pieces[::-1]


def swap_each(arrays):
    pieces = []
    for array in arrays:
        pieces.append(swap(array, "tp", 1))
    return pieces


def kernel_call(body, outs, limit, scratch=(), flops=0, nbytes=0, in_hbm=()):
    whole = pl.BlockSpec(memory_space=pltpu.VMEM)

    def call(*operands):
        spaces = [pltpu.HBM if i in in_hbm else pltpu.VMEM for i in range(len(operands))]
        operands = [
            pltpu.with_memory_space_constraint(operand, space) if space is pltpu.HBM else operand
            for operand, space in zip(operands, spaces, strict=True)
        ]
        return pl.pallas_call(
            body,
            out_shape=[jax.ShapeDtypeStruct(shape, dtype) for shape, dtype in outs],
            in_specs=[pl.BlockSpec(memory_space=space) for space in spaces],
            out_specs=[whole] * len(outs),
            scratch_shapes=list(scratch),
            compiler_params=pltpu.CompilerParams(vmem_limit_bytes=limit),
            cost_estimate=pl.CostEstimate(flops=flops, bytes_accessed=nbytes, transcendentals=0),
        )(*operands)

    return call


def rotate(values, cosines, sines):
    quarter = ROPE // 4
    lane = lax.broadcasted_iota(jnp.int32, values.shape, 1)
    first = (lane // quarter) % 2 == 0
    ahead = pltpu.roll(values, LANES - quarter, 1)
    behind = pltpu.roll(values, quarter, 1)
    return values * cosines + jnp.where(first, ahead, behind) * sines


def low_lanes(shape):
    return lax.broadcasted_iota(jnp.int32, shape, 1) < ROPE


def prepare(
    latent_ref, rope_ref, query_ref, pre_ref, value_ref, attend_ref, conv_ref, partner_ref,
    key_w_ref, query_w_ref, mix_w_ref, own_w_ref, cos_ref, sin_ref, sems,
):
    core = lax.axis_index("tp") % 2
    mine = pl.ds(pl.multiple_of(core * ROPE, ROPE), ROPE)
    moves = [
        (latent_ref, key_w_ref.at[mine]),
        (rope_ref, key_w_ref.at[2 * ROPE : 3 * ROPE]),
        (rope_ref, key_w_ref.at[3 * ROPE :]),
        (pre_ref, mix_w_ref.at[:, :LANES]),
        (value_ref, mix_w_ref.at[:, LANES:]),
        (query_ref, query_w_ref.at[: NOPE + ROPE]),
        (query_ref.at[NOPE:], query_w_ref.at[NOPE + ROPE :]),
        (attend_ref, own_w_ref.at[:VDIM]),
        (conv_ref, own_w_ref.at[VDIM:]),
    ]
    copies = [pltpu.make_async_copy(source, target, sems.at[i]) for i, (source, target) in enumerate(moves)]
    for copy in copies:
        copy.start()
    key_w_ref[pl.ds(pl.multiple_of((1 - core) * ROPE, ROPE), ROPE), :] = partner_ref[...]
    quarter = ROPE // 4
    groups = cos_ref.shape[0] // GRID_W
    first_row = lax.axis_index("sp") * groups

    def angles(rows, start):
        lane = lax.broadcasted_iota(jnp.int32, (rows, LANES), 1) % ROPE
        place = (lax.broadcasted_iota(jnp.int32, (rows, LANES), 0) + start).astype(F32)
        inverse = jnp.exp((lane % quarter).astype(F32) * (-math.log(ROPE_BASE) / quarter))
        angle = place * inverse
        sign = jnp.where((lane // quarter) % 2 == 0, -1.0, 1.0)
        return lane < 2 * quarter, jnp.cos(angle), jnp.sin(angle) * sign

    _, row_cos, row_sin = angles(groups, first_row)
    by_row, col_cos, col_sin = angles(GRID_W, 0)
    for g in range(groups):
        rows = slice(g * GRID_W, (g + 1) * GRID_W)
        cos_ref[rows, :] = jnp.where(by_row, row_cos[g : g + 1], col_cos)
        sin_ref[rows, :] = jnp.where(by_row, row_sin[g : g + 1], col_sin)
    for copy in copies:
        copy.wait()


def dot_nt(left, right):
    return lax.dot_general(left, right, (((1,), (1,)), ((), ())), preferred_element_type=F32)


def project_first(pairs, *refs):
    pieces, refs = refs[: 2 * pairs], refs[2 * pairs :]
    gain_ref, key_w_ref, mix_w_ref, cos_ref, sin_ref = refs[:5]
    scaled_ref, inv_ref, message_ref, mix_ref, key_ref = refs[5:]
    rank = lax.axis_index("tp")
    tokens, width = pieces[0].shape
    half = tokens // 2
    total = jnp.zeros((tokens, LANES), F32)
    for i, ref in enumerate(pieces):
        owner = rank ^ (2 * (i % pairs) + i // pairs)
        piece = ref[...].astype(F32)
        squares = piece * piece
        for j in range(width // LANES):
            total = total + squares[:, j * LANES : (j + 1) * LANES]
        columns = pl.ds(pl.multiple_of(owner * width, width), width)
        scaled_ref[:, columns] = (piece * gain_ref[:, columns]).astype(BF16)
    features = 2 * pairs * width
    inv = lax.rsqrt(jnp.sum(total, axis=1, keepdims=True) / features + EPSILON)
    inv_ref[...] = jnp.broadcast_to(inv, inv_ref.shape)
    scaled = scaled_ref[...]
    keys = dot_nt(scaled, key_w_ref[...]) * inv
    mixes = jnp.dot(scaled, mix_w_ref[...], preferred_element_type=F32) * inv
    mix = (mixes[:, :LANES] * mixes[:, LANES:]).astype(BF16)
    mix_ref[...] = mix
    key_ref[...] = keys
    chip, core = rank // 2, rank % 2
    start = pl.multiple_of(core * half, half)
    message_ref[:half, :] = key_ref[pl.ds(start, half), :LANES].astype(BF16)
    share = half // (2 * pairs)
    turned = []
    for base in (0, half // 2):
        rows = pl.ds(pl.multiple_of(start + base + chip * share, share), share)
        turned.append(rotate(key_ref[rows, LANES:], cos_ref[rows, :], sin_ref[rows, :]))
    low = low_lanes((share, LANES))
    message_ref[half : half + share, :] = jnp.where(low, turned[0], turned[1]).astype(BF16)
    row = lax.broadcasted_iota(jnp.int32, (HALO, LANES), 0)
    first = jnp.broadcast_to(mix[:1].astype(F32), (HALO, LANES))
    last = jnp.broadcast_to(mix[tokens - 1 :].astype(F32), (HALO, LANES))
    message_ref[half + share :, :] = jnp.where(row == 0, first, last).astype(BF16)


def project_second(natural, *refs):
    scaled_ref, inv_ref, query_w_ref, gate_w_ref, cos_ref, sin_ref, mix_ref, taps_ref = refs[:8]
    halos, (query_ref, conv_ref) = refs[8:-2], refs[-2:]
    scaled = scaled_ref[...]
    inv = inv_ref[...]
    scale = (NOPE + ROPE) ** (-0.5)
    query = dot_nt(scaled, query_w_ref[...])
    nope = (query[:, :NOPE] * inv * scale).astype(BF16)
    rope = rotate(query[:, NOPE:] * inv, cos_ref[...], sin_ref[...]) * scale
    low = low_lanes(rope.shape)
    query_ref[0, :, :NOPE] = nope
    query_ref[1, :, :NOPE] = nope
    query_ref[0, :, NOPE:] = jnp.where(low, rope, 0.0).astype(BF16)
    query_ref[1, :, NOPE:] = jnp.where(low, 0.0, rope).astype(BF16)

    gate = jnp.dot(scaled, gate_w_ref[...], preferred_element_type=F32) * inv
    mix = mix_ref[...].astype(F32)
    tokens = mix.shape[0]
    place, places = lax.axis_index("sp"), lax.axis_size("sp")

    def edge_of(other, at):
        inside = (other >= 0) & (other < places)
        other = jnp.clip(other, 0, places - 1)
        if natural:
            edges = halos[0][other].astype(F32)
        else:
            edges = jnp.zeros((HALO, LANES), F32)
            for i, ref in enumerate(halos):
                edges = jnp.where((other ^ place) == i, ref[ref.shape[0] - HALO :, :].astype(F32), edges)
        return jnp.where(inside, edges[at : at + 1, :], 0.0)

    row = lax.broadcasted_iota(jnp.int32, mix.shape, 0)
    earlier = jnp.where(row == 0, edge_of(place - 1, 1), pltpu.roll(mix, 1, 0))
    later = jnp.where(row == tokens - 1, edge_of(place + 1, 0), pltpu.roll(mix, tokens - 1, 0))
    taps = taps_ref[...].astype(F32)
    convolved = taps[0:1] * earlier + taps[1:2] * mix + taps[2:3] * later
    conv_ref[...] = (gate * convolved).astype(BF16)


def attend(slots, chunk, last, *refs):
    inputs = 1 + max(place for chip_slots in slots for place, _ in chip_slots)
    pieces, refs = refs[:inputs], refs[inputs:]
    gain_ref, expand_ref, query_ref = refs[:3]
    refs = refs[3:]
    if last:
        stats_in, out_in, conv_ref, keep_ref, send_ref, log_ref = refs[:6]
    else:
        stats_ref, out_ref = refs[:2]
    latent_ref, rope_ref = refs[-2:]
    rank = lax.axis_index("tp")
    chip, core = rank // 2, rank % 2
    pairs = len(slots)
    tokens = query_ref.shape[1]
    half = tokens // 2
    group = half // 2
    share = group // pairs
    entries = pairs * LANES

    views = [(chip ^ i, chip_slots) for i, chip_slots in enumerate(slots)]

    def rows_of(chip_slots, slot, first, start, count):
        place, at = chip_slots[slot if first is None else 0]
        at = at if first is None else first + slot
        rows = slice(start, start + count)
        return pieces[place][rows, :] if at is None else pieces[place][at, rows, :]

    def one_chunk(first, state):
        for slot in range(chunk):
            total = jnp.zeros((half, LANES), F32)
            for owner, chip_slots in views:
                piece = rows_of(chip_slots, slot, first, 0, half).astype(F32)
                total = total + piece * piece
                start = pl.multiple_of(slot * group + owner * share, share)
                rope_ref[pl.ds(start, share), :] = rows_of(chip_slots, slot, first, half, share)
            inv = lax.rsqrt(jnp.sum(total, axis=1, keepdims=True) / entries + EPSILON)
            for owner, chip_slots in views:
                piece = rows_of(chip_slots, slot, first, 0, half).astype(F32)
                columns = pl.ds(pl.multiple_of(owner * LANES, LANES), LANES)
                scaled = (piece * inv * gain_ref[:, columns]).astype(BF16)
                for side in range(2):
                    base = (side * chunk + slot) * group
                    latent_ref[base : base + group, columns] = scaled[side * group : (side + 1) * group]
        latent = latent_ref[...]
        keys = jnp.dot(latent, expand_ref[:, :NOPE], preferred_element_type=F32).astype(BF16)
        values = lax.dot_general(
            expand_ref[:, NOPE:], latent, (((0,), (1,)), ((), ())), preferred_element_type=F32
        ).astype(BF16)
        rope = rope_ref[...]
        count = chunk * group
        scores = [
            dot_nt(jnp.concatenate([keys[i * count : (i + 1) * count], rope], axis=1), query_ref[i])
            for i in range(2)
        ]
        peak = jnp.max(jnp.maximum(*scores), axis=0, keepdims=True)
        if state is not None:
            peak = jnp.maximum(peak, state[0])
        weights = [jnp.exp(piece - peak) for piece in scores]
        total = jnp.sum(weights[0] + weights[1], axis=0, keepdims=True)
        out = sum(
            jnp.dot(values[:, i * count : (i + 1) * count], weights[i].astype(BF16), preferred_element_type=F32)
            for i in range(2)
        )
        if state is not None:
            rescale = jnp.exp(state[0] - peak)
            total = total + state[1] * rescale
            out = out + state[2] * rescale
        return peak, total, out

    state = (stats_in[0:1], stats_in[1:2], out_in[...]) if last else None
    if chunk == len(views[0][1]):
        peak, total, out = one_chunk(None, state)
    else:
        if state is None:
            state = (
                jnp.full((1, tokens), -jnp.inf, F32),
                jnp.zeros((1, tokens), F32),
                jnp.zeros((VDIM, tokens), F32),
            )
        steps = len(views[0][1]) // chunk
        peak, total, out = lax.fori_loop(0, steps, lambda i, state: one_chunk(i * chunk, state), state)
    if not last:
        stats_ref[0:1] = peak
        stats_ref[1:2] = total
        out_ref[...] = out
        return
    log_ref[...] = peak + jnp.log(total)
    attended = jnp.transpose(out / total)
    rows = tokens // (2 * pairs)
    attend_ref = refs[-3]
    attend_ref[...] = attended.astype(BF16)
    for i in range(pairs):
        base = 2 * (chip ^ i)
        for ref, at in ((keep_ref, base + core), (send_ref, base + 1 - core)):
            source = pl.ds(pl.multiple_of(at * rows, rows), rows)
            ref[i * rows : (i + 1) * rows, :VDIM] = attend_ref[source, :]
            ref[i * rows : (i + 1) * rows, VDIM:] = conv_ref[source, :]


def output(keep_ref, got_ref, own_w_ref, other_w_ref, first_ref, *rest_refs):
    out = jnp.dot(keep_ref[...], own_w_ref[...], preferred_element_type=F32)
    out = out + jnp.dot(got_ref[...], other_w_ref[...], preferred_element_type=F32)
    rows = first_ref.shape[0]
    first_ref[...] = out[:rows]
    for i, ref in enumerate(rest_refs):
        ref[...] = out[(i + 1) * rows : (i + 2) * rows].astype(BF16)


def body(
    activations,
    norm_gain,
    query_weight,
    latent_weight,
    rope_key_weight,
    latent_gain,
    expand_weight,
    gate_weight,
    pre_weight,
    value_weight,
    conv_kernel,
    output_attend,
    output_conv,
):
    ranks = lax.axis_size("tp")
    places = lax.axis_size("sp")
    pairs = ranks // 2
    tokens, width = activations.shape
    features = ranks * width
    half = tokens // 2
    share = half // ranks
    rows = tokens // ranks
    channels = gate_weight.shape[1]

    even = [activations] + exchange(activations, "tp", 2, pairs)
    odd = swap_each(even)

    latent_t = latent_weight.T
    partner_t = swap(latent_t, "tp", 1)
    key_w, query_w, mix_w, own_w, cosines, sines = kernel_call(
        prepare,
        [
            ((4 * ROPE, features), BF16),
            ((NOPE + 2 * ROPE, features), BF16),
            ((features, 2 * LANES), BF16),
            ((VDIM + channels, features), BF16),
            ((tokens, LANES), F32),
            ((tokens, LANES), F32),
        ],
        16 << 20,
        scratch=[pltpu.SemaphoreType.DMA((9,))],
        flops=1 << 28,
        nbytes=1 << 23,
        in_hbm=range(7),
    )(
        latent_t, rope_key_weight.T, query_weight.T, pre_weight, value_weight, output_attend, output_conv,
        partner_t,
    )
    other_w = swap(own_w, "tp", 1)

    scaled, inv, message, mix = kernel_call(
        functools.partial(project_first, pairs),
        [
            ((tokens, features), BF16),
            ((tokens, LANES), F32),
            ((half + share + HALO, LANES), BF16),
            ((tokens, channels), BF16),
        ],
        12 << 20,
        scratch=[pltpu.VMEM((tokens, 2 * LANES), F32)],
        flops=2 * tokens * features * 4 * LANES,
        nbytes=4 * tokens * features,
    )(*even, *odd, norm_gain.reshape(1, -1), key_w, mix_w, cosines, sines)

    small = places <= 8 and places & (places - 1) == 0
    if small:
        halos = [message] + exchange(message, "sp", 1, places)
        near = message[: half + share]
        nears = [near] + exchange(near, "tp", 2, pairs)
        near_other = swap(jnp.stack(nears), "tp", 1)
        around = jnp.stack([piece[: half + share] for piece in halos[1:]])
    else:
        around = lax.all_gather(message, "sp", axis=0)
        around, halos = around[:, : half + share], [around[:, half + share :]]
    arounds = [around] + exchange(around, "tp", 2, pairs)
    others = swap_each(arounds)
    blocks = range(places - 1) if small else range(places)
    slots = [[(i, k) for k in blocks] for i in range(pairs)]
    other_slots = slots
    if small:
        other_slots = [[(pairs, i)] + chip_slots for i, chip_slots in enumerate(slots)]
        slots = [[(pairs + i, None)] + chip_slots for i, chip_slots in enumerate(slots)]
        arounds += nears
        others.append(near_other)

    query, conv = kernel_call(
        functools.partial(project_second, not small),
        [((2, tokens, NOPE + LANES), BF16), ((tokens, channels), BF16)],
        12 << 20,
        flops=2 * tokens * features * 3 * LANES,
        nbytes=4 * tokens * features,
    )(scaled, inv, query_w, gate_weight, cosines, sines, mix, conv_kernel, *halos)

    chunk = places if small else 4

    def attend_to(arrays, slots, last, outs, *operands):
        scratch = [
            pltpu.VMEM((tokens, VDIM), BF16),
            pltpu.VMEM((chunk * half, pairs * LANES), BF16),
            pltpu.VMEM((chunk * half // 2, LANES), BF16),
        ]
        return kernel_call(
            functools.partial(attend, slots, chunk, last),
            outs,
            (12 << 20) if small else (40 << 20),
            scratch=scratch if last else scratch[1:],
            flops=1 << 29,
            nbytes=1 << 22,
        )(*arrays, latent_gain.reshape(1, -1), expand_weight, query, *operands)

    stats, out = attend_to(arounds, slots, False, [((8, tokens), F32), ((VDIM, tokens), F32)])
    keep, send, logs = attend_to(
        others,
        other_slots,
        True,
        [((half, VDIM + channels), BF16), ((half, VDIM + channels), BF16), ((1, tokens), F32)],
        stats,
        out,
        conv,
    )

    got = swap(send, "tp", 1)
    outs = kernel_call(
        output,
        [((rows, features), F32)] + [((rows, features), BF16)] * (pairs - 1),
        12 << 20,
        flops=1 << 28,
        nbytes=1 << 22,
    )(keep, got, own_w, other_w)
    arrived = [swap(outs[i], "tp", 2 * i) for i in reversed(range(1, pairs))]
    total = outs[0]
    for piece in arrived:
        total = total + piece.astype(F32)
    return total.astype(BF16), logs


def solution(mesh):
    return jax.shard_map(
        body,
        mesh=mesh,
        in_specs=(
            P("sp", "tp"),
            P(),
            P(None, "tp"),
            P(None, "tp"),
            P(),
            P(),
            P(None, "tp"),
            P(None, "tp"),
            P(None, "tp"),
            P(None, "tp"),
            P(None, "tp"),
            P("tp", None),
            P("tp", None),
        ),
        out_specs=(P(("sp", "tp"), None), P("tp", "sp")),
        check_vma=False,
    )
```

time: 49.8 us -> 51.8 us (1.040)
  starting transfers between devices: 17.6 us -> 22.2 us
  waiting for transfers between devices: 22.9 us -> 18.4 us
  local copies, waits for them, and re-layouts: 0.37 us -> 2.04 us
    ppermute x22 -> x27, starting transfers between devices: 17.6 us -> 22.2 us  [swap(): return lax.ppermute(array, axis, [(i, i ^ mask) for i in range(peers)])]
    ppermute x22 -> x27, waiting for transfers between devices: 22.9 us -> 18.4 us  [swap(): return lax.ppermute(array, axis, [(i, i ^ mask) for i in range(peers)])]
    unnamed x6 -> x12, local copies, waits for them, and re-layouts: 0.36 us -> 2.02 us
    pallas_call x5 -> x6, Pallas kernels: 7.21 us -> 7.37 us  [call(): pl.pallas_call(body, out_shape=[jax.ShapeDtypeStruct(shape, dtype) for sh...]
  transfers between devices with their start and end apart: 22 -> 27, of which waited for: 12 -> 9; matrix products, arithmetic and copies ran while one was open for 0% -> 0% of each run, Pallas kernels for 14% -> 11%
where the time goes in v1:
time: 51.8 us; the launch traced here: 51.5 us
  starting transfers between devices  22.2 us (43%)
  waiting for transfers between devices  18.4 us (36%)
  Pallas kernels  7.37 us (14%)
  local copies, waits for them, and re-layouts  2.04 us (4%)
  between operations  0.81 us (2%)
  other arithmetic  0.76 us (1%)
    ppermute x27, starting transfers between devices, swap(): return lax.ppermute(array, axis, [(i, i ^ mask) for i in range(peers)])  22.2 us
    ppermute x27, waiting for transfers between devices, swap(): return lax.ppermute(array, axis, [(i, i ^ mask) for i in range(peers)])  18.4 us
    pallas_call x6, Pallas kernels, call(): pl.pallas_call(body, out_shape=[jax.ShapeDtypeStruct(shape, dtype) for sh...  7.37 us
    unnamed x12, local copies, waits for them, and re-layouts  2.02 us
  transfers between devices with their start and end apart: 27, of which 9 were waited for; matrix products, arithmetic and copies ran while one was open for 0% of the time, Pallas kernels for 11%

profile of v1, /device:TPU:0, one launch (start us, length us, event | category | flops | bytes accessed | tf_op | source)
XLA Modules:
  0.0 51.5 jit_solution(7975965132399309393)
XLA Ops:
  0.6 0.6 %collective-permute-start.7 = (bf16[64,2048]{1,0:T(8,128)(2,1)}, bf16[64,2048]{1,0:T(8,128)(2,1)S(1)}, u32[]{:S(2)}, u32[]{:S(2)}) collective-permute-start(bf16[64,2048]{1,0:T(8,128)(2,1)} %bitcast.23), channel_id=1, source_target_pairs={{0,1},{1,0},{2,3},{3,2},{4,5},{5,4},{6,7},{7,6},{8,9},{9,8},{10,11... | collective-permute-start | bytes 786440 | tf_op jit(solution)/shard_map/ppermute | solution.py:26
  1.2 3.5 %collective-permute-start.2 = (bf16[256,256]{1,0:T(8,128)(2,1)}, bf16[256,256]{1,0:T(8,128)(2,1)S(1)}, u32[]{:S(2)}, u32[]{:S(2)}) collective-permute-start(bf16[256,256]{1,0:T(8,128)(2,1)} %refs_0_.1), channel_id=1, source_target_pairs={{0,6},{1,7},{2,4},{3,5},{4,2},{5,3},{6,0},{7,1},{8,14},{9,15},{10,... | collective-permute-start | bytes 393224 | tf_op jit(solution)/shard_map/ppermute | solution.py:26
  4.7 0.5 collective-permute-start.1
  5.3 3.8 %collective-permute-done.2.refs_3_ = bf16[256,256]{1,0:T(8,128)(2,1)S(1)} collective-permute-done((bf16[256,256]{1,0:T(8,128)(2,1)}, bf16[256,256]{1,0:T(8,128)(2,1)S(1)}, u32[]{:S(2)}, u32[]{:S(2)}) %collective-permute-start.2) | collective-permute-done | bytes 131104 | tf_op jit(solution)/shard_map/ppermute | solution.py:26
  9.2 2.6 %collective-permute-done.1.refs_2_ = bf16[256,256]{1,0:T(8,128)(2,1)S(1)} collective-permute-done((bf16[256,256]{1,0:T(8,128)(2,1)}, bf16[256,256]{1,0:T(8,128)(2,1)S(1)}, u32[]{:S(2)}, u32[]{:S(2)}) %collective-permute-start.1) | collective-permute-done | bytes 131104 | tf_op jit(solution)/shard_map/ppermute | solution.py:26
  12.3 2.2 %shard_map.140 = (bf16[256,2048]{1,0:T(8,128)(2,1)S(1)}, bf16[256,2048]{1,0:T(8,128)(2,1)S(1)}, bf16[2048,256]{1,0:T(8,128)(2,1)S(1)}, bf16[256,2048]{1,0:T(8,12...) custom-call(bf16[64,2048]{1,0:T(8,128)(2,1)} %bitcast.24, bf16[64,2048]{1,0:T(8,128)(2,1)} %bitcast.25, ...), custom_call_target="tpu_custom_call" | custom-call | flops 268435456 | bytes 8388608 | tf_op jit(solution)/shard_map/pallas_call | solution.py:52
  14.6 0.6 %copy-done.2 = f32[2048]{0:T(1024)S(1)} copy-done((f32[2048]{0:T(1024)S(1)}, f32[2048]{0:T(1024)}, u32[]{:S(2)}) %copy-start.2) | copy-done | bytes 8216
  15.2 1.1 %shard_map.141 = (bf16[256,2048]{1,0:T(8,128)(2,1)S(1)}, f32[256,128]{1,0:T(8,128)S(1)}, bf16[152,128]{1,0:T(8,128)(2,1)S(1)}, bf16[256,128]{1,0:T(8,128)(2,1)S(1)}) custom-call(bf16[256,256]{1,0:T(8,128)(2,1)S(1)} %copy-done.1, bf16[256,256]{1,0:T(8,128)(2,1)S(1)} %collective-permute-done.refs_1_, bf16[256,256]{1,0:T(8,128)(2,1)S(1)} %collective-permute-done.1.refs_2_, ...), custom_call_target="tpu_custom_call" | custom-call | flops 536870912 | bytes 2097152 | tf_op jit(solution)/shard_map/pallas_call | solution.py:52
  16.4 3.9 %collective-permute-start.10 = (bf16[152,128]{1,0:T(8,128)(2,1)S(1)}, bf16[152,128]{1,0:T(8,128)(2,1)S(1)}, u32[]{:S(2)}, u32[]{:S(2)}) collective-permute-start(bf16[152,128]{1,0:T(8,128)(2,1)S(1)} %get-tuple-element.27.refs_8_), channel_id=1, source_target_pairs={{0,24},{8,16},{16,8},{24,0},{1,25},{9,17},{17,9},{25,1},{2,26},{10... | collective-permute-start | bytes 116744 | tf_op jit(solution)/shard_map/ppermute | solution.py:26
  20.2 0.6 %collective-permute-start.8 = (bf16[152,128]{1,0:T(8,128)(2,1)S(1)}, bf16[152,128]{1,0:T(8,128)(2,1)S(1)}, u32[]{:S(2)}, u32[]{:S(2)}) collective-permute-start(bf16[152,128]{1,0:T(8,128)(2,1)S(1)} %get-tuple-element.27.refs_8_), channel_id=1, source_target_pairs={{0,8},{8,0},{16,24},{24,16},{1,9},{9,1},{17,25},{25,17},{2,10},{10... | collective-permute-start | bytes 116744 | tf_op jit(solution)/shard_map/ppermute | solution.py:26
  20.9 1.7 %collective-permute-start.20 = (bf16[144,128]{1,0:T(8,128)(2,1)S(1)}, bf16[144,128]{1,0:T(8,128)(2,1)S(1)}, u32[]{:S(2)}, u32[]{:S(2)}) collective-permute-start(bf16[144,128]{1,0:T(8,128)(2,1)S(1)} %get-tuple-element.45.refs_4_), channel_id=1, source_target_pairs={{0,6},{1,7},{2,4},{3,5},{4,2},{5,3},{6,0},{7,1},{8,14},{9,15},{10,... | collective-permute-start | bytes 110600 | tf_op jit(solution)/shard_map/ppermute | solution.py:26
  22.6 1.4 %collective-permute-start.19 = (bf16[144,128]{1,0:T(8,128)(2,1)S(1)}, bf16[144,128]{1,0:T(8,128)(2,1)S(1)}, u32[]{:S(2)}, u32[]{:S(2)}) collective-permute-start(bf16[144,128]{1,0:T(8,128)(2,1)S(1)} %get-tuple-element.45.refs_4_), channel_id=1, source_target_pairs={{0,4},{1,5},{2,6},{3,7},{4,0},{5,1},{6,2},{7,3},{8,12},{9,13},{10,... | collective-permute-start | bytes 110600 | tf_op jit(solution)/shard_map/ppermute | solution.py:26
  24.0 1.1 %collective-permute-done.9.refs_10_ = bf16[152,128]{1,0:T(8,128)(2,1)S(1)} collective-permute-done((bf16[152,128]{1,0:T(8,128)(2,1)S(1)}, bf16[152,128]{1,0:T(8,128)(2,1)S(1)}, u32[]{:S(2)}, u32[]{:S(2)}) %collective-permute-start.9) | collective-permute-done | bytes 38944 | tf_op jit(solution)/shard_map/ppermute | solution.py:26
  25.1 1.5 %collective-permute-start.18 = (bf16[144,128]{1,0:T(8,128)(2,1)S(1)}, bf16[144,128]{1,0:T(8,128)(2,1)S(1)}, u32[]{:S(2)}, u32[]{:S(2)}) collective-permute-start(bf16[144,128]{1,0:T(8,128)(2,1)S(1)} %get-tuple-element.45.refs_4_), channel_id=1, source_target_pairs={{0,2},{1,3},{2,0},{3,1},{4,6},{5,7},{6,4},{7,5},{8,10},{9,11},{10,... | collective-permute-start | bytes 110600 | tf_op jit(solution)/shard_map/ppermute | solution.py:26
  26.6 1.6 %collective-permute-start.16 = (bf16[3,144,128]{2,1,0:T(8,128)(2,1)S(1)}, bf16[3,144,128]{2,1,0:T(8,128)(2,1)S(1)}, u32[]{:S(2)}, u32[]{:S(2)}) collective-permute-start(bf16[3,144,128]{2,1,0:T(8,128)(2,1)S(1)} %pad_maximum_fusion.1.refs_0_), channel_id=1, source_target_pairs={{0,6},{1,7},{2,4},{3,5},{4,2},{5,3},{6,0},{7,1},{8,14},{9,15},{10,... | collective-permute-start | bytes 331784 | tf_op jit(solution)/shard_map/ppermute | solution.py:26
  28.2 0.5 collective-permute-start.14
  28.7 1.5 %collective-permute-start.12 = (bf16[3,144,128]{2,1,0:T(8,128)(2,1)S(1)}, bf16[3,144,128]{2,1,0:T(8,128)(2,1)S(1)}, u32[]{:S(2)}, u32[]{:S(2)}) collective-permute-start(bf16[3,144,128]{2,1,0:T(8,128)(2,1)S(1)} %pad_maximum_fusion.1.refs_0_), channel_id=1, source_target_pairs={{0,2},{1,3},{2,0},{3,1},{4,6},{5,7},{6,4},{7,5},{8,10},{9,11},{10,... | collective-permute-start | bytes 331784 | tf_op jit(solution)/shard_map/ppermute | solution.py:26
  30.2 2.8 %collective-permute-done.16.refs_3_ = bf16[3,144,128]{2,1,0:T(8,128)(2,1)S(1)} collective-permute-done((bf16[3,144,128]{2,1,0:T(8,128)(2,1)S(1)}, bf16[3,144,128]{2,1,0:T(8,128)(2,1)S(1)}, u32[]{:S(2)}, u32[]{:S(2)}) %collective-permute-start.16) | collective-permute-done | bytes 110624 | tf_op jit(solution)/shard_map/ppermute | solution.py:26
  33.1 0.7 %collective-permute-done.14.refs_2_ = bf16[3,144,128]{2,1,0:T(8,128)(2,1)S(1)} collective-permute-done((bf16[3,144,128]{2,1,0:T(8,128)(2,1)S(1)}, bf16[3,144,128]{2,1,0:T(8,128)(2,1)S(1)}, u32[]{:S(2)}, u32[]{:S(2)}) %collective-permute-start.14) | collective-permute-done | bytes 110624 | tf_op jit(solution)/shard_map/ppermute | solution.py:26
  33.8 0.5 collective-permute-start.15
  34.4 0.7 %copy-done.3 = bf16[3,128]{1,0:T(4,128)(2,1)S(1)} copy-done((bf16[3,128]{1,0:T(4,128)(2,1)S(1)}, bf16[3,128]{1,0:T(4,128)(2,1)}, u32[]{:S(2)}) %copy-start.3) | copy-done | bytes 792
  35.1 0.8 %shard_map.142 = (bf16[2,256,256]{2,1,0:T(8,128)(2,1)S(1)}, bf16[256,128]{1,0:T(8,128)(2,1)S(1)}) custom-call(bf16[256,2048]{1,0:T(8,128)(2,1)S(1)} %get-tuple-element.28.refs_0_, f32[256,128]{1,0:T(8,128)S(1)} %get-tuple-element.29.refs_1_, bf16[256,2048]{1,0:T(8,128)(2,1)S(1)} %get-tuple-element.30.refs_2_, bf16[2048,128]{1,0:T(8,128)(2,1)S(1)} %copy-done, ...), custom_call_target="tpu_custom_call" | custom-call | flops 402653184 | bytes 2097152 | tf_op jit(solution)/shard_map/pallas_call | solution.py:52
  36.0 0.6 %copy-done.5 = f32[512]{0:T(512)S(1)} copy-done((f32[512]{0:T(512)S(1)}, f32[512]{0:T(512)}, u32[]{:S(2)}) %copy-start.5) | copy-done | bytes 2072
  36.6 1.1 %shard_map.143 = (f32[8,256]{1,0:T(8,128)S(1)}, f32[128,256]{1,0:T(8,128)S(1)}) custom-call(bf16[3,144,128]{2,1,0:T(8,128)(2,1)S(1)} %pad_maximum_fusion.1.refs_0_, bf16[3,144,128]{2,1,0:T(8,128)(2,1)S(1)} %collective-permute-done.12.refs_1_, bf16[3,144,128]{2,1,0:T(8,128)(2,1)S(1)} %collective-permute-done.14.refs_2_, ...), custom_call_target="tpu_custom_call" | custom-call | flops 536870912 | bytes 4194304 | tf_op jit(solution)/shard_map/pallas_call | solution.py:52
  37.8 1.7 %shard_map.144 = (bf16[128,256]{1,0:T(8,128)(2,1)S(1)}, bf16[128,256]{1,0:T(8,128)(2,1)S(1)}, f32[1,256]{1,0:T(1,128)}) custom-call(bf16[3,144,128]{2,1,0:T(8,128)(2,1)S(1)} %collective-permute-done.11.refs_0_, bf16[3,144,128]{2,1,0:T(8,128)(2,1)S(1)} %collective-permute-done.13.refs_1_, bf16[3,144,128]{2,1,0:T(8,128)(2,1)S(1)} %collective-permute-done.15.refs_2_, ...), custom_call_target="tpu_custom_call" | custom-call | flops 536870912 | bytes 4194304 | tf_op jit(solution)/shard_map/pallas_call | solution.py:52
  39.9 0.9 %collective-permute-done.22.got_ref = bf16[128,256]{1,0:T(8,128)(2,1)S(1)} collective-permute-done((bf16[128,256]{1,0:T(8,128)(2,1)S(1)}, bf16[128,256]{1,0:T(8,128)(2,1)S(1)}, u32[]{:S(2)}, u32[]{:S(2)}) %collective-permute-start.22) | collective-permute-done | bytes 65568 | tf_op jit(solution)/shard_map/ppermute | solution.py:26
  41.3 1.5 %collective-permute-start.24 = (bf16[32,2048]{1,0:T(8,128)(2,1)S(1)}, bf16[32,2048]{1,0:T(8,128)(2,1)S(1)}, u32[]{:S(2)}, u32[]{:S(2)}) collective-permute-start(bf16[32,2048]{1,0:T(8,128)(2,1)S(1)} %get-tuple-element.40), channel_id=1, source_target_pairs={{0,6},{1,7},{2,4},{3,5},{4,2},{5,3},{6,0},{7,1},{8,14},{9,15},{10,... | collective-permute-start | bytes 393224 | tf_op jit(solution)/shard_map/ppermute | solution.py:26
  42.8 1.0 %collective-permute-start.25 = (bf16[32,2048]{1,0:T(8,128)(2,1)S(1)}, bf16[32,2048]{1,0:T(8,128)(2,1)S(1)}, u32[]{:S(2)}, u32[]{:S(2)}) collective-permute-start(bf16[32,2048]{1,0:T(8,128)(2,1)S(1)} %get-tuple-element.41), channel_id=1, source_target_pairs={{0,4},{1,5},{2,6},{3,7},{4,0},{5,1},{6,2},{7,3},{8,12},{9,13},{10,... | collective-permute-start | bytes 393224 | tf_op jit(solution)/shard_map/ppermute | solution.py:26
  43.8 1.1 %collective-permute-start.26 = (bf16[32,2048]{1,0:T(8,128)(2,1)S(1)}, bf16[32,2048]{1,0:T(8,128)(2,1)S(1)}, u32[]{:S(2)}, u32[]{:S(2)}) collective-permute-start(bf16[32,2048]{1,0:T(8,128)(2,1)S(1)} %get-tuple-element.42), channel_id=1, source_target_pairs={{0,2},{1,3},{2,0},{3,1},{4,6},{5,7},{6,4},{7,5},{8,10},{9,11},{10,... | collective-permute-start | bytes 393224 | tf_op jit(solution)/shard_map/ppermute | solution.py:26
  44.8 3.8 %collective-permute-done.24 = bf16[32,2048]{1,0:T(8,128)(2,1)S(1)} collective-permute-done((bf16[32,2048]{1,0:T(8,128)(2,1)S(1)}, bf16[32,2048]{1,0:T(8,128)(2,1)S(1)}, u32[]{:S(2)}, u32[]{:S(2)}) %collective-permute-start.24) | collective-permute-done | bytes 131104 | tf_op jit(solution)/shard_map/ppermute | solution.py:26
  48.7 2.1 %collective-permute-done.25 = bf16[32,2048]{1,0:T(8,128)(2,1)S(1)} collective-permute-done((bf16[32,2048]{1,0:T(8,128)(2,1)S(1)}, bf16[32,2048]{1,0:T(8,128)(2,1)S(1)}, u32[]{:S(2)}, u32[]{:S(2)}) %collective-permute-start.25) | collective-permute-done | bytes 131104 | tf_op jit(solution)/shard_map/ppermute | solution.py:26
  50.8 0.7 %add_convert_fusion = bf16[32,2048]{1,0:T(8,128)(2,1)} fusion(bf16[32,2048]{1,0:T(8,128)(2,1)S(1)} %collective-permute-done.26, bf16[32,2048]{1,0:T(8,128)(2,1)S(1)} %collective-permute-done.25, f32[32,2048]{1,0:T(8,128)S(1)} %get-tuple-element.39, bf16[32,2048]{1,0:T(8,128)(2,1)S(1)} %collective-permute-done.24), kind=kLoop, calls=%fused_computation | loop fusion | flops 458752 | bytes 786432 | tf_op jit(solution)/shard_map/convert_element_type | solution.py:447
  (47 shorter events, 1.9 us)
Async XLA Ops:
  0.6 11.7 %collective-permute-start.7 = (bf16[64,2048]{1,0:T(8,128)(2,1)}, bf16[64,2048]{1,0:T(8,128)(2,1)S(1)}, u32[]{:S(2)}, u32[]{:S(2)}) collective-permute-start(bf16[64,2048]{1,0:T(8,128)(2,1)} %bitcast.23), channel_id=1, source_target_pairs={{0,1},{1,0},{2,3},{3,2},{4,5},{5,4},{6,7},{7,6},{8,9},{9,8},{10,11... | collective-permute-start | bytes 786440 | tf_op jit(solution)/shard_map/ppermute | solution.py:26
  1.2 8.0 %collective-permute-start.2 = (bf16[256,256]{1,0:T(8,128)(2,1)}, bf16[256,256]{1,0:T(8,128)(2,1)S(1)}, u32[]{:S(2)}, u32[]{:S(2)}) collective-permute-start(bf16[256,256]{1,0:T(8,128)(2,1)} %refs_0_.1), channel_id=1, source_target_pairs={{0,6},{1,7},{2,4},{3,5},{4,2},{5,3},{6,0},{7,1},{8,14},{9,15},{10,... | collective-permute-start | bytes 393224 | tf_op jit(solution)/shard_map/ppermute | solution.py:26
  4.7 7.1 %collective-permute-start.1 = (bf16[256,256]{1,0:T(8,128)(2,1)}, bf16[256,256]{1,0:T(8,128)(2,1)S(1)}, u32[]{:S(2)}, u32[]{:S(2)}) collective-permute-start(bf16[256,256]{1,0:T(8,128)(2,1)} %refs_0_.1), channel_id=1, source_target_pairs={{0,4},{1,5},{2,6},{3,7},{4,0},{5,1},{6,2},{7,3},{8,12},{9,13},{10,... | collective-permute-start | bytes 393224 | tf_op jit(solution)/shard_map/ppermute | solution.py:26
  5.2 6.9 %collective-permute-start = (bf16[256,256]{1,0:T(8,128)(2,1)}, bf16[256,256]{1,0:T(8,128)(2,1)S(1)}, u32[]{:S(2)}, u32[]{:S(2)}) collective-permute-start(bf16[256,256]{1,0:T(8,128)(2,1)} %refs_0_.1), channel_id=1, source_target_pairs={{0,2},{1,3},{2,0},{3,1},{4,6},{5,7},{6,4},{7,5},{8,10},{9,11},{10,... | collective-permute-start | bytes 393224 | tf_op jit(solution)/shard_map/ppermute | solution.py:26
  5.3 9.2 %collective-permute-start.3 = (bf16[256,256]{1,0:T(8,128)(2,1)}, bf16[256,256]{1,0:T(8,128)(2,1)S(1)}, u32[]{:S(2)}, u32[]{:S(2)}) collective-permute-start(bf16[256,256]{1,0:T(8,128)(2,1)} %refs_0_.1), channel_id=1, source_target_pairs={{0,1},{1,0},{2,3},{3,2},{4,5},{5,4},{6,7},{7,6},{8,9},{9,8},{10,11... | collective-permute-start | bytes 393224 | tf_op jit(solution)/shard_map/ppermute | solution.py:26
  9.2 5.4 %collective-permute-start.6 = (bf16[256,256]{1,0:T(8,128)(2,1)S(1)}, bf16[256,256]{1,0:T(8,128)(2,1)S(1)}, u32[]{:S(2)}, u32[]{:S(2)}) collective-permute-start(bf16[256,256]{1,0:T(8,128)(2,1)S(1)} %collective-permute-done.2.refs_3_), channel_id=1, source_target_pairs={{0,1},{1,0},{2,3},{3,2},{4,5},{5,4},{6,7},{7,6},{8,9},{9,8},{10,11... | collective-permute-start | bytes 393224 | tf_op jit(solution)/shard_map/ppermute | solution.py:26
  11.8 2.8 %collective-permute-start.5 = (bf16[256,256]{1,0:T(8,128)(2,1)S(1)}, bf16[256,256]{1,0:T(8,128)(2,1)S(1)}, u32[]{:S(2)}, u32[]{:S(2)}) collective-permute-start(bf16[256,256]{1,0:T(8,128)(2,1)S(1)} %collective-permute-done.1.refs_2_), channel_id=1, source_target_pairs={{0,1},{1,0},{2,3},{3,2},{4,5},{5,4},{6,7},{7,6},{8,9},{9,8},{10,11... | collective-permute-start | bytes 393224 | tf_op jit(solution)/shard_map/ppermute | solution.py:26
  12.1 2.5 %collective-permute-start.4 = (bf16[256,256]{1,0:T(8,128)(2,1)S(1)}, bf16[256,256]{1,0:T(8,128)(2,1)S(1)}, u32[]{:S(2)}, u32[]{:S(2)}) collective-permute-start(bf16[256,256]{1,0:T(8,128)(2,1)S(1)} %collective-permute-done.refs_1_), channel_id=1, source_target_pairs={{0,1},{1,0},{2,3},{3,2},{4,5},{5,4},{6,7},{7,6},{8,9},{9,8},{10,11... | collective-permute-start | bytes 393224 | tf_op jit(solution)/shard_map/ppermute | solution.py:26
  12.3 2.3 %copy-start.1 = (bf16[256,256]{1,0:T(8,128)(2,1)S(1)}, bf16[256,256]{1,0:T(8,128)(2,1)}, u32[]{:S(2)}) copy-start(bf16[256,256]{1,0:T(8,128)(2,1)} %refs_0_.1) | copy-start | bytes 393220
  14.5 0.7 %copy-start.2 = (f32[2048]{0:T(1024)S(1)}, f32[2048]{0:T(1024)}, u32[]{:S(2)}) copy-start(f32[2048]{0:T(1024)} %param.14) | copy-start | bytes 24580
  16.4 18.1 %copy-start = (bf16[2048,128]{1,0:T(8,128)(2,1)S(1)}, bf16[2048,128]{1,0:T(8,128)(2,1)}, u32[]{:S(2)}) copy-start(bf16[2048,128]{1,0:T(8,128)(2,1)} %refs_3_.1) | copy-start | bytes 1572868
  16.4 7.6 %collective-permute-start.10 = (bf16[152,128]{1,0:T(8,128)(2,1)S(1)}, bf16[152,128]{1,0:T(8,128)(2,1)S(1)}, u32[]{:S(2)}, u32[]{:S(2)}) collective-permute-start(bf16[152,128]{1,0:T(8,128)(2,1)S(1)} %get-tuple-element.27.refs_8_), channel_id=1, source_target_pairs={{0,24},{8,16},{16,8},{24,0},{1,25},{9,17},{17,9},{25,1},{2,26},{10... | collective-permute-start | bytes 116744 | tf_op jit(solution)/shard_map/ppermute | solution.py:26
  20.2 4.9 %collective-permute-start.9 = (bf16[152,128]{1,0:T(8,128)(2,1)S(1)}, bf16[152,128]{1,0:T(8,128)(2,1)S(1)}, u32[]{:S(2)}, u32[]{:S(2)}) collective-permute-start(bf16[152,128]{1,0:T(8,128)(2,1)S(1)} %get-tuple-element.27.refs_8_), channel_id=1, source_target_pairs={{0,16},{8,24},{16,0},{24,8},{1,17},{9,25},{17,1},{25,9},{2,18},{10... | collective-permute-start | bytes 116744 | tf_op jit(solution)/shard_map/ppermute | solution.py:26
  20.2 6.4 %collective-permute-start.8 = (bf16[152,128]{1,0:T(8,128)(2,1)S(1)}, bf16[152,128]{1,0:T(8,128)(2,1)S(1)}, u32[]{:S(2)}, u32[]{:S(2)}) collective-permute-start(bf16[152,128]{1,0:T(8,128)(2,1)S(1)} %get-tuple-element.27.refs_8_), channel_id=1, source_target_pairs={{0,8},{8,0},{16,24},{24,16},{1,9},{9,1},{17,25},{25,17},{2,10},{10... | collective-permute-start | bytes 116744 | tf_op jit(solution)/shard_map/ppermute | solution.py:26
  20.9 7.3 %collective-permute-start.20 = (bf16[144,128]{1,0:T(8,128)(2,1)S(1)}, bf16[144,128]{1,0:T(8,128)(2,1)S(1)}, u32[]{:S(2)}, u32[]{:S(2)}) collective-permute-start(bf16[144,128]{1,0:T(8,128)(2,1)S(1)} %get-tuple-element.45.refs_4_), channel_id=1, source_target_pairs={{0,6},{1,7},{2,4},{3,5},{4,2},{5,3},{6,0},{7,1},{8,14},{9,15},{10,... | collective-permute-start | bytes 110600 | tf_op jit(solution)/shard_map/ppermute | solution.py:26
  22.6 6.1 %collective-permute-start.19 = (bf16[144,128]{1,0:T(8,128)(2,1)S(1)}, bf16[144,128]{1,0:T(8,128)(2,1)S(1)}, u32[]{:S(2)}, u32[]{:S(2)}) collective-permute-start(bf16[144,128]{1,0:T(8,128)(2,1)S(1)} %get-tuple-element.45.refs_4_), channel_id=1, source_target_pairs={{0,4},{1,5},{2,6},{3,7},{4,0},{5,1},{6,2},{7,3},{8,12},{9,13},{10,... | collective-permute-start | bytes 110600 | tf_op jit(solution)/shard_map/ppermute | solution.py:26
  24.0 16.8 %collective-permute-start.23 = (bf16[256,2048]{1,0:T(8,128)(2,1)S(1)}, bf16[256,2048]{1,0:T(8,128)(2,1)S(1)}, u32[]{:S(2)}, u32[]{:S(2)}) collective-permute-start(bf16[256,2048]{1,0:T(8,128)(2,1)S(1)} %get-tuple-element.38.own_w_ref), channel_id=1, source_target_pairs={{0,1},{1,0},{2,3},{3,2},{4,5},{5,4},{6,7},{7,6},{8,9},{9,8},{10,11... | collective-permute-start | bytes 3145736 | tf_op jit(solution)/shard_map/ppermute | solution.py:26
  25.1 5.1 %collective-permute-start.18 = (bf16[144,128]{1,0:T(8,128)(2,1)S(1)}, bf16[144,128]{1,0:T(8,128)(2,1)S(1)}, u32[]{:S(2)}, u32[]{:S(2)}) collective-permute-start(bf16[144,128]{1,0:T(8,128)(2,1)S(1)} %get-tuple-element.45.refs_4_), channel_id=1, source_target_pairs={{0,2},{1,3},{2,0},{3,1},{4,6},{5,7},{6,4},{7,5},{8,10},{9,11},{10,... | collective-permute-start | bytes 110600 | tf_op jit(solution)/shard_map/ppermute | solution.py:26
  26.6 6.4 %collective-permute-start.16 = (bf16[3,144,128]{2,1,0:T(8,128)(2,1)S(1)}, bf16[3,144,128]{2,1,0:T(8,128)(2,1)S(1)}, u32[]{:S(2)}, u32[]{:S(2)}) collective-permute-start(bf16[3,144,128]{2,1,0:T(8,128)(2,1)S(1)} %pad_maximum_fusion.1.refs_0_), channel_id=1, source_target_pairs={{0,6},{1,7},{2,4},{3,5},{4,2},{5,3},{6,0},{7,1},{8,14},{9,15},{10,... | collective-permute-start | bytes 331784 | tf_op jit(solution)/shard_map/ppermute | solution.py:26
  28.2 5.6 %collective-permute-start.14 = (bf16[3,144,128]{2,1,0:T(8,128)(2,1)S(1)}, bf16[3,144,128]{2,1,0:T(8,128)(2,1)S(1)}, u32[]{:S(2)}, u32[]{:S(2)}) collective-permute-start(bf16[3,144,128]{2,1,0:T(8,128)(2,1)S(1)} %pad_maximum_fusion.1.refs_0_), channel_id=1, source_target_pairs={{0,4},{1,5},{2,6},{3,7},{4,0},{5,1},{6,2},{7,3},{8,12},{9,13},{10,... | collective-permute-start | bytes 331784 | tf_op jit(solution)/shard_map/ppermute | solution.py:26
  28.7 5.1 %collective-permute-start.12 = (bf16[3,144,128]{2,1,0:T(8,128)(2,1)S(1)}, bf16[3,144,128]{2,1,0:T(8,128)(2,1)S(1)}, u32[]{:S(2)}, u32[]{:S(2)}) collective-permute-start(bf16[3,144,128]{2,1,0:T(8,128)(2,1)S(1)} %pad_maximum_fusion.1.refs_0_), channel_id=1, source_target_pairs={{0,2},{1,3},{2,0},{3,1},{4,6},{5,7},{6,4},{7,5},{8,10},{9,11},{10,... | collective-permute-start | bytes 331784 | tf_op jit(solution)/shard_map/ppermute | solution.py:26
  30.2 4.1 %collective-permute-start.11 = (bf16[3,144,128]{2,1,0:T(8,128)(2,1)S(1)}, bf16[3,144,128]{2,1,0:T(8,128)(2,1)S(1)}, u32[]{:S(2)}, u32[]{:S(2)}) collective-permute-start(bf16[3,144,128]{2,1,0:T(8,128)(2,1)S(1)} %pad_maximum_fusion.1.refs_0_), channel_id=1, source_target_pairs={{0,1},{1,0},{2,3},{3,2},{4,5},{5,4},{6,7},{7,6},{8,9},{9,8},{10,11... | collective-permute-start | bytes 331784 | tf_op jit(solution)/shard_map/ppermute | solution.py:26
  33.1 4.7 %collective-permute-start.21 = (bf16[4,144,128]{2,1,0:T(8,128)(2,1)S(1)}, bf16[4,144,128]{2,1,0:T(8,128)(2,1)S(1)}, u32[]{:S(2)}, u32[]{:S(2)}) collective-permute-start(bf16[4,144,128]{2,1,0:T(8,128)(2,1)S(1)} %pad_maximum_fusion), channel_id=1, source_target_pairs={{0,1},{1,0},{2,3},{3,2},{4,5},{5,4},{6,7},{7,6},{8,9},{9,8},{10,11... | collective-permute-start | bytes 442376 | tf_op jit(solution)/shard_map/ppermute | solution.py:26
  33.8 3.9 %collective-permute-start.17 = (bf16[3,144,128]{2,1,0:T(8,128)(2,1)S(1)}, bf16[3,144,128]{2,1,0:T(8,128)(2,1)S(1)}, u32[]{:S(2)}, u32[]{:S(2)}) collective-permute-start(bf16[3,144,128]{2,1,0:T(8,128)(2,1)S(1)} %collective-permute-done.16.refs_3_), channel_id=1, source_target_pairs={{0,1},{1,0},{2,3},{3,2},{4,5},{5,4},{6,7},{7,6},{8,9},{9,8},{10,11... | collective-permute-start | bytes 331784 | tf_op jit(solution)/shard_map/ppermute | solution.py:26
  33.8 3.9 %collective-permute-start.15 = (bf16[3,144,128]{2,1,0:T(8,128)(2,1)S(1)}, bf16[3,144,128]{2,1,0:T(8,128)(2,1)S(1)}, u32[]{:S(2)}, u32[]{:S(2)}) collective-permute-start(bf16[3,144,128]{2,1,0:T(8,128)(2,1)S(1)} %collective-permute-done.14.refs_2_), channel_id=1, source_target_pairs={{0,1},{1,0},{2,3},{3,2},{4,5},{5,4},{6,7},{7,6},{8,9},{9,8},{10,11... | collective-permute-start | bytes 331784 | tf_op jit(solution)/shard_map/ppermute | solution.py:26
  34.3 3.4 %collective-permute-start.13 = (bf16[3,144,128]{2,1,0:T(8,128)(2,1)S(1)}, bf16[3,144,128]{2,1,0:T(8,128)(2,1)S(1)}, u32[]{:S(2)}, u32[]{:S(2)}) collective-permute-start(bf16[3,144,128]{2,1,0:T(8,128)(2,1)S(1)} %collective-permute-done.12.refs_1_), channel_id=1, source_target_pairs={{0,1},{1,0},{2,3},{3,2},{4,5},{5,4},{6,7},{7,6},{8,9},{9,8},{10,11... | collective-permute-start | bytes 331784 | tf_op jit(solution)/shard_map/ppermute | solution.py:26
  35.1 0.9 %copy-start.4 = (bf16[512,256]{1,0:T(8,128)(2,1)S(1)}, bf16[512,256]{1,0:T(8,128)(2,1)}, u32[]{:S(2)}) copy-start(bf16[512,256]{1,0:T(8,128)(2,1)} %refs_6_.1) | copy-start | bytes 786436
  35.9 0.7 %copy-start.5 = (f32[512]{0:T(512)S(1)}, f32[512]{0:T(512)}, u32[]{:S(2)}) copy-start(f32[512]{0:T(512)} %param.18) | copy-start | bytes 6148
  39.5 1.3 %collective-permute-start.22 = (bf16[128,256]{1,0:T(8,128)(2,1)S(1)}, bf16[128,256]{1,0:T(8,128)(2,1)S(1)}, u32[]{:S(2)}, u32[]{:S(2)}) collective-permute-start(bf16[128,256]{1,0:T(8,128)(2,1)S(1)} %get-tuple-element.37), channel_id=1, source_target_pairs={{0,1},{1,0},{2,3},{3,2},{4,5},{5,4},{6,7},{7,6},{8,9},{9,8},{10,11... | collective-permute-start | bytes 196616 | tf_op jit(solution)/shard_map/ppermute | solution.py:26
  41.3 7.4 %collective-permute-start.24 = (bf16[32,2048]{1,0:T(8,128)(2,1)S(1)}, bf16[32,2048]{1,0:T(8,128)(2,1)S(1)}, u32[]{:S(2)}, u32[]{:S(2)}) collective-permute-start(bf16[32,2048]{1,0:T(8,128)(2,1)S(1)} %get-tuple-element.40), channel_id=1, source_target_pairs={{0,6},{1,7},{2,4},{3,5},{4,2},{5,3},{6,0},{7,1},{8,14},{9,15},{10,... | collective-permute-start | bytes 393224 | tf_op jit(solution)/shard_map/ppermute | solution.py:26
  42.8 8.0 %collective-permute-start.25 = (bf16[32,2048]{1,0:T(8,128)(2,1)S(1)}, bf16[32,2048]{1,0:T(8,128)(2,1)S(1)}, u32[]{:S(2)}, u32[]{:S(2)}) collective-permute-start(bf16[32,2048]{1,0:T(8,128)(2,1)S(1)} %get-tuple-element.41), channel_id=1, source_target_pairs={{0,4},{1,5},{2,6},{3,7},{4,0},{5,1},{6,2},{7,3},{8,12},{9,13},{10,... | collective-permute-start | bytes 393224 | tf_op jit(solution)/shard_map/ppermute | solution.py:26
  43.8 7.0 %collective-permute-start.26 = (bf16[32,2048]{1,0:T(8,128)(2,1)S(1)}, bf16[32,2048]{1,0:T(8,128)(2,1)S(1)}, u32[]{:S(2)}, u32[]{:S(2)}) collective-permute-start(bf16[32,2048]{1,0:T(8,128)(2,1)S(1)} %get-tuple-element.42), channel_id=1, source_target_pairs={{0,2},{1,3},{2,0},{3,1},{4,6},{5,7},{6,4},{7,5},{8,10},{9,11},{10,... | collective-permute-start | bytes 393224 | tf_op jit(solution)/shard_map/ppermute | solution.py:26
  (1 other events, 0.7 us)

commit v2 on v1

--- a/solution.py
+++ b/solution.py
@@ -38,6 +38,13 @@
     for array in arrays:
         pieces.append(swap(array, "tp", 1))
     return pieces
+
+
+def exchange_blocks(blocks):
+    arrived = []
+    for i in reversed(range(1, len(blocks))):
+        arrived.append(swap(blocks[i], "tp", 2 * i))
+    return arrived
 
 
 def kernel_call(body, outs, limit, scratch=(), flops=0, nbytes=0, in_hbm=()):
@@ -165,18 +172,13 @@
 
 def project_second(natural, *refs):
     scaled_ref, inv_ref, query_w_ref, gate_w_ref, cos_ref, sin_ref, mix_ref, taps_ref = refs[:8]
-    halos, (query_ref, conv_ref) = refs[8:-2], refs[-2:]
+    halos, (keep_ref, send_ref, both_ref) = refs[8:-3], refs[-3:]
     scaled = scaled_ref[...]
     inv = inv_ref[...]
     scale = (NOPE + ROPE) ** (-0.5)
     query = dot_nt(scaled, query_w_ref[...])
-    nope = (query[:, :NOPE] * inv * scale).astype(BF16)
-    rope = rotate(query[:, NOPE:] * inv, cos_ref[...], sin_ref[...]) * scale
-    low = low_lanes(rope.shape)
-    query_ref[0, :, :NOPE] = nope
-    query_ref[1, :, :NOPE] = nope
-    query_ref[0, :, NOPE:] = jnp.where(low, rope, 0.0).astype(BF16)
-    query_ref[1, :, NOPE:] = jnp.where(low, 0.0, rope).astype(BF16)
+    both_ref[:, :NOPE] = query[:, :NOPE] * inv * scale
+    both_ref[:, NOPE : NOPE + LANES] = rotate(query[:, NOPE:] * inv, cos_ref[...], sin_ref[...]) * scale
 
     gate = jnp.dot(scaled, gate_w_ref[...], preferred_element_type=F32) * inv
     mix = mix_ref[...].astype(F32)
@@ -199,28 +201,44 @@
     later = jnp.where(row == tokens - 1, edge_of(place + 1, 0), pltpu.roll(mix, tokens - 1, 0))
     taps = taps_ref[...].astype(F32)
     convolved = taps[0:1] * earlier + taps[1:2] * mix + taps[2:3] * later
-    conv_ref[...] = (gate * convolved).astype(BF16)
+    both_ref[:, NOPE + LANES :] = gate * convolved
+    core = lax.axis_index("tp") % 2
+    rows = tokens // lax.axis_size("tp")
+    for i in range(lax.axis_size("tp") // 2):
+        for ref, side in ((keep_ref, core), (send_ref, 1 - core)):
+            source = pl.ds(pl.multiple_of((2 * i + side) * rows, rows), rows)
+            ref[i * rows : (i + 1) * rows, :] = both_ref[source, :].astype(BF16)
 
 
 def attend(slots, chunk, last, *refs):
     inputs = 1 + max(place for chip_slots in slots for place, _ in chip_slots)
     pieces, refs = refs[:inputs], refs[inputs:]
-    gain_ref, expand_ref, query_ref = refs[:3]
-    refs = refs[3:]
+    gain_ref, expand_refs, query_refs = refs[0], refs[1:3], refs[3:5]
+    refs = refs[5:]
     if last:
-        stats_in, out_in, conv_ref, keep_ref, send_ref, log_ref = refs[:6]
+        stats_in, out_in, own_w_ref, other_w_ref = refs[:4]
+        block_refs, (keep_log_ref, send_log_ref, both_ref) = refs[4:-5], refs[-5:-2]
     else:
         stats_ref, out_ref = refs[:2]
     latent_ref, rope_ref = refs[-2:]
     rank = lax.axis_index("tp")
-    chip, core = rank // 2, rank % 2
+    chip = rank // 2
     pairs = len(slots)
-    tokens = query_ref.shape[1]
-    half = tokens // 2
+    half = query_refs[0].shape[0]
+    tokens = 2 * half
     group = half // 2
     share = group // pairs
     entries = pairs * LANES
 
+    low = low_lanes((half, LANES))
+    queries = []
+    for ref in query_refs:
+        nope, rope = ref[:, :NOPE], ref[:, NOPE : NOPE + LANES]
+        zeros = jnp.zeros_like(rope)
+        sides = (jnp.where(low, rope, zeros), jnp.where(low, zeros, rope))
+        queries.append([jnp.concatenate([nope, side], axis=1) for side in sides])
+    key_w = jnp.concatenate([ref[:, :NOPE] for ref in expand_refs], axis=1)
+    value_w = jnp.concatenate([ref[:, NOPE:] for ref in expand_refs], axis=1)
     views = [(chip ^ i, chip_slots) for i, chip_slots in enumerate(slots)]
 
     def rows_of(chip_slots, slot, first, start, count):
@@ -246,24 +264,36 @@
                     base = (side * chunk + slot) * group
                     latent_ref[base : base + group, columns] = scaled[side * group : (side + 1) * group]
         latent = latent_ref[...]
-        keys = jnp.dot(latent, expand_ref[:, :NOPE], preferred_element_type=F32).astype(BF16)
+        keys = jnp.dot(latent, key_w, preferred_element_type=F32).astype(BF16)
         values = lax.dot_general(
-            expand_ref[:, NOPE:], latent, (((0,), (1,)), ((), ())), preferred_element_type=F32
+            value_w, latent, (((0,), (1,)), ((), ())), preferred_element_type=F32
         ).astype(BF16)
         rope = rope_ref[...]
         count = chunk * group
+        spans = [slice(i * count, (i + 1) * count) for i in range(2)]
+        heads = [slice(i * NOPE, (i + 1) * NOPE) for i in range(2)]
         scores = [
-            dot_nt(jnp.concatenate([keys[i * count : (i + 1) * count], rope], axis=1), query_ref[i])
-            for i in range(2)
+            jnp.concatenate(
+                [dot_nt(jnp.concatenate([keys[span, head], rope], axis=1), query[i]) for head, query in zip(heads, queries)],
+                axis=1,
+            )
+            for i, span in enumerate(spans)
         ]
         peak = jnp.max(jnp.maximum(*scores), axis=0, keepdims=True)
         if state is not None:
             peak = jnp.maximum(peak, state[0])
         weights = [jnp.exp(piece - peak) for piece in scores]
         total = jnp.sum(weights[0] + weights[1], axis=0, keepdims=True)
-        out = sum(
-            jnp.dot(values[:, i * count : (i + 1) * count], weights[i].astype(BF16), preferred_element_type=F32)
-            for i in range(2)
+        weights = [piece.astype(BF16) for piece in weights]
+        out = jnp.concatenate(
+            [
+                sum(
+                    jnp.dot(values[head, span], weight[:, i * half : (i + 1) * half], preferred_element_type=F32)
+                    for span, weight in zip(spans, weights)
+                )
+                for i, head in enumerate(heads)
+            ],
+            axis=1,
         )
         if state is not None:
             rescale = jnp.exp(state[0] - peak)
@@ -288,26 +318,36 @@
         stats_ref[1:2] = total
         out_ref[...] = out
         return
-    log_ref[...] = peak + jnp.log(total)
-    attended = jnp.transpose(out / total)
-    rows = tokens // (2 * pairs)
-    attend_ref = refs[-3]
-    attend_ref[...] = attended.astype(BF16)
-    for i in range(pairs):
-        base = 2 * (chip ^ i)
-        for ref, at in ((keep_ref, base + core), (send_ref, base + 1 - core)):
-            source = pl.ds(pl.multiple_of(at * rows, rows), rows)
-            ref[i * rows : (i + 1) * rows, :VDIM] = attend_ref[source, :]
-            ref[i * rows : (i + 1) * rows, VDIM:] = conv_ref[source, :]
-
-
-def output(keep_ref, got_ref, own_w_ref, other_w_ref, first_ref, *rest_refs):
-    out = jnp.dot(keep_ref[...], own_w_ref[...], preferred_element_type=F32)
-    out = out + jnp.dot(got_ref[...], other_w_ref[...], preferred_element_type=F32)
-    rows = first_ref.shape[0]
-    first_ref[...] = out[:rows]
-    for i, ref in enumerate(rest_refs):
-        ref[...] = out[(i + 1) * rows : (i + 2) * rows].astype(BF16)
+    logs = peak + jnp.log(total)
+    keep_log_ref[...] = logs[:, :half]
+    send_log_ref[...] = logs[:, half:]
+    out = out * (1.0 / total)
+    rows = half // pairs
+    result = None
+    for i, weight_ref in enumerate((own_w_ref, other_w_ref)):
+        attended = jnp.transpose(out[:, i * half : (i + 1) * half]).astype(BF16)
+        both_ref[i, :, :VDIM] = attended
+        both_ref[i, :, VDIM:] = query_refs[i][:, NOPE + LANES :]
+        order = [both_ref[i, pl.ds(pl.multiple_of((chip ^ j) * rows, rows), rows), :] for j in range(pairs)]
+        product = jnp.dot(jnp.concatenate(order, axis=0), weight_ref[...], preferred_element_type=F32)
+        result = product if result is None else result + product
+    for i, ref in enumerate(block_refs):
+        ref[...] = result[i * rows : (i + 1) * rows].astype(ref.dtype)
+
+
+def join_logs(own_ref, got_ref, log_ref):
+    ranks = lax.axis_size("tp")
+    rows = log_ref.shape[1] // ranks
+    first = lax.axis_index("tp") % 2 == 0
+    own, got = own_ref[...], got_ref[...]
+    sides = [jnp.where(first, own, got), jnp.where(first, got, own)]
+    lane = lax.broadcasted_iota(jnp.int32, log_ref.shape, 1) // rows
+    logs = jnp.zeros(log_ref.shape, F32)
+    for i in range(ranks):
+        side = jnp.concatenate([sides[i % 2]] * 2, axis=1)
+        shift = (i - i // 2) * rows
+        logs = jnp.where(lane == i, pltpu.roll(side, shift, 1) if shift else side, logs)
+    log_ref[...] = logs
 
 
 def body(
@@ -340,6 +380,7 @@
 
     latent_t = latent_weight.T
     partner_t = swap(latent_t, "tp", 1)
+    other_expand = swap(expand_weight, "tp", 1)
     key_w, query_w, mix_w, own_w, cosines, sines = kernel_call(
         prepare,
         [
@@ -396,51 +437,48 @@
         arounds += nears
         others.append(near_other)
 
-    query, conv = kernel_call(
+    columns = NOPE + LANES + channels
+    keep, send = kernel_call(
         functools.partial(project_second, not small),
-        [((2, tokens, NOPE + LANES), BF16), ((tokens, channels), BF16)],
+        [((half, columns), BF16)] * 2,
         12 << 20,
+        scratch=[pltpu.VMEM((tokens, columns), F32)],
         flops=2 * tokens * features * 3 * LANES,
         nbytes=4 * tokens * features,
     )(scaled, inv, query_w, gate_weight, cosines, sines, mix, conv_kernel, *halos)
+    got = swap(send, "tp", 1)
 
     chunk = places if small else 4
 
     def attend_to(arrays, slots, last, outs, *operands):
         scratch = [
-            pltpu.VMEM((tokens, VDIM), BF16),
+            pltpu.VMEM((2, half, VDIM + channels), BF16),
             pltpu.VMEM((chunk * half, pairs * LANES), BF16),
             pltpu.VMEM((chunk * half // 2, LANES), BF16),
         ]
         return kernel_call(
             functools.partial(attend, slots, chunk, last),
             outs,
-            (12 << 20) if small else (40 << 20),
+            (14 << 20) if small else (40 << 20),
             scratch=scratch if last else scratch[1:],
             flops=1 << 29,
             nbytes=1 << 22,
-        )(*arrays, latent_gain.reshape(1, -1), expand_weight, query, *operands)
+        )(*arrays, latent_gain.reshape(1, -1), expand_weight, other_expand, keep, got, *operands)
 
     stats, out = attend_to(arounds, slots, False, [((8, tokens), F32), ((VDIM, tokens), F32)])
-    keep, send, logs = attend_to(
+    *outs, own_log, send_log = attend_to(
         others,
         other_slots,
         True,
-        [((half, VDIM + channels), BF16), ((half, VDIM + channels), BF16), ((1, tokens), F32)],
+        [((rows, features), F32)] + [((rows, features), BF16)] * (pairs - 1) + [((1, half), F32)] * 2,
         stats,
         out,
-        conv,
+        own_w,
+        other_w,
     )
-
-    got = swap(send, "tp", 1)
-    outs = kernel_call(
-        output,
-        [((rows, features), F32)] + [((rows, features), BF16)] * (pairs - 1),
-        12 << 20,
-        flops=1 << 28,
-        nbytes=1 << 22,
-    )(keep, got, own_w, other_w)
-    arrived = [swap(outs[i], "tp", 2 * i) for i in reversed(range(1, pairs))]
+    arrived = exchange_blocks(outs)
+    got_log = swap(send_log, "tp", 1)
+    (logs,) = kernel_call(join_logs, [((1, tokens), F32)], 1 << 20, flops=1 << 22, nbytes=1 << 12)(own_log, got_log)
     total = outs[0]
     for piece in arrived:
         total = total + piece.astype(F32)

time: 51.8 us -> 52.4 us (1.012)
  waiting for transfers between devices: 18.4 us -> 20 us
  local copies, waits for them, and re-layouts: 2.04 us -> 1.35 us
  starting transfers between devices: 22.2 us -> 21.6 us
    ppermute x27 -> x29, waiting for transfers between devices: 18.4 us -> 20 us  [swap(): return lax.ppermute(array, axis, [(i, i ^ mask) for i in range(peers)])]
    unnamed x12, local copies, waits for them, and re-layouts: 2.02 us -> 1.34 us
    ppermute x27 -> x29, starting transfers between devices: 22.2 us -> 21.6 us  [swap(): return lax.ppermute(array, axis, [(i, i ^ mask) for i in range(peers)])]
  transfers between devices with their start and end apart: 27 -> 29, of which waited for: 9 -> 11; matrix products, arithmetic and copies ran while one was open for 0% -> 0% of each run, Pallas kernels for 11% -> 11%
where the time goes in v2:
time: 52.4 us; the launch traced here: 52.1 us
  starting transfers between devices  21.6 us (41%)
  waiting for transfers between devices  20 us (38%)
  Pallas kernels  7.56 us (14%)
  local copies, waits for them, and re-layouts  1.35 us (3%)
  between operations  0.83 us (2%)
  other arithmetic  0.76 us (1%)
    ppermute x29, starting transfers between devices, swap(): return lax.ppermute(array, axis, [(i, i ^ mask) for i in range(peers)])  21.6 us
    ppermute x29, waiting for transfers between devices, swap(): return lax.ppermute(array, axis, [(i, i ^ mask) for i in range(peers)])  20 us
    pallas_call x6, Pallas kernels, call(): pl.pallas_call(body, out_shape=[jax.ShapeDtypeStruct(shape, dtype) for sh...  7.56 us
    unnamed x12, local copies, waits for them, and re-layouts  1.34 us
  transfers between devices with their start and end apart: 29, of which 11 were waited for; matrix products, arithmetic and copies ran while one was open for 0% of the time, Pallas kernels for 11%

profile of v2, /device:TPU:0, one launch (start us, length us, event | category | flops | bytes accessed | tf_op | source)
XLA Modules:
  0.0 52.1 jit_solution(12133770398854953595)
XLA Ops:
  0.6 0.6 %collective-permute-start.7 = (bf16[64,2048]{1,0:T(8,128)(2,1)}, bf16[64,2048]{1,0:T(8,128)(2,1)S(1)}, u32[]{:S(2)}, u32[]{:S(2)}) collective-permute-start(bf16[64,2048]{1,0:T(8,128)(2,1)} %bitcast.23), channel_id=1, source_target_pairs={{0,1},{1,0},{2,3},{3,2},{4,5},{5,4},{6,7},{7,6},{8,9},{9,8},{10,11... | collective-permute-start | bytes 786440 | tf_op jit(solution)/shard_map/ppermute | solution.py:26
  1.2 2.6 %collective-permute-start = (bf16[256,256]{1,0:T(8,128)(2,1)}, bf16[256,256]{1,0:T(8,128)(2,1)S(1)}, u32[]{:S(2)}, u32[]{:S(2)}) collective-permute-start(bf16[256,256]{1,0:T(8,128)(2,1)} %refs_0_.1), channel_id=1, source_target_pairs={{0,2},{1,3},{2,0},{3,1},{4,6},{5,7},{6,4},{7,5},{8,10},{9,11},{10,... | collective-permute-start | bytes 393224 | tf_op jit(solution)/shard_map/ppermute | solution.py:26
  3.7 1.5 %collective-permute-start.1 = (bf16[256,256]{1,0:T(8,128)(2,1)}, bf16[256,256]{1,0:T(8,128)(2,1)S(1)}, u32[]{:S(2)}, u32[]{:S(2)}) collective-permute-start(bf16[256,256]{1,0:T(8,128)(2,1)} %refs_0_.1), channel_id=1, source_target_pairs={{0,4},{1,5},{2,6},{3,7},{4,0},{5,1},{6,2},{7,3},{8,12},{9,13},{10,... | collective-permute-start | bytes 393224 | tf_op jit(solution)/shard_map/ppermute | solution.py:26
  5.3 2.9 %collective-permute-done.refs_1_ = bf16[256,256]{1,0:T(8,128)(2,1)S(1)} collective-permute-done((bf16[256,256]{1,0:T(8,128)(2,1)}, bf16[256,256]{1,0:T(8,128)(2,1)S(1)}, u32[]{:S(2)}, u32[]{:S(2)}) %collective-permute-start) | collective-permute-done | bytes 131104 | tf_op jit(solution)/shard_map/ppermute | solution.py:26
  8.2 4.1 %collective-permute-done.1.refs_2_ = bf16[256,256]{1,0:T(8,128)(2,1)S(1)} collective-permute-done((bf16[256,256]{1,0:T(8,128)(2,1)}, bf16[256,256]{1,0:T(8,128)(2,1)S(1)}, u32[]{:S(2)}, u32[]{:S(2)}) %collective-permute-start.1) | collective-permute-done | bytes 131104 | tf_op jit(solution)/shard_map/ppermute | solution.py:26
  12.3 0.5 collective-permute-start.6
  12.9 2.2 %shard_map.140 = (bf16[256,2048]{1,0:T(8,128)(2,1)S(1)}, bf16[256,2048]{1,0:T(8,128)(2,1)S(1)}, bf16[2048,256]{1,0:T(8,128)(2,1)S(1)}, bf16[256,2048]{1,0:T(8,12...) custom-call(bf16[64,2048]{1,0:T(8,128)(2,1)} %bitcast.24, bf16[64,2048]{1,0:T(8,128)(2,1)} %bitcast.25, ...), custom_call_target="tpu_custom_call" | custom-call | flops 268435456 | bytes 8388608 | tf_op jit(solution)/shard_map/pallas_call | solution.py:59
  15.2 0.6 %copy-done.3 = f32[2048]{0:T(1024)S(1)} copy-done((f32[2048]{0:T(1024)S(1)}, f32[2048]{0:T(1024)}, u32[]{:S(2)}) %copy-start.3) | copy-done | bytes 8216
  15.8 1.1 %shard_map.141 = (bf16[256,2048]{1,0:T(8,128)(2,1)S(1)}, f32[256,128]{1,0:T(8,128)S(1)}, bf16[152,128]{1,0:T(8,128)(2,1)S(1)}, bf16[256,128]{1,0:T(8,128)(2,1)S(1)}) custom-call(bf16[256,256]{1,0:T(8,128)(2,1)S(1)} %copy-done.2, bf16[256,256]{1,0:T(8,128)(2,1)S(1)} %collective-permute-done.refs_1_, bf16[256,256]{1,0:T(8,128)(2,1)S(1)} %collective-permute-done.1.refs_2_, ...), custom_call_target="tpu_custom_call" | custom-call | flops 536870912 | bytes 2097152 | tf_op jit(solution)/shard_map/pallas_call | solution.py:59
  16.9 3.7 %collective-permute-start.10 = (bf16[152,128]{1,0:T(8,128)(2,1)S(1)}, bf16[152,128]{1,0:T(8,128)(2,1)S(1)}, u32[]{:S(2)}, u32[]{:S(2)}) collective-permute-start(bf16[152,128]{1,0:T(8,128)(2,1)S(1)} %get-tuple-element.26.refs_8_), channel_id=1, source_target_pairs={{0,24},{8,16},{16,8},{24,0},{1,25},{9,17},{17,9},{25,1},{2,26},{10... | collective-permute-start | bytes 116744 | tf_op jit(solution)/shard_map/ppermute | solution.py:26
  20.6 0.8 %collective-permute-start.9 = (bf16[152,128]{1,0:T(8,128)(2,1)S(1)}, bf16[152,128]{1,0:T(8,128)(2,1)S(1)}, u32[]{:S(2)}, u32[]{:S(2)}) collective-permute-start(bf16[152,128]{1,0:T(8,128)(2,1)S(1)} %get-tuple-element.26.refs_8_), channel_id=1, source_target_pairs={{0,16},{8,24},{16,0},{24,8},{1,17},{9,25},{17,1},{25,9},{2,18},{10... | collective-permute-start | bytes 116744 | tf_op jit(solution)/shard_map/ppermute | solution.py:26
  21.4 1.2 %collective-permute-start.18 = (bf16[144,128]{1,0:T(8,128)(2,1)S(1)}, bf16[144,128]{1,0:T(8,128)(2,1)S(1)}, u32[]{:S(2)}, u32[]{:S(2)}) collective-permute-start(bf16[144,128]{1,0:T(8,128)(2,1)S(1)} %get-tuple-element.43.refs_4_), channel_id=1, source_target_pairs={{0,2},{1,3},{2,0},{3,1},{4,6},{5,7},{6,4},{7,5},{8,10},{9,11},{10,... | collective-permute-start | bytes 110600 | tf_op jit(solution)/shard_map/ppermute | solution.py:26
  22.6 0.6 %collective-permute-done.10.refs_11_ = bf16[152,128]{1,0:T(8,128)(2,1)S(1)} collective-permute-done((bf16[152,128]{1,0:T(8,128)(2,1)S(1)}, bf16[152,128]{1,0:T(8,128)(2,1)S(1)}, u32[]{:S(2)}, u32[]{:S(2)}) %collective-permute-start.10) | collective-permute-done | bytes 38944 | tf_op jit(solution)/shard_map/ppermute | solution.py:26
  23.2 2.3 %collective-permute-done.9.refs_10_ = bf16[152,128]{1,0:T(8,128)(2,1)S(1)} collective-permute-done((bf16[152,128]{1,0:T(8,128)(2,1)S(1)}, bf16[152,128]{1,0:T(8,128)(2,1)S(1)}, u32[]{:S(2)}, u32[]{:S(2)}) %collective-permute-start.9) | collective-permute-done | bytes 38944 | tf_op jit(solution)/shard_map/ppermute | solution.py:26
  25.5 1.5 %collective-permute-start.19 = (bf16[144,128]{1,0:T(8,128)(2,1)S(1)}, bf16[144,128]{1,0:T(8,128)(2,1)S(1)}, u32[]{:S(2)}, u32[]{:S(2)}) collective-permute-start(bf16[144,128]{1,0:T(8,128)(2,1)S(1)} %get-tuple-element.43.refs_4_), channel_id=1, source_target_pairs={{0,4},{1,5},{2,6},{3,7},{4,0},{5,1},{6,2},{7,3},{8,12},{9,13},{10,... | collective-permute-start | bytes 110600 | tf_op jit(solution)/shard_map/ppermute | solution.py:26
  27.0 1.5 %collective-permute-start.20 = (bf16[144,128]{1,0:T(8,128)(2,1)S(1)}, bf16[144,128]{1,0:T(8,128)(2,1)S(1)}, u32[]{:S(2)}, u32[]{:S(2)}) collective-permute-start(bf16[144,128]{1,0:T(8,128)(2,1)S(1)} %get-tuple-element.43.refs_4_), channel_id=1, source_target_pairs={{0,6},{1,7},{2,4},{3,5},{4,2},{5,3},{6,0},{7,1},{8,14},{9,15},{10,... | collective-permute-start | bytes 110600 | tf_op jit(solution)/shard_map/ppermute | solution.py:26
  28.5 0.7 %copy-done.5 = bf16[3,128]{1,0:T(4,128)(2,1)S(1)} copy-done((bf16[3,128]{1,0:T(4,128)(2,1)S(1)}, bf16[3,128]{1,0:T(4,128)(2,1)}, u32[]{:S(2)}) %copy-start.5) | copy-done | bytes 792
  29.2 0.9 %shard_map.142 = (bf16[128,384]{1,0:T(8,128)(2,1)S(1)}, bf16[128,384]{1,0:T(8,128)(2,1)S(1)}) custom-call(bf16[256,2048]{1,0:T(8,128)(2,1)S(1)} %get-tuple-element.27.refs_0_, f32[256,128]{1,0:T(8,128)S(1)} %get-tuple-element.28.refs_1_, bf16[256,2048]{1,0:T(8,128)(2,1)S(1)} %get-tuple-element.29.refs_2_, bf16[2048,128]{1,0:T(8,128)(2,1)S(1)} %copy-done, ...), custom_call_target="tpu_custom_call" | custom-call | flops 402653184 | bytes 2097152 | tf_op jit(solution)/shard_map/pallas_call | solution.py:59
  30.2 0.6 %collective-permute-start.12 = (bf16[3,144,128]{2,1,0:T(8,128)(2,1)S(1)}, bf16[3,144,128]{2,1,0:T(8,128)(2,1)S(1)}, u32[]{:S(2)}, u32[]{:S(2)}) collective-permute-start(bf16[3,144,128]{2,1,0:T(8,128)(2,1)S(1)} %pad_maximum_fusion.1.refs_0_), channel_id=1, source_target_pairs={{0,2},{1,3},{2,0},{3,1},{4,6},{5,7},{6,4},{7,5},{8,10},{9,11},{10,... | collective-permute-start | bytes 331784 | tf_op jit(solution)/shard_map/ppermute | solution.py:26
  30.8 1.5 %collective-permute-start.14 = (bf16[3,144,128]{2,1,0:T(8,128)(2,1)S(1)}, bf16[3,144,128]{2,1,0:T(8,128)(2,1)S(1)}, u32[]{:S(2)}, u32[]{:S(2)}) collective-permute-start(bf16[3,144,128]{2,1,0:T(8,128)(2,1)S(1)} %pad_maximum_fusion.1.refs_0_), channel_id=1, source_target_pairs={{0,4},{1,5},{2,6},{3,7},{4,0},{5,1},{6,2},{7,3},{8,12},{9,13},{10,... | collective-permute-start | bytes 331784 | tf_op jit(solution)/shard_map/ppermute | solution.py:26
  32.3 1.5 %collective-permute-start.16 = (bf16[3,144,128]{2,1,0:T(8,128)(2,1)S(1)}, bf16[3,144,128]{2,1,0:T(8,128)(2,1)S(1)}, u32[]{:S(2)}, u32[]{:S(2)}) collective-permute-start(bf16[3,144,128]{2,1,0:T(8,128)(2,1)S(1)} %pad_maximum_fusion.1.refs_0_), channel_id=1, source_target_pairs={{0,6},{1,7},{2,4},{3,5},{4,2},{5,3},{6,0},{7,1},{8,14},{9,15},{10,... | collective-permute-start | bytes 331784 | tf_op jit(solution)/shard_map/ppermute | solution.py:26
  33.8 2.4 %collective-permute-done.12.refs_1_ = bf16[3,144,128]{2,1,0:T(8,128)(2,1)S(1)} collective-permute-done((bf16[3,144,128]{2,1,0:T(8,128)(2,1)S(1)}, bf16[3,144,128]{2,1,0:T(8,128)(2,1)S(1)}, u32[]{:S(2)}, u32[]{:S(2)}) %collective-permute-start.12) | collective-permute-done | bytes 110624 | tf_op jit(solution)/shard_map/ppermute | solution.py:26
  36.2 2.1 %collective-permute-done.14.refs_2_ = bf16[3,144,128]{2,1,0:T(8,128)(2,1)S(1)} collective-permute-done((bf16[3,144,128]{2,1,0:T(8,128)(2,1)S(1)}, bf16[3,144,128]{2,1,0:T(8,128)(2,1)S(1)}, u32[]{:S(2)}, u32[]{:S(2)}) %collective-permute-start.14) | collective-permute-done | bytes 110624 | tf_op jit(solution)/shard_map/ppermute | solution.py:26
  38.9 1.1 %shard_map.143 = (f32[8,256]{1,0:T(8,128)S(1)}, f32[128,256]{1,0:T(8,128)S(1)}) custom-call(bf16[3,144,128]{2,1,0:T(8,128)(2,1)S(1)} %pad_maximum_fusion.1.refs_0_, bf16[3,144,128]{2,1,0:T(8,128)(2,1)S(1)} %collective-permute-done.12.refs_1_, bf16[3,144,128]{2,1,0:T(8,128)(2,1)S(1)} %collective-permute-done.14.refs_2_, ...), custom_call_target="tpu_custom_call" | custom-call | flops 536870912 | bytes 4194304 | tf_op jit(solution)/shard_map/pallas_call | solution.py:59
  40.2 1.6 %shard_map.144 = (f32[32,2048]{1,0:T(8,128)S(1)}, bf16[32,2048]{1,0:T(8,128)(2,1)S(1)}, bf16[32,2048]{1,0:T(8,128)(2,1)S(1)}, bf16[32,2048]{1,0:T(8,128)(2,1)S(1...) custom-call(bf16[3,144,128]{2,1,0:T(8,128)(2,1)S(1)} %collective-permute-done.11.refs_0_, ...), custom_call_target="tpu_custom_call" | custom-call | flops 536870912 | bytes 4194304 | tf_op jit(solution)/shard_map/pallas_call | solution.py:59
  41.8 1.5 %collective-permute-start.25 = (bf16[32,2048]{1,0:T(8,128)(2,1)S(1)}, bf16[32,2048]{1,0:T(8,128)(2,1)S(1)}, u32[]{:S(2)}, u32[]{:S(2)}) collective-permute-start(bf16[32,2048]{1,0:T(8,128)(2,1)S(1)} %get-tuple-element.37), channel_id=1, source_target_pairs={{0,6},{1,7},{2,4},{3,5},{4,2},{5,3},{6,0},{7,1},{8,14},{9,15},{10,... | collective-permute-start | bytes 393224 | tf_op jit(solution)/shard_map/ppermute | solution.py:26
  43.3 1.5 %collective-permute-start.26 = (bf16[32,2048]{1,0:T(8,128)(2,1)S(1)}, bf16[32,2048]{1,0:T(8,128)(2,1)S(1)}, u32[]{:S(2)}, u32[]{:S(2)}) collective-permute-start(bf16[32,2048]{1,0:T(8,128)(2,1)S(1)} %get-tuple-element.38), channel_id=1, source_target_pairs={{0,4},{1,5},{2,6},{3,7},{4,0},{5,1},{6,2},{7,3},{8,12},{9,13},{10,... | collective-permute-start | bytes 393224 | tf_op jit(solution)/shard_map/ppermute | solution.py:26
  45.3 1.2 %collective-permute-done.28.got_ref = f32[1,128]{1,0:T(1,128)S(1)} collective-permute-done((f32[1,128]{1,0:T(1,128)S(1)}, f32[1,128]{1,0:T(1,128)S(1)}, u32[]{:S(2)}, u32[]{:S(2)}) %collective-permute-start.28) | collective-permute-done | bytes 544 | tf_op jit(solution)/shard_map/ppermute | solution.py:26
  46.5 0.6 %shard_map.145 = f32[1,256]{1,0:T(1,128)} custom-call(f32[1,128]{1,0:T(1,128)S(1)} %get-tuple-element.40.own_ref, f32[1,128]{1,0:T(1,128)S(1)} %collective-permute-done.28.got_ref), custom_call_target="tpu_custom_call" | custom-call | flops 4194304 | bytes 4096 | tf_op jit(solution)/shard_map/pallas_call | solution.py:59
  47.2 2.0 %collective-permute-done.25 = bf16[32,2048]{1,0:T(8,128)(2,1)S(1)} collective-permute-done((bf16[32,2048]{1,0:T(8,128)(2,1)S(1)}, bf16[32,2048]{1,0:T(8,128)(2,1)S(1)}, u32[]{:S(2)}, u32[]{:S(2)}) %collective-permute-start.25) | collective-permute-done | bytes 131104 | tf_op jit(solution)/shard_map/ppermute | solution.py:26
  49.2 2.1 %collective-permute-done.26 = bf16[32,2048]{1,0:T(8,128)(2,1)S(1)} collective-permute-done((bf16[32,2048]{1,0:T(8,128)(2,1)S(1)}, bf16[32,2048]{1,0:T(8,128)(2,1)S(1)}, u32[]{:S(2)}, u32[]{:S(2)}) %collective-permute-start.26) | collective-permute-done | bytes 131104 | tf_op jit(solution)/shard_map/ppermute | solution.py:26
  51.4 0.7 %add_convert_fusion = bf16[32,2048]{1,0:T(8,128)(2,1)} fusion(bf16[32,2048]{1,0:T(8,128)(2,1)S(1)} %collective-permute-done.27, bf16[32,2048]{1,0:T(8,128)(2,1)S(1)} %collective-permute-done.26, f32[32,2048]{1,0:T(8,128)S(1)} %get-tuple-element.36, bf16[32,2048]{1,0:T(8,128)(2,1)S(1)} %collective-permute-done.25), kind=kLoop, calls=%fused_computation | loop fusion | flops 458752 | bytes 786432 | tf_op jit(solution)/shard_map/convert_element_type | solution.py:485
  (51 shorter events, 1.6 us)
Async XLA Ops:
  0.6 12.2 %collective-permute-start.7 = (bf16[64,2048]{1,0:T(8,128)(2,1)}, bf16[64,2048]{1,0:T(8,128)(2,1)S(1)}, u32[]{:S(2)}, u32[]{:S(2)}) collective-permute-start(bf16[64,2048]{1,0:T(8,128)(2,1)} %bitcast.23), channel_id=1, source_target_pairs={{0,1},{1,0},{2,3},{3,2},{4,5},{5,4},{6,7},{7,6},{8,9},{9,8},{10,11... | collective-permute-start | bytes 786440 | tf_op jit(solution)/shard_map/ppermute | solution.py:26
  1.2 7.0 %collective-permute-start = (bf16[256,256]{1,0:T(8,128)(2,1)}, bf16[256,256]{1,0:T(8,128)(2,1)S(1)}, u32[]{:S(2)}, u32[]{:S(2)}) collective-permute-start(bf16[256,256]{1,0:T(8,128)(2,1)} %refs_0_.1), channel_id=1, source_target_pairs={{0,2},{1,3},{2,0},{3,1},{4,6},{5,7},{6,4},{7,5},{8,10},{9,11},{10,... | collective-permute-start | bytes 393224 | tf_op jit(solution)/shard_map/ppermute | solution.py:26
  3.7 8.6 %collective-permute-start.1 = (bf16[256,256]{1,0:T(8,128)(2,1)}, bf16[256,256]{1,0:T(8,128)(2,1)S(1)}, u32[]{:S(2)}, u32[]{:S(2)}) collective-permute-start(bf16[256,256]{1,0:T(8,128)(2,1)} %refs_0_.1), channel_id=1, source_target_pairs={{0,4},{1,5},{2,6},{3,7},{4,0},{5,1},{6,2},{7,3},{8,12},{9,13},{10,... | collective-permute-start | bytes 393224 | tf_op jit(solution)/shard_map/ppermute | solution.py:26
  5.3 7.1 %collective-permute-start.2 = (bf16[256,256]{1,0:T(8,128)(2,1)}, bf16[256,256]{1,0:T(8,128)(2,1)S(1)}, u32[]{:S(2)}, u32[]{:S(2)}) collective-permute-start(bf16[256,256]{1,0:T(8,128)(2,1)} %refs_0_.1), channel_id=1, source_target_pairs={{0,6},{1,7},{2,4},{3,5},{4,2},{5,3},{6,0},{7,1},{8,14},{9,15},{10,... | collective-permute-start | bytes 393224 | tf_op jit(solution)/shard_map/ppermute | solution.py:26
  5.3 9.8 %collective-permute-start.3 = (bf16[256,256]{1,0:T(8,128)(2,1)}, bf16[256,256]{1,0:T(8,128)(2,1)S(1)}, u32[]{:S(2)}, u32[]{:S(2)}) collective-permute-start(bf16[256,256]{1,0:T(8,128)(2,1)} %refs_0_.1), channel_id=1, source_target_pairs={{0,1},{1,0},{2,3},{3,2},{4,5},{5,4},{6,7},{7,6},{8,9},{9,8},{10,11... | collective-permute-start | bytes 393224 | tf_op jit(solution)/shard_map/ppermute | solution.py:26
  8.2 6.9 %collective-permute-start.4 = (bf16[256,256]{1,0:T(8,128)(2,1)S(1)}, bf16[256,256]{1,0:T(8,128)(2,1)S(1)}, u32[]{:S(2)}, u32[]{:S(2)}) collective-permute-start(bf16[256,256]{1,0:T(8,128)(2,1)S(1)} %collective-permute-done.refs_1_), channel_id=1, source_target_pairs={{0,1},{1,0},{2,3},{3,2},{4,5},{5,4},{6,7},{7,6},{8,9},{9,8},{10,11... | collective-permute-start | bytes 393224 | tf_op jit(solution)/shard_map/ppermute | solution.py:26
  12.3 2.8 %collective-permute-start.5 = (bf16[256,256]{1,0:T(8,128)(2,1)S(1)}, bf16[256,256]{1,0:T(8,128)(2,1)S(1)}, u32[]{:S(2)}, u32[]{:S(2)}) collective-permute-start(bf16[256,256]{1,0:T(8,128)(2,1)S(1)} %collective-permute-done.1.refs_2_), channel_id=1, source_target_pairs={{0,1},{1,0},{2,3},{3,2},{4,5},{5,4},{6,7},{7,6},{8,9},{9,8},{10,11... | collective-permute-start | bytes 393224 | tf_op jit(solution)/shard_map/ppermute | solution.py:26
  12.3 2.8 %collective-permute-start.6 = (bf16[256,256]{1,0:T(8,128)(2,1)S(1)}, bf16[256,256]{1,0:T(8,128)(2,1)S(1)}, u32[]{:S(2)}, u32[]{:S(2)}) collective-permute-start(bf16[256,256]{1,0:T(8,128)(2,1)S(1)} %collective-permute-done.2.refs_3_), channel_id=1, source_target_pairs={{0,1},{1,0},{2,3},{3,2},{4,5},{5,4},{6,7},{7,6},{8,9},{9,8},{10,11... | collective-permute-start | bytes 393224 | tf_op jit(solution)/shard_map/ppermute | solution.py:26
  12.8 17.2 %collective-permute-start.22 = (bf16[512,256]{1,0:T(8,128)(2,1)}, bf16[512,256]{1,0:T(8,128)(2,1)S(1)}, u32[]{:S(2)}, u32[]{:S(2)}) collective-permute-start(bf16[512,256]{1,0:T(8,128)(2,1)} %refs_6_.1), channel_id=1, source_target_pairs={{0,1},{1,0},{2,3},{3,2},{4,5},{5,4},{6,7},{7,6},{8,9},{9,8},{10,11... | collective-permute-start | bytes 786440 | tf_op jit(solution)/shard_map/ppermute | solution.py:26
  15.8 12.7 %copy-start = (bf16[2048,128]{1,0:T(8,128)(2,1)S(1)}, bf16[2048,128]{1,0:T(8,128)(2,1)}, u32[]{:S(2)}) copy-start(bf16[2048,128]{1,0:T(8,128)(2,1)} %refs_3_.1) | copy-start | bytes 1572868
  16.9 6.2 %collective-permute-start.10 = (bf16[152,128]{1,0:T(8,128)(2,1)S(1)}, bf16[152,128]{1,0:T(8,128)(2,1)S(1)}, u32[]{:S(2)}, u32[]{:S(2)}) collective-permute-start(bf16[152,128]{1,0:T(8,128)(2,1)S(1)} %get-tuple-element.26.refs_8_), channel_id=1, source_target_pairs={{0,24},{8,16},{16,8},{24,0},{1,25},{9,17},{17,9},{25,1},{2,26},{10... | collective-permute-start | bytes 116744 | tf_op jit(solution)/shard_map/ppermute | solution.py:26
  20.6 6.4 %collective-permute-start.8 = (bf16[152,128]{1,0:T(8,128)(2,1)S(1)}, bf16[152,128]{1,0:T(8,128)(2,1)S(1)}, u32[]{:S(2)}, u32[]{:S(2)}) collective-permute-start(bf16[152,128]{1,0:T(8,128)(2,1)S(1)} %get-tuple-element.26.refs_8_), channel_id=1, source_target_pairs={{0,8},{8,0},{16,24},{24,16},{1,9},{9,1},{17,25},{25,17},{2,10},{10... | collective-permute-start | bytes 116744 | tf_op jit(solution)/shard_map/ppermute | solution.py:26
  20.6 4.9 %collective-permute-start.9 = (bf16[152,128]{1,0:T(8,128)(2,1)S(1)}, bf16[152,128]{1,0:T(8,128)(2,1)S(1)}, u32[]{:S(2)}, u32[]{:S(2)}) collective-permute-start(bf16[152,128]{1,0:T(8,128)(2,1)S(1)} %get-tuple-element.26.refs_8_), channel_id=1, source_target_pairs={{0,16},{8,24},{16,0},{24,8},{1,17},{9,25},{17,1},{25,9},{2,18},{10... | collective-permute-start | bytes 116744 | tf_op jit(solution)/shard_map/ppermute | solution.py:26
  21.4 8.8 %collective-permute-start.18 = (bf16[144,128]{1,0:T(8,128)(2,1)S(1)}, bf16[144,128]{1,0:T(8,128)(2,1)S(1)}, u32[]{:S(2)}, u32[]{:S(2)}) collective-permute-start(bf16[144,128]{1,0:T(8,128)(2,1)S(1)} %get-tuple-element.43.refs_4_), channel_id=1, source_target_pairs={{0,2},{1,3},{2,0},{3,1},{4,6},{5,7},{6,4},{7,5},{8,10},{9,11},{10,... | collective-permute-start | bytes 110600 | tf_op jit(solution)/shard_map/ppermute | solution.py:26
  23.2 17.0 %collective-permute-start.24 = (bf16[256,2048]{1,0:T(8,128)(2,1)S(1)}, bf16[256,2048]{1,0:T(8,128)(2,1)S(1)}, u32[]{:S(2)}, u32[]{:S(2)}) collective-permute-start(bf16[256,2048]{1,0:T(8,128)(2,1)S(1)} %get-tuple-element.35.refs_12_), channel_id=1, source_target_pairs={{0,1},{1,0},{2,3},{3,2},{4,5},{5,4},{6,7},{7,6},{8,9},{9,8},{10,11... | collective-permute-start | bytes 3145736 | tf_op jit(solution)/shard_map/ppermute | solution.py:26
  25.5 5.3 %collective-permute-start.19 = (bf16[144,128]{1,0:T(8,128)(2,1)S(1)}, bf16[144,128]{1,0:T(8,128)(2,1)S(1)}, u32[]{:S(2)}, u32[]{:S(2)}) collective-permute-start(bf16[144,128]{1,0:T(8,128)(2,1)S(1)} %get-tuple-element.43.refs_4_), channel_id=1, source_target_pairs={{0,4},{1,5},{2,6},{3,7},{4,0},{5,1},{6,2},{7,3},{8,12},{9,13},{10,... | collective-permute-start | bytes 110600 | tf_op jit(solution)/shard_map/ppermute | solution.py:26
  27.0 5.3 %collective-permute-start.20 = (bf16[144,128]{1,0:T(8,128)(2,1)S(1)}, bf16[144,128]{1,0:T(8,128)(2,1)S(1)}, u32[]{:S(2)}, u32[]{:S(2)}) collective-permute-start(bf16[144,128]{1,0:T(8,128)(2,1)S(1)} %get-tuple-element.43.refs_4_), channel_id=1, source_target_pairs={{0,6},{1,7},{2,4},{3,5},{4,2},{5,3},{6,0},{7,1},{8,14},{9,15},{10,... | collective-permute-start | bytes 110600 | tf_op jit(solution)/shard_map/ppermute | solution.py:26
  30.1 8.8 %copy-start.1 = (bf16[512,256]{1,0:T(8,128)(2,1)S(1)}, bf16[512,256]{1,0:T(8,128)(2,1)}, u32[]{:S(2)}) copy-start(bf16[512,256]{1,0:T(8,128)(2,1)} %refs_6_.1) | copy-start | bytes 786436
  30.1 3.7 %collective-permute-start.23 = (bf16[128,384]{1,0:T(8,128)(2,1)S(1)}, bf16[128,384]{1,0:T(8,128)(2,1)S(1)}, u32[]{:S(2)}, u32[]{:S(2)}) collective-permute-start(bf16[128,384]{1,0:T(8,128)(2,1)S(1)} %get-tuple-element.32), channel_id=1, source_target_pairs={{0,1},{1,0},{2,3},{3,2},{4,5},{5,4},{6,7},{7,6},{8,9},{9,8},{10,11... | collective-permute-start | bytes 294920 | tf_op jit(solution)/shard_map/ppermute | solution.py:26
  30.2 6.0 %collective-permute-start.12 = (bf16[3,144,128]{2,1,0:T(8,128)(2,1)S(1)}, bf16[3,144,128]{2,1,0:T(8,128)(2,1)S(1)}, u32[]{:S(2)}, u32[]{:S(2)}) collective-permute-start(bf16[3,144,128]{2,1,0:T(8,128)(2,1)S(1)} %pad_maximum_fusion.1.refs_0_), channel_id=1, source_target_pairs={{0,2},{1,3},{2,0},{3,1},{4,6},{5,7},{6,4},{7,5},{8,10},{9,11},{10,... | collective-permute-start | bytes 331784 | tf_op jit(solution)/shard_map/ppermute | solution.py:26
  30.8 7.5 %collective-permute-start.14 = (bf16[3,144,128]{2,1,0:T(8,128)(2,1)S(1)}, bf16[3,144,128]{2,1,0:T(8,128)(2,1)S(1)}, u32[]{:S(2)}, u32[]{:S(2)}) collective-permute-start(bf16[3,144,128]{2,1,0:T(8,128)(2,1)S(1)} %pad_maximum_fusion.1.refs_0_), channel_id=1, source_target_pairs={{0,4},{1,5},{2,6},{3,7},{4,0},{5,1},{6,2},{7,3},{8,12},{9,13},{10,... | collective-permute-start | bytes 331784 | tf_op jit(solution)/shard_map/ppermute | solution.py:26
  32.3 6.0 %collective-permute-start.16 = (bf16[3,144,128]{2,1,0:T(8,128)(2,1)S(1)}, bf16[3,144,128]{2,1,0:T(8,128)(2,1)S(1)}, u32[]{:S(2)}, u32[]{:S(2)}) collective-permute-start(bf16[3,144,128]{2,1,0:T(8,128)(2,1)S(1)} %pad_maximum_fusion.1.refs_0_), channel_id=1, source_target_pairs={{0,6},{1,7},{2,4},{3,5},{4,2},{5,3},{6,0},{7,1},{8,14},{9,15},{10,... | collective-permute-start | bytes 331784 | tf_op jit(solution)/shard_map/ppermute | solution.py:26
  33.8 5.1 %collective-permute-start.11 = (bf16[3,144,128]{2,1,0:T(8,128)(2,1)S(1)}, bf16[3,144,128]{2,1,0:T(8,128)(2,1)S(1)}, u32[]{:S(2)}, u32[]{:S(2)}) collective-permute-start(bf16[3,144,128]{2,1,0:T(8,128)(2,1)S(1)} %pad_maximum_fusion.1.refs_0_), channel_id=1, source_target_pairs={{0,1},{1,0},{2,3},{3,2},{4,5},{5,4},{6,7},{7,6},{8,9},{9,8},{10,11... | collective-permute-start | bytes 331784 | tf_op jit(solution)/shard_map/ppermute | solution.py:26
  33.8 5.1 %copy-start.4 = (f32[512]{0:T(512)S(1)}, f32[512]{0:T(512)}, u32[]{:S(2)}) copy-start(f32[512]{0:T(512)} %param.18) | copy-start | bytes 6148
  36.2 3.8 %collective-permute-start.21 = (bf16[4,144,128]{2,1,0:T(8,128)(2,1)S(1)}, bf16[4,144,128]{2,1,0:T(8,128)(2,1)S(1)}, u32[]{:S(2)}, u32[]{:S(2)}) collective-permute-start(bf16[4,144,128]{2,1,0:T(8,128)(2,1)S(1)} %pad_maximum_fusion), channel_id=1, source_target_pairs={{0,1},{1,0},{2,3},{3,2},{4,5},{5,4},{6,7},{7,6},{8,9},{9,8},{10,11... | collective-permute-start | bytes 442376 | tf_op jit(solution)/shard_map/ppermute | solution.py:26
  38.3 1.7 %collective-permute-start.13 = (bf16[3,144,128]{2,1,0:T(8,128)(2,1)S(1)}, bf16[3,144,128]{2,1,0:T(8,128)(2,1)S(1)}, u32[]{:S(2)}, u32[]{:S(2)}) collective-permute-start(bf16[3,144,128]{2,1,0:T(8,128)(2,1)S(1)} %collective-permute-done.12.refs_1_), channel_id=1, source_target_pairs={{0,1},{1,0},{2,3},{3,2},{4,5},{5,4},{6,7},{7,6},{8,9},{9,8},{10,11... | collective-permute-start | bytes 331784 | tf_op jit(solution)/shard_map/ppermute | solution.py:26
  38.3 1.7 %collective-permute-start.15 = (bf16[3,144,128]{2,1,0:T(8,128)(2,1)S(1)}, bf16[3,144,128]{2,1,0:T(8,128)(2,1)S(1)}, u32[]{:S(2)}, u32[]{:S(2)}) collective-permute-start(bf16[3,144,128]{2,1,0:T(8,128)(2,1)S(1)} %collective-permute-done.14.refs_2_), channel_id=1, source_target_pairs={{0,1},{1,0},{2,3},{3,2},{4,5},{5,4},{6,7},{7,6},{8,9},{9,8},{10,11... | collective-permute-start | bytes 331784 | tf_op jit(solution)/shard_map/ppermute | solution.py:26
  38.8 1.3 %collective-permute-start.17 = (bf16[3,144,128]{2,1,0:T(8,128)(2,1)S(1)}, bf16[3,144,128]{2,1,0:T(8,128)(2,1)S(1)}, u32[]{:S(2)}, u32[]{:S(2)}) collective-permute-start(bf16[3,144,128]{2,1,0:T(8,128)(2,1)S(1)} %collective-permute-done.16.refs_3_), channel_id=1, source_target_pairs={{0,1},{1,0},{2,3},{3,2},{4,5},{5,4},{6,7},{7,6},{8,9},{9,8},{10,11... | collective-permute-start | bytes 331784 | tf_op jit(solution)/shard_map/ppermute | solution.py:26
  41.8 7.4 %collective-permute-start.25 = (bf16[32,2048]{1,0:T(8,128)(2,1)S(1)}, bf16[32,2048]{1,0:T(8,128)(2,1)S(1)}, u32[]{:S(2)}, u32[]{:S(2)}) collective-permute-start(bf16[32,2048]{1,0:T(8,128)(2,1)S(1)} %get-tuple-element.37), channel_id=1, source_target_pairs={{0,6},{1,7},{2,4},{3,5},{4,2},{5,3},{6,0},{7,1},{8,14},{9,15},{10,... | collective-permute-start | bytes 393224 | tf_op jit(solution)/shard_map/ppermute | solution.py:26
  43.3 8.0 %collective-permute-start.26 = (bf16[32,2048]{1,0:T(8,128)(2,1)S(1)}, bf16[32,2048]{1,0:T(8,128)(2,1)S(1)}, u32[]{:S(2)}, u32[]{:S(2)}) collective-permute-start(bf16[32,2048]{1,0:T(8,128)(2,1)S(1)} %get-tuple-element.38), channel_id=1, source_target_pairs={{0,4},{1,5},{2,6},{3,7},{4,0},{5,1},{6,2},{7,3},{8,12},{9,13},{10,... | collective-permute-start | bytes 393224 | tf_op jit(solution)/shard_map/ppermute | solution.py:26
  44.8 6.6 %collective-permute-start.27 = (bf16[32,2048]{1,0:T(8,128)(2,1)S(1)}, bf16[32,2048]{1,0:T(8,128)(2,1)S(1)}, u32[]{:S(2)}, u32[]{:S(2)}) collective-permute-start(bf16[32,2048]{1,0:T(8,128)(2,1)S(1)} %get-tuple-element.39), channel_id=1, source_target_pairs={{0,2},{1,3},{2,0},{3,1},{4,6},{5,7},{6,4},{7,5},{8,10},{9,11},{10,... | collective-permute-start | bytes 393224 | tf_op jit(solution)/shard_map/ppermute | solution.py:26
  45.3 1.2 %collective-permute-start.28 = (f32[1,128]{1,0:T(1,128)S(1)}, f32[1,128]{1,0:T(1,128)S(1)}, u32[]{:S(2)}, u32[]{:S(2)}) collective-permute-start(f32[1,128]{1,0:T(1,128)S(1)} %get-tuple-element.41), channel_id=1, source_target_pairs={{0,1},{1,0},{2,3},{3,2},{4,5},{5,4},{6,7},{7,6},{8,9},{9,8},{10,11... | collective-permute-start | bytes 1544 | tf_op jit(solution)/shard_map/ppermute | solution.py:26
  (3 other events, 3.6 us)

commit v3 on v2

--- a/solution.py
+++ b/solution.py
@@ -83,7 +83,7 @@
 
 
 def prepare(
-    latent_ref, rope_ref, query_ref, pre_ref, value_ref, attend_ref, conv_ref, partner_ref,
+    latent_ref, rope_ref, query_ref, pre_ref, value_ref, attend_ref, conv_ref, expand_ref, partner_ref,
     key_w_ref, query_w_ref, mix_w_ref, own_w_ref, cos_ref, sin_ref, sems,
 ):
     core = lax.axis_index("tp") % 2
@@ -97,8 +97,13 @@
         (query_ref, query_w_ref.at[: NOPE + ROPE]),
         (query_ref.at[NOPE:], query_w_ref.at[NOPE + ROPE :]),
         (attend_ref, own_w_ref.at[:VDIM]),
-        (conv_ref, own_w_ref.at[VDIM:]),
+        (conv_ref, own_w_ref.at[VDIM : 2 * VDIM]),
     ]
+    wide = NOPE + VDIM
+    high = own_w_ref.shape[0] - 2 * VDIM
+    for k in range(own_w_ref.shape[1] // wide):
+        target = own_w_ref.at[2 * VDIM :, k * wide : (k + 1) * wide]
+        moves.append((expand_ref.at[k * high : (k + 1) * high], target))
     copies = [pltpu.make_async_copy(source, target, sems.at[i]) for i, (source, target) in enumerate(moves)]
     for copy in copies:
         copy.start()
@@ -210,14 +215,17 @@
             ref[i * rows : (i + 1) * rows, :] = both_ref[source, :].astype(BF16)
 
 
-def attend(slots, chunk, last, *refs):
+def attend(slots, chunk, stage, *refs):
     inputs = 1 + max(place for chip_slots in slots for place, _ in chip_slots)
     pieces, refs = refs[:inputs], refs[inputs:]
-    gain_ref, expand_refs, query_refs = refs[0], refs[1:3], refs[3:5]
+    gain_ref, own_w_ref, other_w_ref, query_refs = refs[0], refs[1], refs[2], refs[3:5]
     refs = refs[5:]
+    if stage > 0:
+        stats_in, out_in = refs[:2]
+        refs = refs[2:]
+    last = stage == 2
     if last:
-        stats_in, out_in, own_w_ref, other_w_ref = refs[:4]
-        block_refs, (keep_log_ref, send_log_ref, both_ref) = refs[4:-5], refs[-5:-2]
+        block_refs, (keep_log_ref, send_log_ref, both_ref) = refs[:-5], refs[-5:-2]
     else:
         stats_ref, out_ref = refs[:2]
     latent_ref, rope_ref = refs[-2:]
@@ -237,8 +245,14 @@
         zeros = jnp.zeros_like(rope)
         sides = (jnp.where(low, rope, zeros), jnp.where(low, zeros, rope))
         queries.append([jnp.concatenate([nope, side], axis=1) for side in sides])
-    key_w = jnp.concatenate([ref[:, :NOPE] for ref in expand_refs], axis=1)
-    value_w = jnp.concatenate([ref[:, NOPE:] for ref in expand_refs], axis=1)
+    wide = NOPE + VDIM
+    starts = range(0, own_w_ref.shape[1], wide)
+
+    def expansion(ref, begin, size):
+        return jnp.concatenate([ref[2 * VDIM :, k + begin : k + begin + size] for k in starts], axis=0)
+
+    key_w = jnp.concatenate([expansion(ref, 0, NOPE) for ref in (own_w_ref, other_w_ref)], axis=1)
+    value_w = jnp.concatenate([expansion(ref, NOPE, VDIM) for ref in (own_w_ref, other_w_ref)], axis=1)
     views = [(chip ^ i, chip_slots) for i, chip_slots in enumerate(slots)]
 
     def rows_of(chip_slots, slot, first, start, count):
@@ -301,7 +315,7 @@
             out = out + state[2] * rescale
         return peak, total, out
 
-    state = (stats_in[0:1], stats_in[1:2], out_in[...]) if last else None
+    state = (stats_in[0:1], stats_in[1:2], out_in[...]) if stage > 0 else None
     if chunk == len(views[0][1]):
         peak, total, out = one_chunk(None, state)
     else:
@@ -329,7 +343,7 @@
         both_ref[i, :, :VDIM] = attended
         both_ref[i, :, VDIM:] = query_refs[i][:, NOPE + LANES :]
         order = [both_ref[i, pl.ds(pl.multiple_of((chip ^ j) * rows, rows), rows), :] for j in range(pairs)]
-        product = jnp.dot(jnp.concatenate(order, axis=0), weight_ref[...], preferred_element_type=F32)
+        product = jnp.dot(jnp.concatenate(order, axis=0), weight_ref[: 2 * VDIM], preferred_element_type=F32)
         result = product if result is None else result + product
     for i, ref in enumerate(block_refs):
         ref[...] = result[i * rows : (i + 1) * rows].astype(ref.dtype)
@@ -380,25 +394,24 @@
 
     latent_t = latent_weight.T
     partner_t = swap(latent_t, "tp", 1)
-    other_expand = swap(expand_weight, "tp", 1)
     key_w, query_w, mix_w, own_w, cosines, sines = kernel_call(
         prepare,
         [
             ((4 * ROPE, features), BF16),
             ((NOPE + 2 * ROPE, features), BF16),
             ((features, 2 * LANES), BF16),
-            ((VDIM + channels, features), BF16),
+            ((VDIM + channels + expand_weight.size // features, features), BF16),
             ((tokens, LANES), F32),
             ((tokens, LANES), F32),
         ],
         16 << 20,
-        scratch=[pltpu.SemaphoreType.DMA((9,))],
+        scratch=[pltpu.SemaphoreType.DMA((9 + features // (NOPE + VDIM),))],
         flops=1 << 28,
         nbytes=1 << 23,
-        in_hbm=range(7),
+        in_hbm=range(8),
     )(
         latent_t, rope_key_weight.T, query_weight.T, pre_weight, value_weight, output_attend, output_conv,
-        partner_t,
+        expand_weight, partner_t,
     )
     other_w = swap(own_w, "tp", 1)
 
@@ -428,14 +441,7 @@
         around, halos = around[:, : half + share], [around[:, half + share :]]
     arounds = [around] + exchange(around, "tp", 2, pairs)
     others = swap_each(arounds)
-    blocks = range(places - 1) if small else range(places)
-    slots = [[(i, k) for k in blocks] for i in range(pairs)]
-    other_slots = slots
-    if small:
-        other_slots = [[(pairs, i)] + chip_slots for i, chip_slots in enumerate(slots)]
-        slots = [[(pairs + i, None)] + chip_slots for i, chip_slots in enumerate(slots)]
-        arounds += nears
-        others.append(near_other)
+    slots = [[(i, k) for k in (range(places - 1) if small else range(places))] for i in range(pairs)]
 
     columns = NOPE + LANES + channels
     keep, send = kernel_call(
@@ -448,34 +454,30 @@
     )(scaled, inv, query_w, gate_weight, cosines, sines, mix, conv_kernel, *halos)
     got = swap(send, "tp", 1)
 
-    chunk = places if small else 4
-
-    def attend_to(arrays, slots, last, outs, *operands):
+    def attend_to(arrays, slots, stage, outs, *state):
+        chunk = len(slots[0]) if small else 4
         scratch = [
             pltpu.VMEM((2, half, VDIM + channels), BF16),
             pltpu.VMEM((chunk * half, pairs * LANES), BF16),
             pltpu.VMEM((chunk * half // 2, LANES), BF16),
         ]
         return kernel_call(
-            functools.partial(attend, slots, chunk, last),
+            functools.partial(attend, slots, chunk, stage),
             outs,
             (14 << 20) if small else (40 << 20),
-            scratch=scratch if last else scratch[1:],
+            scratch=scratch if stage == 2 else scratch[1:],
             flops=1 << 29,
             nbytes=1 << 22,
-        )(*arrays, latent_gain.reshape(1, -1), expand_weight, other_expand, keep, got, *operands)
-
-    stats, out = attend_to(arounds, slots, False, [((8, tokens), F32), ((VDIM, tokens), F32)])
-    *outs, own_log, send_log = attend_to(
-        others,
-        other_slots,
-        True,
-        [((rows, features), F32)] + [((rows, features), BF16)] * (pairs - 1) + [((1, half), F32)] * 2,
-        stats,
-        out,
-        own_w,
-        other_w,
-    )
+        )(*arrays, latent_gain.reshape(1, -1), own_w, other_w, keep, got, *state)
+
+    state_outs = [((8, tokens), F32), ((VDIM, tokens), F32)]
+    state = []
+    if small:
+        near_slots = [[(i, None), (pairs, i)] for i in range(pairs)]
+        state = attend_to([*nears, near_other], near_slots, 0, state_outs)
+    state = attend_to(arounds, slots, 1 if small else 0, state_outs, *state)
+    final_outs = [((rows, features), F32)] + [((rows, features), BF16)] * (pairs - 1) + [((1, half), F32)] * 2
+    *outs, own_log, send_log = attend_to(others, slots, 2, final_outs, *state)
     arrived = exchange_blocks(outs)
     got_log = swap(send_log, "tp", 1)
     (logs,) = kernel_call(join_logs, [((1, tokens), F32)], 1 << 20, flops=1 << 22, nbytes=1 << 12)(own_log, got_log)

time: 52.4 us -> 52.5 us (level)
  local copies, waits for them, and re-layouts: 1.35 us -> 0.05 us
  starting transfers between devices: 21.6 us -> 22.3 us
  Pallas kernels: 7.56 us -> 8.22 us
    unnamed x12 -> x10, local copies, waits for them, and re-layouts: 1.34 us -> 0.03 us
    ppermute x29 -> x28, starting transfers between devices: 21.6 us -> 22.3 us  [swap(): return lax.ppermute(array, axis, [(i, i ^ mask) for i in range(peers)])]
    pallas_call x6 -> x7, Pallas kernels: 7.56 us -> 8.22 us  [call(): pl.pallas_call(body, out_shape=[jax.ShapeDtypeStruct(shape, dtype) for sh...]
    ppermute x29 -> x28, waiting for transfers between devices: 20 us -> 20.2 us  [swap(): return lax.ppermute(array, axis, [(i, i ^ mask) for i in range(peers)])]
  transfers between devices with their start and end apart: 29 -> 28, of which waited for: 11 -> 11; matrix products, arithmetic and copies ran while one was open for 0% -> 0% of each run, Pallas kernels for 11% -> 13%
where the time goes in v3:
time: 52.5 us; the launch traced here: 52.4 us
  starting transfers between devices  22.3 us (42%)
  waiting for transfers between devices  20.2 us (38%)
  Pallas kernels  8.22 us (16%)
  between operations  0.85 us (2%)
  other arithmetic  0.76 us (1%)
    ppermute x28, starting transfers between devices, swap(): return lax.ppermute(array, axis, [(i, i ^ mask) for i in range(peers)])  22.3 us
    ppermute x28, waiting for transfers between devices, swap(): return lax.ppermute(array, axis, [(i, i ^ mask) for i in range(peers)])  20.2 us
    pallas_call x7, Pallas kernels, call(): pl.pallas_call(body, out_shape=[jax.ShapeDtypeStruct(shape, dtype) for sh...  8.22 us
  transfers between devices with their start and end apart: 28, of which 11 were waited for; matrix products, arithmetic and copies ran while one was open for 0% of the time, Pallas kernels for 13%

profile of v3, /device:TPU:0, one launch (start us, length us, event | category | flops | bytes accessed | tf_op | source)
XLA Modules:
  0.0 52.4 jit_solution(8487861988366828824)
XLA Ops:
  0.6 0.6 %collective-permute-start.7 = (bf16[64,2048]{1,0:T(8,128)(2,1)}, bf16[64,2048]{1,0:T(8,128)(2,1)S(1)}, u32[]{:S(2)}, u32[]{:S(2)}) collective-permute-start(bf16[64,2048]{1,0:T(8,128)(2,1)} %bitcast.24), channel_id=1, source_target_pairs={{0,1},{1,0},{2,3},{3,2},{4,5},{5,4},{6,7},{7,6},{8,9},{9,8},{10,11... | collective-permute-start | bytes 786440 | tf_op jit(solution)/shard_map/ppermute | solution.py:26
  1.2 3.5 %collective-permute-start.2 = (bf16[256,256]{1,0:T(8,128)(2,1)}, bf16[256,256]{1,0:T(8,128)(2,1)S(1)}, u32[]{:S(2)}, u32[]{:S(2)}) collective-permute-start(bf16[256,256]{1,0:T(8,128)(2,1)} %refs_0_.1), channel_id=1, source_target_pairs={{0,6},{1,7},{2,4},{3,5},{4,2},{5,3},{6,0},{7,1},{8,14},{9,15},{10,... | collective-permute-start | bytes 393224 | tf_op jit(solution)/shard_map/ppermute | solution.py:26
  4.7 0.5 collective-permute-start.1
  5.3 3.8 %collective-permute-done.2.refs_3_ = bf16[256,256]{1,0:T(8,128)(2,1)S(1)} collective-permute-done((bf16[256,256]{1,0:T(8,128)(2,1)}, bf16[256,256]{1,0:T(8,128)(2,1)S(1)}, u32[]{:S(2)}, u32[]{:S(2)}) %collective-permute-start.2) | collective-permute-done | bytes 131104 | tf_op jit(solution)/shard_map/ppermute | solution.py:26
  9.2 2.6 %collective-permute-done.1.refs_2_ = bf16[256,256]{1,0:T(8,128)(2,1)S(1)} collective-permute-done((bf16[256,256]{1,0:T(8,128)(2,1)}, bf16[256,256]{1,0:T(8,128)(2,1)S(1)}, u32[]{:S(2)}, u32[]{:S(2)}) %collective-permute-start.1) | collective-permute-done | bytes 131104 | tf_op jit(solution)/shard_map/ppermute | solution.py:26
  12.3 2.3 %shard_map.140 = (bf16[256,2048]{1,0:T(8,128)(2,1)S(1)}, bf16[256,2048]{1,0:T(8,128)(2,1)S(1)}, bf16[2048,256]{1,0:T(8,128)(2,1)S(1)}, bf16[320,2048]{1,0:T(8,12...) custom-call(bf16[64,2048]{1,0:T(8,128)(2,1)} %bitcast.25, bf16[64,2048]{1,0:T(8,128)(2,1)} %bitcast.26, ...), custom_call_target="tpu_custom_call" | custom-call | flops 268435456 | bytes 8388608 | tf_op jit(solution)/shard_map/pallas_call | solution.py:59
  15.0 1.1 %shard_map.141 = (bf16[256,2048]{1,0:T(8,128)(2,1)S(1)}, f32[256,128]{1,0:T(8,128)S(1)}, bf16[152,128]{1,0:T(8,128)(2,1)S(1)}, bf16[256,128]{1,0:T(8,128)(2,1)S(1)}) custom-call(bf16[256,256]{1,0:T(8,128)(2,1)S(1)} %copy-done.1, bf16[256,256]{1,0:T(8,128)(2,1)S(1)} %collective-permute-done.refs_1_, bf16[256,256]{1,0:T(8,128)(2,1)S(1)} %collective-permute-done.1.refs_2_, ...), custom_call_target="tpu_custom_call" | custom-call | flops 536870912 | bytes 2097152 | tf_op jit(solution)/shard_map/pallas_call | solution.py:59
  16.2 1.6 %collective-permute-start.22 = (bf16[144,128]{1,0:T(8,128)(2,1)S(1)}, bf16[144,128]{1,0:T(8,128)(2,1)S(1)}, u32[]{:S(2)}, u32[]{:S(2)}) collective-permute-start(bf16[144,128]{1,0:T(8,128)(2,1)S(1)} %get-tuple-element.47.refs_0_), channel_id=1, source_target_pairs={{0,6},{1,7},{2,4},{3,5},{4,2},{5,3},{6,0},{7,1},{8,14},{9,15},{10,... | collective-permute-start | bytes 110600 | tf_op jit(solution)/shard_map/ppermute | solution.py:26
  17.7 1.5 %collective-permute-start.21 = (bf16[144,128]{1,0:T(8,128)(2,1)S(1)}, bf16[144,128]{1,0:T(8,128)(2,1)S(1)}, u32[]{:S(2)}, u32[]{:S(2)}) collective-permute-start(bf16[144,128]{1,0:T(8,128)(2,1)S(1)} %get-tuple-element.47.refs_0_), channel_id=1, source_target_pairs={{0,4},{1,5},{2,6},{3,7},{4,0},{5,1},{6,2},{7,3},{8,12},{9,13},{10,... | collective-permute-start | bytes 110600 | tf_op jit(solution)/shard_map/ppermute | solution.py:26
  19.2 0.5 %collective-permute-start.20 = (bf16[144,128]{1,0:T(8,128)(2,1)S(1)}, bf16[144,128]{1,0:T(8,128)(2,1)S(1)}, u32[]{:S(2)}, u32[]{:S(2)}) collective-permute-start(bf16[144,128]{1,0:T(8,128)(2,1)S(1)} %get-tuple-element.47.refs_0_), channel_id=1, source_target_pairs={{0,2},{1,3},{2,0},{3,1},{4,6},{5,7},{6,4},{7,5},{8,10},{9,11},{10,... | collective-permute-start | bytes 110600 | tf_op jit(solution)/shard_map/ppermute | solution.py:26
  19.7 3.6 %collective-permute-start.10 = (bf16[152,128]{1,0:T(8,128)(2,1)S(1)}, bf16[152,128]{1,0:T(8,128)(2,1)S(1)}, u32[]{:S(2)}, u32[]{:S(2)}) collective-permute-start(bf16[152,128]{1,0:T(8,128)(2,1)S(1)} %get-tuple-element.28.refs_8_), channel_id=1, source_target_pairs={{0,24},{8,16},{16,8},{24,0},{1,25},{9,17},{17,9},{25,1},{2,26},{10... | collective-permute-start | bytes 116744 | tf_op jit(solution)/shard_map/ppermute | solution.py:26
  23.7 1.6 %collective-permute-start.8 = (bf16[152,128]{1,0:T(8,128)(2,1)S(1)}, bf16[152,128]{1,0:T(8,128)(2,1)S(1)}, u32[]{:S(2)}, u32[]{:S(2)}) collective-permute-start(bf16[152,128]{1,0:T(8,128)(2,1)S(1)} %get-tuple-element.28.refs_8_), channel_id=1, source_target_pairs={{0,8},{8,0},{16,24},{24,16},{1,9},{9,1},{17,25},{25,17},{2,10},{10... | collective-permute-start | bytes 116744 | tf_op jit(solution)/shard_map/ppermute | solution.py:26
  25.4 0.5 collective-permute-done.10.refs_11_
  25.9 2.3 %collective-permute-done.9.refs_10_ = bf16[152,128]{1,0:T(8,128)(2,1)S(1)} collective-permute-done((bf16[152,128]{1,0:T(8,128)(2,1)S(1)}, bf16[152,128]{1,0:T(8,128)(2,1)S(1)}, u32[]{:S(2)}, u32[]{:S(2)}) %collective-permute-start.9) | collective-permute-done | bytes 38944 | tf_op jit(solution)/shard_map/ppermute | solution.py:26
  28.2 0.9 %shard_map.142 = (bf16[128,384]{1,0:T(8,128)(2,1)S(1)}, bf16[128,384]{1,0:T(8,128)(2,1)S(1)}) custom-call(bf16[256,2048]{1,0:T(8,128)(2,1)S(1)} %get-tuple-element.30.refs_0_, f32[256,128]{1,0:T(8,128)S(1)} %get-tuple-element.31.refs_1_, bf16[256,2048]{1,0:T(8,128)(2,1)S(1)} %get-tuple-element.32.refs_2_, bf16[2048,128]{1,0:T(8,128)(2,1)S(1)} %copy-done, ...), custom_call_target="tpu_custom_call" | custom-call | flops 402653184 | bytes 2097152 | tf_op jit(solution)/shard_map/pallas_call | solution.py:59
  29.3 1.7 %collective-permute-start.16 = (bf16[3,144,128]{2,1,0:T(8,128)(2,1)S(1)}, bf16[3,144,128]{2,1,0:T(8,128)(2,1)S(1)}, u32[]{:S(2)}, u32[]{:S(2)}) collective-permute-start(bf16[3,144,128]{2,1,0:T(8,128)(2,1)S(1)} %pad_maximum_fusion.1.refs_0_), channel_id=1, source_target_pairs={{0,6},{1,7},{2,4},{3,5},{4,2},{5,3},{6,0},{7,1},{8,14},{9,15},{10,... | collective-permute-start | bytes 331784 | tf_op jit(solution)/shard_map/ppermute | solution.py:26
  31.0 1.3 %collective-permute-start.14 = (bf16[3,144,128]{2,1,0:T(8,128)(2,1)S(1)}, bf16[3,144,128]{2,1,0:T(8,128)(2,1)S(1)}, u32[]{:S(2)}, u32[]{:S(2)}) collective-permute-start(bf16[3,144,128]{2,1,0:T(8,128)(2,1)S(1)} %pad_maximum_fusion.1.refs_0_), channel_id=1, source_target_pairs={{0,4},{1,5},{2,6},{3,7},{4,0},{5,1},{6,2},{7,3},{8,12},{9,13},{10,... | collective-permute-start | bytes 331784 | tf_op jit(solution)/shard_map/ppermute | solution.py:26
  32.3 0.5 %collective-permute-start.12 = (bf16[3,144,128]{2,1,0:T(8,128)(2,1)S(1)}, bf16[3,144,128]{2,1,0:T(8,128)(2,1)S(1)}, u32[]{:S(2)}, u32[]{:S(2)}) collective-permute-start(bf16[3,144,128]{2,1,0:T(8,128)(2,1)S(1)} %pad_maximum_fusion.1.refs_0_), channel_id=1, source_target_pairs={{0,2},{1,3},{2,0},{3,1},{4,6},{5,7},{6,4},{7,5},{8,10},{9,11},{10,... | collective-permute-start | bytes 331784 | tf_op jit(solution)/shard_map/ppermute | solution.py:26
  32.8 3.3 %collective-permute-done.16.refs_3_ = bf16[3,144,128]{2,1,0:T(8,128)(2,1)S(1)} collective-permute-done((bf16[3,144,128]{2,1,0:T(8,128)(2,1)S(1)}, bf16[3,144,128]{2,1,0:T(8,128)(2,1)S(1)}, u32[]{:S(2)}, u32[]{:S(2)}) %collective-permute-start.16) | collective-permute-done | bytes 110624 | tf_op jit(solution)/shard_map/ppermute | solution.py:26
  36.2 1.9 %collective-permute-done.14.refs_2_ = bf16[3,144,128]{2,1,0:T(8,128)(2,1)S(1)} collective-permute-done((bf16[3,144,128]{2,1,0:T(8,128)(2,1)S(1)}, bf16[3,144,128]{2,1,0:T(8,128)(2,1)S(1)}, u32[]{:S(2)}, u32[]{:S(2)}) %collective-permute-start.14) | collective-permute-done | bytes 110624 | tf_op jit(solution)/shard_map/ppermute | solution.py:26
  38.1 0.5 collective-permute-start.15
  38.6 0.8 %shard_map.143 = (f32[8,256]{1,0:T(8,128)S(1)}, f32[128,256]{1,0:T(8,128)S(1)}) custom-call(bf16[144,128]{1,0:T(8,128)(2,1)S(1)} %get-tuple-element.47.refs_0_, bf16[144,128]{1,0:T(8,128)(2,1)S(1)} %collective-permute-done.20.refs_1_, bf16[144,128]{1,0:T(8,128)(2,1)S(1)} %collective-permute-done.21.refs_2_, ...), custom_call_target="tpu_custom_call" | custom-call | flops 536870912 | bytes 4194304 | tf_op jit(solution)/shard_map/pallas_call | solution.py:59
  39.4 1.0 %shard_map.144 = (f32[8,256]{1,0:T(8,128)S(1)}, f32[128,256]{1,0:T(8,128)S(1)}) custom-call(bf16[3,144,128]{2,1,0:T(8,128)(2,1)S(1)} %pad_maximum_fusion.1.refs_0_, bf16[3,144,128]{2,1,0:T(8,128)(2,1)S(1)} %collective-permute-done.12.refs_1_, bf16[3,144,128]{2,1,0:T(8,128)(2,1)S(1)} %collective-permute-done.14.refs_2_, ...), custom_call_target="tpu_custom_call" | custom-call | flops 536870912 | bytes 4194304 | tf_op jit(solution)/shard_map/pallas_call | solution.py:59
  40.5 1.5 %shard_map.145 = (f32[32,2048]{1,0:T(8,128)S(1)}, bf16[32,2048]{1,0:T(8,128)(2,1)S(1)}, bf16[32,2048]{1,0:T(8,128)(2,1)S(1)}, bf16[32,2048]{1,0:T(8,128)(2,1)S(1...) custom-call(bf16[3,144,128]{2,1,0:T(8,128)(2,1)S(1)} %collective-permute-done.11.refs_0_, ...), custom_call_target="tpu_custom_call" | custom-call | flops 536870912 | bytes 4194304 | tf_op jit(solution)/shard_map/pallas_call | solution.py:59
  42.0 1.8 %collective-permute-start.24 = (bf16[32,2048]{1,0:T(8,128)(2,1)S(1)}, bf16[32,2048]{1,0:T(8,128)(2,1)S(1)}, u32[]{:S(2)}, u32[]{:S(2)}) collective-permute-start(bf16[32,2048]{1,0:T(8,128)(2,1)S(1)} %get-tuple-element.41), channel_id=1, source_target_pairs={{0,6},{1,7},{2,4},{3,5},{4,2},{5,3},{6,0},{7,1},{8,14},{9,15},{10,... | collective-permute-start | bytes 393224 | tf_op jit(solution)/shard_map/ppermute | solution.py:26
  43.8 1.3 %collective-permute-start.25 = (bf16[32,2048]{1,0:T(8,128)(2,1)S(1)}, bf16[32,2048]{1,0:T(8,128)(2,1)S(1)}, u32[]{:S(2)}, u32[]{:S(2)}) collective-permute-start(bf16[32,2048]{1,0:T(8,128)(2,1)S(1)} %get-tuple-element.42), channel_id=1, source_target_pairs={{0,4},{1,5},{2,6},{3,7},{4,0},{5,1},{6,2},{7,3},{8,12},{9,13},{10,... | collective-permute-start | bytes 393224 | tf_op jit(solution)/shard_map/ppermute | solution.py:26
  45.0 0.5 %collective-permute-start.26 = (bf16[32,2048]{1,0:T(8,128)(2,1)S(1)}, bf16[32,2048]{1,0:T(8,128)(2,1)S(1)}, u32[]{:S(2)}, u32[]{:S(2)}) collective-permute-start(bf16[32,2048]{1,0:T(8,128)(2,1)S(1)} %get-tuple-element.43), channel_id=1, source_target_pairs={{0,2},{1,3},{2,0},{3,1},{4,6},{5,7},{6,4},{7,5},{8,10},{9,11},{10,... | collective-permute-start | bytes 393224 | tf_op jit(solution)/shard_map/ppermute | solution.py:26
  45.6 1.2 %collective-permute-done.27.got_ref = f32[1,128]{1,0:T(1,128)S(1)} collective-permute-done((f32[1,128]{1,0:T(1,128)S(1)}, f32[1,128]{1,0:T(1,128)S(1)}, u32[]{:S(2)}, u32[]{:S(2)}) %collective-permute-start.27) | collective-permute-done | bytes 544 | tf_op jit(solution)/shard_map/ppermute | solution.py:26
  46.7 0.6 %shard_map.146 = f32[1,256]{1,0:T(1,128)} custom-call(f32[1,128]{1,0:T(1,128)S(1)} %get-tuple-element.44.own_ref, f32[1,128]{1,0:T(1,128)S(1)} %collective-permute-done.27.got_ref), custom_call_target="tpu_custom_call" | custom-call | flops 4194304 | bytes 4096 | tf_op jit(solution)/shard_map/pallas_call | solution.py:59
  47.4 2.0 %collective-permute-done.24 = bf16[32,2048]{1,0:T(8,128)(2,1)S(1)} collective-permute-done((bf16[32,2048]{1,0:T(8,128)(2,1)S(1)}, bf16[32,2048]{1,0:T(8,128)(2,1)S(1)}, u32[]{:S(2)}, u32[]{:S(2)}) %collective-permute-start.24) | collective-permute-done | bytes 131104 | tf_op jit(solution)/shard_map/ppermute | solution.py:26
  49.4 2.2 %collective-permute-done.25 = bf16[32,2048]{1,0:T(8,128)(2,1)S(1)} collective-permute-done((bf16[32,2048]{1,0:T(8,128)(2,1)S(1)}, bf16[32,2048]{1,0:T(8,128)(2,1)S(1)}, u32[]{:S(2)}, u32[]{:S(2)}) %collective-permute-start.25) | collective-permute-done | bytes 131104 | tf_op jit(solution)/shard_map/ppermute | solution.py:26
  51.7 0.7 %add_convert_fusion = bf16[32,2048]{1,0:T(8,128)(2,1)} fusion(bf16[32,2048]{1,0:T(8,128)(2,1)S(1)} %collective-permute-done.26, bf16[32,2048]{1,0:T(8,128)(2,1)S(1)} %collective-permute-done.25, f32[32,2048]{1,0:T(8,128)S(1)} %get-tuple-element.40, bf16[32,2048]{1,0:T(8,128)(2,1)S(1)} %collective-permute-done.24), kind=kLoop, calls=%fused_computation | loop fusion | flops 458752 | bytes 786432 | tf_op jit(solution)/shard_map/convert_element_type | solution.py:487
  (48 shorter events, 1.9 us)
Async XLA Ops:
  0.6 11.7 %collective-permute-start.7 = (bf16[64,2048]{1,0:T(8,128)(2,1)}, bf16[64,2048]{1,0:T(8,128)(2,1)S(1)}, u32[]{:S(2)}, u32[]{:S(2)}) collective-permute-start(bf16[64,2048]{1,0:T(8,128)(2,1)} %bitcast.24), channel_id=1, source_target_pairs={{0,1},{1,0},{2,3},{3,2},{4,5},{5,4},{6,7},{7,6},{8,9},{9,8},{10,11... | collective-permute-start | bytes 786440 | tf_op jit(solution)/shard_map/ppermute | solution.py:26
  1.2 8.0 %collective-permute-start.2 = (bf16[256,256]{1,0:T(8,128)(2,1)}, bf16[256,256]{1,0:T(8,128)(2,1)S(1)}, u32[]{:S(2)}, u32[]{:S(2)}) collective-permute-start(bf16[256,256]{1,0:T(8,128)(2,1)} %refs_0_.1), channel_id=1, source_target_pairs={{0,6},{1,7},{2,4},{3,5},{4,2},{5,3},{6,0},{7,1},{8,14},{9,15},{10,... | collective-permute-start | bytes 393224 | tf_op jit(solution)/shard_map/ppermute | solution.py:26
  4.7 7.1 %collective-permute-start.1 = (bf16[256,256]{1,0:T(8,128)(2,1)}, bf16[256,256]{1,0:T(8,128)(2,1)S(1)}, u32[]{:S(2)}, u32[]{:S(2)}) collective-permute-start(bf16[256,256]{1,0:T(8,128)(2,1)} %refs_0_.1), channel_id=1, source_target_pairs={{0,4},{1,5},{2,6},{3,7},{4,0},{5,1},{6,2},{7,3},{8,12},{9,13},{10,... | collective-permute-start | bytes 393224 | tf_op jit(solution)/shard_map/ppermute | solution.py:26
  5.2 6.9 %collective-permute-start = (bf16[256,256]{1,0:T(8,128)(2,1)}, bf16[256,256]{1,0:T(8,128)(2,1)S(1)}, u32[]{:S(2)}, u32[]{:S(2)}) collective-permute-start(bf16[256,256]{1,0:T(8,128)(2,1)} %refs_0_.1), channel_id=1, source_target_pairs={{0,2},{1,3},{2,0},{3,1},{4,6},{5,7},{6,4},{7,5},{8,10},{9,11},{10,... | collective-permute-start | bytes 393224 | tf_op jit(solution)/shard_map/ppermute | solution.py:26
  5.3 9.6 %collective-permute-start.3 = (bf16[256,256]{1,0:T(8,128)(2,1)}, bf16[256,256]{1,0:T(8,128)(2,1)S(1)}, u32[]{:S(2)}, u32[]{:S(2)}) collective-permute-start(bf16[256,256]{1,0:T(8,128)(2,1)} %refs_0_.1), channel_id=1, source_target_pairs={{0,1},{1,0},{2,3},{3,2},{4,5},{5,4},{6,7},{7,6},{8,9},{9,8},{10,11... | collective-permute-start | bytes 393224 | tf_op jit(solution)/shard_map/ppermute | solution.py:26
  9.2 5.8 %collective-permute-start.6 = (bf16[256,256]{1,0:T(8,128)(2,1)S(1)}, bf16[256,256]{1,0:T(8,128)(2,1)S(1)}, u32[]{:S(2)}, u32[]{:S(2)}) collective-permute-start(bf16[256,256]{1,0:T(8,128)(2,1)S(1)} %collective-permute-done.2.refs_3_), channel_id=1, source_target_pairs={{0,1},{1,0},{2,3},{3,2},{4,5},{5,4},{6,7},{7,6},{8,9},{9,8},{10,11... | collective-permute-start | bytes 393224 | tf_op jit(solution)/shard_map/ppermute | solution.py:26
  11.8 3.2 %collective-permute-start.5 = (bf16[256,256]{1,0:T(8,128)(2,1)S(1)}, bf16[256,256]{1,0:T(8,128)(2,1)S(1)}, u32[]{:S(2)}, u32[]{:S(2)}) collective-permute-start(bf16[256,256]{1,0:T(8,128)(2,1)S(1)} %collective-permute-done.1.refs_2_), channel_id=1, source_target_pairs={{0,1},{1,0},{2,3},{3,2},{4,5},{5,4},{6,7},{7,6},{8,9},{9,8},{10,11... | collective-permute-start | bytes 393224 | tf_op jit(solution)/shard_map/ppermute | solution.py:26
  12.1 2.9 %collective-permute-start.4 = (bf16[256,256]{1,0:T(8,128)(2,1)S(1)}, bf16[256,256]{1,0:T(8,128)(2,1)S(1)}, u32[]{:S(2)}, u32[]{:S(2)}) collective-permute-start(bf16[256,256]{1,0:T(8,128)(2,1)S(1)} %collective-permute-done.refs_1_), channel_id=1, source_target_pairs={{0,1},{1,0},{2,3},{3,2},{4,5},{5,4},{6,7},{7,6},{8,9},{9,8},{10,11... | collective-permute-start | bytes 393224 | tf_op jit(solution)/shard_map/ppermute | solution.py:26
  12.3 2.7 %copy-start.3 = (f32[2048]{0:T(1024)S(1)}, f32[2048]{0:T(1024)}, u32[]{:S(2)}) copy-start(f32[2048]{0:T(1024)} %param.14) | copy-start | bytes 24580
  14.6 24.0 %collective-permute-start.18 = (bf16[320,2048]{1,0:T(8,128)(2,1)S(1)}, bf16[320,2048]{1,0:T(8,128)(2,1)S(1)}, u32[]{:S(2)}, u32[]{:S(2)}) collective-permute-start(bf16[320,2048]{1,0:T(8,128)(2,1)S(1)} %get-tuple-element.29.refs_6_.refs_5_), channel_id=1, source_target_pairs={{0,1},{1,0},{2,3},{3,2},{4,5},{5,4},{6,7},{7,6},{8,9},{9,8},{10,11... | collective-permute-start | bytes 3932168 | tf_op jit(solution)/shard_map/ppermute | solution.py:26
  15.0 13.2 %copy-start = (bf16[2048,128]{1,0:T(8,128)(2,1)S(1)}, bf16[2048,128]{1,0:T(8,128)(2,1)}, u32[]{:S(2)}) copy-start(bf16[2048,128]{1,0:T(8,128)(2,1)} %refs_3_.1) | copy-start | bytes 1572868
  15.0 13.2 %copy-start.4 = (bf16[3,128]{1,0:T(4,128)(2,1)S(1)}, bf16[3,128]{1,0:T(4,128)(2,1)}, u32[]{:S(2)}) copy-start(bf16[3,128]{1,0:T(4,128)(2,1)} %refs_7_.1) | copy-start | bytes 2308
  16.2 7.2 %collective-permute-start.22 = (bf16[144,128]{1,0:T(8,128)(2,1)S(1)}, bf16[144,128]{1,0:T(8,128)(2,1)S(1)}, u32[]{:S(2)}, u32[]{:S(2)}) collective-permute-start(bf16[144,128]{1,0:T(8,128)(2,1)S(1)} %get-tuple-element.47.refs_0_), channel_id=1, source_target_pairs={{0,6},{1,7},{2,4},{3,5},{4,2},{5,3},{6,0},{7,1},{8,14},{9,15},{10,... | collective-permute-start | bytes 110600 | tf_op jit(solution)/shard_map/ppermute | solution.py:26
  17.7 6.0 %collective-permute-start.21 = (bf16[144,128]{1,0:T(8,128)(2,1)S(1)}, bf16[144,128]{1,0:T(8,128)(2,1)S(1)}, u32[]{:S(2)}, u32[]{:S(2)}) collective-permute-start(bf16[144,128]{1,0:T(8,128)(2,1)S(1)} %get-tuple-element.47.refs_0_), channel_id=1, source_target_pairs={{0,4},{1,5},{2,6},{3,7},{4,0},{5,1},{6,2},{7,3},{8,12},{9,13},{10,... | collective-permute-start | bytes 110600 | tf_op jit(solution)/shard_map/ppermute | solution.py:26
  19.2 6.1 %collective-permute-start.20 = (bf16[144,128]{1,0:T(8,128)(2,1)S(1)}, bf16[144,128]{1,0:T(8,128)(2,1)S(1)}, u32[]{:S(2)}, u32[]{:S(2)}) collective-permute-start(bf16[144,128]{1,0:T(8,128)(2,1)S(1)} %get-tuple-element.47.refs_0_), channel_id=1, source_target_pairs={{0,2},{1,3},{2,0},{3,1},{4,6},{5,7},{6,4},{7,5},{8,10},{9,11},{10,... | collective-permute-start | bytes 110600 | tf_op jit(solution)/shard_map/ppermute | solution.py:26
  19.7 6.2 %collective-permute-start.10 = (bf16[152,128]{1,0:T(8,128)(2,1)S(1)}, bf16[152,128]{1,0:T(8,128)(2,1)S(1)}, u32[]{:S(2)}, u32[]{:S(2)}) collective-permute-start(bf16[152,128]{1,0:T(8,128)(2,1)S(1)} %get-tuple-element.28.refs_8_), channel_id=1, source_target_pairs={{0,24},{8,16},{16,8},{24,0},{1,25},{9,17},{17,9},{25,1},{2,26},{10... | collective-permute-start | bytes 116744 | tf_op jit(solution)/shard_map/ppermute | solution.py:26
  23.3 4.9 %collective-permute-start.9 = (bf16[152,128]{1,0:T(8,128)(2,1)S(1)}, bf16[152,128]{1,0:T(8,128)(2,1)S(1)}, u32[]{:S(2)}, u32[]{:S(2)}) collective-permute-start(bf16[152,128]{1,0:T(8,128)(2,1)S(1)} %get-tuple-element.28.refs_8_), channel_id=1, source_target_pairs={{0,16},{8,24},{16,0},{24,8},{1,17},{9,25},{17,1},{25,9},{2,18},{10... | collective-permute-start | bytes 116744 | tf_op jit(solution)/shard_map/ppermute | solution.py:26
  23.7 4.5 %collective-permute-start.8 = (bf16[152,128]{1,0:T(8,128)(2,1)S(1)}, bf16[152,128]{1,0:T(8,128)(2,1)S(1)}, u32[]{:S(2)}, u32[]{:S(2)}) collective-permute-start(bf16[152,128]{1,0:T(8,128)(2,1)S(1)} %get-tuple-element.28.refs_8_), channel_id=1, source_target_pairs={{0,8},{8,0},{16,24},{24,16},{1,9},{9,1},{17,25},{25,17},{2,10},{10... | collective-permute-start | bytes 116744 | tf_op jit(solution)/shard_map/ppermute | solution.py:26
  25.3 13.2 %collective-permute-start.23 = (bf16[4,144,128]{2,1,0:T(8,128)(2,1)S(1)}, bf16[4,144,128]{2,1,0:T(8,128)(2,1)S(1)}, u32[]{:S(2)}, u32[]{:S(2)}) collective-permute-start(bf16[4,144,128]{2,1,0:T(8,128)(2,1)S(1)} %pad_maximum_fusion), channel_id=1, source_target_pairs={{0,1},{1,0},{2,3},{3,2},{4,5},{5,4},{6,7},{7,6},{8,9},{9,8},{10,11... | collective-permute-start | bytes 442376 | tf_op jit(solution)/shard_map/ppermute | solution.py:26
  28.2 10.4 %copy-start.2 = (f32[512]{0:T(512)S(1)}, f32[512]{0:T(512)}, u32[]{:S(2)}) copy-start(f32[512]{0:T(512)} %param.18) | copy-start | bytes 6148
  29.1 3.2 %collective-permute-start.19 = (bf16[128,384]{1,0:T(8,128)(2,1)S(1)}, bf16[128,384]{1,0:T(8,128)(2,1)S(1)}, u32[]{:S(2)}, u32[]{:S(2)}) collective-permute-start(bf16[128,384]{1,0:T(8,128)(2,1)S(1)} %get-tuple-element.35), channel_id=1, source_target_pairs={{0,1},{1,0},{2,3},{3,2},{4,5},{5,4},{6,7},{7,6},{8,9},{9,8},{10,11... | collective-permute-start | bytes 294920 | tf_op jit(solution)/shard_map/ppermute | solution.py:26
  29.3 6.9 %collective-permute-start.16 = (bf16[3,144,128]{2,1,0:T(8,128)(2,1)S(1)}, bf16[3,144,128]{2,1,0:T(8,128)(2,1)S(1)}, u32[]{:S(2)}, u32[]{:S(2)}) collective-permute-start(bf16[3,144,128]{2,1,0:T(8,128)(2,1)S(1)} %pad_maximum_fusion.1.refs_0_), channel_id=1, source_target_pairs={{0,6},{1,7},{2,4},{3,5},{4,2},{5,3},{6,0},{7,1},{8,14},{9,15},{10,... | collective-permute-start | bytes 331784 | tf_op jit(solution)/shard_map/ppermute | solution.py:26
  31.0 7.0 %collective-permute-start.14 = (bf16[3,144,128]{2,1,0:T(8,128)(2,1)S(1)}, bf16[3,144,128]{2,1,0:T(8,128)(2,1)S(1)}, u32[]{:S(2)}, u32[]{:S(2)}) collective-permute-start(bf16[3,144,128]{2,1,0:T(8,128)(2,1)S(1)} %pad_maximum_fusion.1.refs_0_), channel_id=1, source_target_pairs={{0,4},{1,5},{2,6},{3,7},{4,0},{5,1},{6,2},{7,3},{8,12},{9,13},{10,... | collective-permute-start | bytes 331784 | tf_op jit(solution)/shard_map/ppermute | solution.py:26
  32.3 5.8 %collective-permute-start.12 = (bf16[3,144,128]{2,1,0:T(8,128)(2,1)S(1)}, bf16[3,144,128]{2,1,0:T(8,128)(2,1)S(1)}, u32[]{:S(2)}, u32[]{:S(2)}) collective-permute-start(bf16[3,144,128]{2,1,0:T(8,128)(2,1)S(1)} %pad_maximum_fusion.1.refs_0_), channel_id=1, source_target_pairs={{0,2},{1,3},{2,0},{3,1},{4,6},{5,7},{6,4},{7,5},{8,10},{9,11},{10,... | collective-permute-start | bytes 331784 | tf_op jit(solution)/shard_map/ppermute | solution.py:26
  36.2 4.3 %collective-permute-start.11 = (bf16[3,144,128]{2,1,0:T(8,128)(2,1)S(1)}, bf16[3,144,128]{2,1,0:T(8,128)(2,1)S(1)}, u32[]{:S(2)}, u32[]{:S(2)}) collective-permute-start(bf16[3,144,128]{2,1,0:T(8,128)(2,1)S(1)} %pad_maximum_fusion.1.refs_0_), channel_id=1, source_target_pairs={{0,1},{1,0},{2,3},{3,2},{4,5},{5,4},{6,7},{7,6},{8,9},{9,8},{10,11... | collective-permute-start | bytes 331784 | tf_op jit(solution)/shard_map/ppermute | solution.py:26
  38.1 2.4 %collective-permute-start.17 = (bf16[3,144,128]{2,1,0:T(8,128)(2,1)S(1)}, bf16[3,144,128]{2,1,0:T(8,128)(2,1)S(1)}, u32[]{:S(2)}, u32[]{:S(2)}) collective-permute-start(bf16[3,144,128]{2,1,0:T(8,128)(2,1)S(1)} %collective-permute-done.16.refs_3_), channel_id=1, source_target_pairs={{0,1},{1,0},{2,3},{3,2},{4,5},{5,4},{6,7},{7,6},{8,9},{9,8},{10,11... | collective-permute-start | bytes 331784 | tf_op jit(solution)/shard_map/ppermute | solution.py:26
  38.1 2.4 %collective-permute-start.15 = (bf16[3,144,128]{2,1,0:T(8,128)(2,1)S(1)}, bf16[3,144,128]{2,1,0:T(8,128)(2,1)S(1)}, u32[]{:S(2)}, u32[]{:S(2)}) collective-permute-start(bf16[3,144,128]{2,1,0:T(8,128)(2,1)S(1)} %collective-permute-done.14.refs_2_), channel_id=1, source_target_pairs={{0,1},{1,0},{2,3},{3,2},{4,5},{5,4},{6,7},{7,6},{8,9},{9,8},{10,11... | collective-permute-start | bytes 331784 | tf_op jit(solution)/shard_map/ppermute | solution.py:26
  38.6 1.9 %collective-permute-start.13 = (bf16[3,144,128]{2,1,0:T(8,128)(2,1)S(1)}, bf16[3,144,128]{2,1,0:T(8,128)(2,1)S(1)}, u32[]{:S(2)}, u32[]{:S(2)}) collective-permute-start(bf16[3,144,128]{2,1,0:T(8,128)(2,1)S(1)} %collective-permute-done.12.refs_1_), channel_id=1, source_target_pairs={{0,1},{1,0},{2,3},{3,2},{4,5},{5,4},{6,7},{7,6},{8,9},{9,8},{10,11... | collective-permute-start | bytes 331784 | tf_op jit(solution)/shard_map/ppermute | solution.py:26
  42.0 7.4 %collective-permute-start.24 = (bf16[32,2048]{1,0:T(8,128)(2,1)S(1)}, bf16[32,2048]{1,0:T(8,128)(2,1)S(1)}, u32[]{:S(2)}, u32[]{:S(2)}) collective-permute-start(bf16[32,2048]{1,0:T(8,128)(2,1)S(1)} %get-tuple-element.41), channel_id=1, source_target_pairs={{0,6},{1,7},{2,4},{3,5},{4,2},{5,3},{6,0},{7,1},{8,14},{9,15},{10,... | collective-permute-start | bytes 393224 | tf_op jit(solution)/shard_map/ppermute | solution.py:26
  43.8 7.9 %collective-permute-start.25 = (bf16[32,2048]{1,0:T(8,128)(2,1)S(1)}, bf16[32,2048]{1,0:T(8,128)(2,1)S(1)}, u32[]{:S(2)}, u32[]{:S(2)}) collective-permute-start(bf16[32,2048]{1,0:T(8,128)(2,1)S(1)} %get-tuple-element.42), channel_id=1, source_target_pairs={{0,4},{1,5},{2,6},{3,7},{4,0},{5,1},{6,2},{7,3},{8,12},{9,13},{10,... | collective-permute-start | bytes 393224 | tf_op jit(solution)/shard_map/ppermute | solution.py:26
  45.0 6.7 %collective-permute-start.26 = (bf16[32,2048]{1,0:T(8,128)(2,1)S(1)}, bf16[32,2048]{1,0:T(8,128)(2,1)S(1)}, u32[]{:S(2)}, u32[]{:S(2)}) collective-permute-start(bf16[32,2048]{1,0:T(8,128)(2,1)S(1)} %get-tuple-element.43), channel_id=1, source_target_pairs={{0,2},{1,3},{2,0},{3,1},{4,6},{5,7},{6,4},{7,5},{8,10},{9,11},{10,... | collective-permute-start | bytes 393224 | tf_op jit(solution)/shard_map/ppermute | solution.py:26
  45.6 1.2 %collective-permute-start.27 = (f32[1,128]{1,0:T(1,128)S(1)}, f32[1,128]{1,0:T(1,128)S(1)}, u32[]{:S(2)}, u32[]{:S(2)}) collective-permute-start(f32[1,128]{1,0:T(1,128)S(1)} %get-tuple-element.45), channel_id=1, source_target_pairs={{0,1},{1,0},{2,3},{3,2},{4,5},{5,4},{6,7},{7,6},{8,9},{9,8},{10,11... | collective-permute-start | bytes 1544 | tf_op jit(solution)/shard_map/ppermute | solution.py:26
  (1 other events, 2.7 us)

commit v4 on v3

--- a/solution.py
+++ b/solution.py
@@ -134,28 +134,54 @@
     return lax.dot_general(left, right, (((1,), (1,)), ((), ())), preferred_element_type=F32)
 
 
-def project_first(pairs, *refs):
-    pieces, refs = refs[: 2 * pairs], refs[2 * pairs :]
-    gain_ref, key_w_ref, mix_w_ref, cos_ref, sin_ref = refs[:5]
-    scaled_ref, inv_ref, message_ref, mix_ref, key_ref = refs[5:]
-    rank = lax.axis_index("tp")
+def weights_for(ref, owners, width, axis):
+    spans = [pl.ds(pl.multiple_of(owner * width, width), width) for owner in owners]
+    return jnp.concatenate([ref[:, span] if axis else ref[span, :] for span in spans], axis=axis)
+
+
+def owners_of(core, pairs):
+    return [lax.axis_index("tp") ^ (2 * i + core) for i in range(pairs)]
+
+
+def project(core, pieces, gain_ref, key_w_ref, mix_w_ref, scaled_ref):
+    owners = owners_of(core, len(pieces))
     tokens, width = pieces[0].shape
-    half = tokens // 2
     total = jnp.zeros((tokens, LANES), F32)
-    for i, ref in enumerate(pieces):
-        owner = rank ^ (2 * (i % pairs) + i // pairs)
+    for i, (owner, ref) in enumerate(zip(owners, pieces)):
         piece = ref[...].astype(F32)
         squares = piece * piece
         for j in range(width // LANES):
             total = total + squares[:, j * LANES : (j + 1) * LANES]
-        columns = pl.ds(pl.multiple_of(owner * width, width), width)
-        scaled_ref[:, columns] = (piece * gain_ref[:, columns]).astype(BF16)
+        gain = gain_ref[:, pl.ds(pl.multiple_of(owner * width, width), width)]
+        scaled_ref[:, i * width : (i + 1) * width] = (piece * gain).astype(BF16)
+    scaled = scaled_ref[...]
+    keys = dot_nt(scaled, weights_for(key_w_ref, owners, width, 1))
+    mixes = jnp.dot(scaled, weights_for(mix_w_ref, owners, width, 0), preferred_element_type=F32)
+    return total, keys, mixes
+
+
+def project_even(pairs, *refs):
+    pieces, (gain_ref, key_w_ref, mix_w_ref, scaled_ref, total_ref, keys_ref, mixes_ref) = refs[:pairs], refs[pairs:]
+    total, keys, mixes = project(0, pieces, gain_ref, key_w_ref, mix_w_ref, scaled_ref)
+    total_ref[...] = total
+    keys_ref[...] = keys
+    mixes_ref[...] = mixes
+
+
+def project_first(pairs, *refs):
+    pieces, refs = refs[:pairs], refs[pairs:]
+    gain_ref, key_w_ref, mix_w_ref, cos_ref, sin_ref, total_ref, keys_ref, mixes_ref = refs[:8]
+    scaled_ref, inv_ref, message_ref, mix_ref, key_ref = refs[8:]
+    total, keys, mixes = project(1, pieces, gain_ref, key_w_ref, mix_w_ref, scaled_ref)
+    rank = lax.axis_index("tp")
+    tokens, width = pieces[0].shape
+    half = tokens // 2
     features = 2 * pairs * width
-    inv = lax.rsqrt(jnp.sum(total, axis=1, keepdims=True) / features + EPSILON)
+    total = jnp.sum(total + total_ref[...], axis=1, keepdims=True)
+    inv = lax.rsqrt(total / features + EPSILON)
     inv_ref[...] = jnp.broadcast_to(inv, inv_ref.shape)
-    scaled = scaled_ref[...]
-    keys = dot_nt(scaled, key_w_ref[...]) * inv
-    mixes = jnp.dot(scaled, mix_w_ref[...], preferred_element_type=F32) * inv
+    keys = (keys + keys_ref[...]) * inv
+    mixes = (mixes + mixes_ref[...]) * inv
     mix = (mixes[:, :LANES] * mixes[:, LANES:]).astype(BF16)
     mix_ref[...] = mix
     key_ref[...] = keys
@@ -176,16 +202,19 @@
 
 
 def project_second(natural, *refs):
-    scaled_ref, inv_ref, query_w_ref, gate_w_ref, cos_ref, sin_ref, mix_ref, taps_ref = refs[:8]
-    halos, (keep_ref, send_ref, both_ref) = refs[8:-3], refs[-3:]
-    scaled = scaled_ref[...]
+    even_ref, odd_ref, inv_ref, query_w_ref, gate_w_ref, cos_ref, sin_ref, mix_ref, taps_ref = refs[:9]
+    halos, (keep_ref, send_ref, both_ref) = refs[9:-3], refs[-3:]
+    pairs = lax.axis_size("tp") // 2
+    width = even_ref.shape[1] // pairs
+    owners = owners_of(0, pairs) + owners_of(1, pairs)
+    scaled = jnp.concatenate([even_ref[...], odd_ref[...]], axis=1)
     inv = inv_ref[...]
     scale = (NOPE + ROPE) ** (-0.5)
-    query = dot_nt(scaled, query_w_ref[...])
+    query = dot_nt(scaled, weights_for(query_w_ref, owners, width, 1))
     both_ref[:, :NOPE] = query[:, :NOPE] * inv * scale
     both_ref[:, NOPE : NOPE + LANES] = rotate(query[:, NOPE:] * inv, cos_ref[...], sin_ref[...]) * scale
 
-    gate = jnp.dot(scaled, gate_w_ref[...], preferred_element_type=F32) * inv
+    gate = jnp.dot(scaled, weights_for(gate_w_ref, owners, width, 0), preferred_element_type=F32) * inv
     mix = mix_ref[...].astype(F32)
     tokens = mix.shape[0]
     place, places = lax.axis_index("sp"), lax.axis_size("sp")
@@ -415,19 +444,28 @@
     )
     other_w = swap(own_w, "tp", 1)
 
-    scaled, inv, message, mix = kernel_call(
+    gain = norm_gain.reshape(1, -1)
+    part = features // 2
+    scaled_even, *partial = kernel_call(
+        functools.partial(project_even, pairs),
+        [((tokens, part), BF16), ((tokens, LANES), F32), ((tokens, 2 * LANES), F32), ((tokens, 2 * LANES), F32)],
+        12 << 20,
+        flops=2 * tokens * part * 4 * LANES,
+        nbytes=4 * tokens * part,
+    )(*even, gain, key_w, mix_w)
+    scaled_odd, inv, message, mix = kernel_call(
         functools.partial(project_first, pairs),
         [
-            ((tokens, features), BF16),
+            ((tokens, part), BF16),
             ((tokens, LANES), F32),
             ((half + share + HALO, LANES), BF16),
             ((tokens, channels), BF16),
         ],
         12 << 20,
         scratch=[pltpu.VMEM((tokens, 2 * LANES), F32)],
-        flops=2 * tokens * features * 4 * LANES,
-        nbytes=4 * tokens * features,
-    )(*even, *odd, norm_gain.reshape(1, -1), key_w, mix_w, cosines, sines)
+        flops=2 * tokens * part * 4 * LANES,
+        nbytes=4 * tokens * part,
+    )(*odd, gain, key_w, mix_w, cosines, sines, *partial)
 
     small = places <= 8 and places & (places - 1) == 0
     if small:
@@ -451,7 +489,7 @@
         scratch=[pltpu.VMEM((tokens, columns), F32)],
         flops=2 * tokens * features * 3 * LANES,
         nbytes=4 * tokens * features,
-    )(scaled, inv, query_w, gate_weight, cosines, sines, mix, conv_kernel, *halos)
+    )(scaled_even, scaled_odd, inv, query_w, gate_weight, cosines, sines, mix, conv_kernel, *halos)
     got = swap(send, "tp", 1)
 
     def attend_to(arrays, slots, stage, outs, *state):
@@ -471,13 +509,14 @@
         )(*arrays, latent_gain.reshape(1, -1), own_w, other_w, keep, got, *state)
 
     state_outs = [((8, tokens), F32), ((VDIM, tokens), F32)]
-    state = []
+    first_slots, last_slots, first_in, last_in = slots, slots, arounds, others
     if small:
-        near_slots = [[(i, None), (pairs, i)] for i in range(pairs)]
-        state = attend_to([*nears, near_other], near_slots, 0, state_outs)
-    state = attend_to(arounds, slots, 1 if small else 0, state_outs, *state)
+        first_slots = [[(pairs + i, None)] + chip_slots for i, chip_slots in enumerate(slots)]
+        last_slots = [[(pairs, i)] + chip_slots for i, chip_slots in enumerate(slots)]
+        first_in, last_in = arounds + nears, others + [near_other]
+    state = attend_to(first_in, first_slots, 0, state_outs)
     final_outs = [((rows, features), F32)] + [((rows, features), BF16)] * (pairs - 1) + [((1, half), F32)] * 2
-    *outs, own_log, send_log = attend_to(others, slots, 2, final_outs, *state)
+    *outs, own_log, send_log = attend_to(last_in, last_slots, 2, final_outs, *state)
     arrived = exchange_blocks(outs)
     got_log = swap(send_log, "tp", 1)
     (logs,) = kernel_call(join_logs, [((1, tokens), F32)], 1 << 20, flops=1 << 22, nbytes=1 << 12)(own_log, got_log)

time: 52.5 us -> 47.8 us (0.910)
  waiting for transfers between devices: 20.2 us -> 16.2 us
  Pallas kernels: 8.22 us -> 7.64 us
    ppermute x28, waiting for transfers between devices: 20.2 us -> 16.2 us  [swap(): return lax.ppermute(array, axis, [(i, i ^ mask) for i in range(peers)])]
    pallas_call x7, Pallas kernels: 8.22 us -> 7.64 us  [call(): pl.pallas_call(body, out_shape=[jax.ShapeDtypeStruct(shape, dtype) for sh...]
where the time goes in v4:
time: 47.8 us; the launch traced here: 47.7 us
  starting transfers between devices  22.2 us (46%)
  waiting for transfers between devices  16.2 us (34%)
  Pallas kernels  7.64 us (16%)
  between operations  0.82 us (2%)
  other arithmetic  0.75 us (2%)
    ppermute x28, starting transfers between devices, swap(): return lax.ppermute(array, axis, [(i, i ^ mask) for i in range(peers)])  22.2 us
    ppermute x28, waiting for transfers between devices, swap(): return lax.ppermute(array, axis, [(i, i ^ mask) for i in range(peers)])  16.2 us
    pallas_call x7, Pallas kernels, call(): pl.pallas_call(body, out_shape=[jax.ShapeDtypeStruct(shape, dtype) for sh...  7.64 us
  transfers between devices with their start and end apart: 28, of which 11 were waited for; matrix products, arithmetic and copies ran while one was open for 0% of the time, Pallas kernels for 13%

profile of v4, /device:TPU:0, one launch (start us, length us, event | category | flops | bytes accessed | tf_op | source)
XLA Modules:
  0.0 47.7 jit_solution(15167698194031008546)
XLA Ops:
  0.6 0.6 %collective-permute-start.7 = (bf16[64,2048]{1,0:T(8,128)(2,1)}, bf16[64,2048]{1,0:T(8,128)(2,1)S(1)}, u32[]{:S(2)}, u32[]{:S(2)}) collective-permute-start(bf16[64,2048]{1,0:T(8,128)(2,1)} %bitcast.24), channel_id=1, source_target_pairs={{0,1},{1,0},{2,3},{3,2},{4,5},{5,4},{6,7},{7,6},{8,9},{9,8},{10,11... | collective-permute-start | bytes 786440 | tf_op jit(solution)/shard_map/ppermute | solution.py:26
  1.2 2.6 %collective-permute-start.3 = (bf16[256,256]{1,0:T(8,128)(2,1)}, bf16[256,256]{1,0:T(8,128)(2,1)S(1)}, u32[]{:S(2)}, u32[]{:S(2)}) collective-permute-start(bf16[256,256]{1,0:T(8,128)(2,1)} %refs_0_.1), channel_id=1, source_target_pairs={{0,4},{1,5},{2,6},{3,7},{4,0},{5,1},{6,2},{7,3},{8,12},{9,13},{10,... | collective-permute-start | bytes 393224 | tf_op jit(solution)/shard_map/ppermute | solution.py:26
  3.8 1.5 %collective-permute-start.1 = (bf16[256,256]{1,0:T(8,128)(2,1)}, bf16[256,256]{1,0:T(8,128)(2,1)S(1)}, u32[]{:S(2)}, u32[]{:S(2)}) collective-permute-start(bf16[256,256]{1,0:T(8,128)(2,1)} %refs_0_.1), channel_id=1, source_target_pairs={{0,2},{1,3},{2,0},{3,1},{4,6},{5,7},{6,4},{7,5},{8,10},{9,11},{10,... | collective-permute-start | bytes 393224 | tf_op jit(solution)/shard_map/ppermute | solution.py:26
  5.3 2.8 %collective-permute-done.3.refs_2_ = bf16[256,256]{1,0:T(8,128)(2,1)S(1)} collective-permute-done((bf16[256,256]{1,0:T(8,128)(2,1)}, bf16[256,256]{1,0:T(8,128)(2,1)S(1)}, u32[]{:S(2)}, u32[]{:S(2)}) %collective-permute-start.3) | collective-permute-done | bytes 131104 | tf_op jit(solution)/shard_map/ppermute | solution.py:26
  8.1 2.3 %collective-permute-done.1.refs_1_ = bf16[256,256]{1,0:T(8,128)(2,1)S(1)} collective-permute-done((bf16[256,256]{1,0:T(8,128)(2,1)}, bf16[256,256]{1,0:T(8,128)(2,1)S(1)}, u32[]{:S(2)}, u32[]{:S(2)}) %collective-permute-start.1) | collective-permute-done | bytes 131104 | tf_op jit(solution)/shard_map/ppermute | solution.py:26
  10.4 1.7 %collective-permute-done.5.refs_3_ = bf16[256,256]{1,0:T(8,128)(2,1)S(1)} collective-permute-done((bf16[256,256]{1,0:T(8,128)(2,1)}, bf16[256,256]{1,0:T(8,128)(2,1)S(1)}, u32[]{:S(2)}, u32[]{:S(2)}) %collective-permute-start.5) | collective-permute-done | bytes 131104 | tf_op jit(solution)/shard_map/ppermute | solution.py:26
  12.1 2.3 %shard_map.140 = (bf16[256,2048]{1,0:T(8,128)(2,1)S(1)}, bf16[256,2048]{1,0:T(8,128)(2,1)S(1)}, bf16[2048,256]{1,0:T(8,128)(2,1)S(1)}, bf16[320,2048]{1,0:T(8,12...) custom-call(bf16[64,2048]{1,0:T(8,128)(2,1)} %bitcast.25, bf16[64,2048]{1,0:T(8,128)(2,1)} %bitcast.26, ...), custom_call_target="tpu_custom_call" | custom-call | flops 268435456 | bytes 8388608 | tf_op jit(solution)/shard_map/pallas_call | solution.py:59
  14.4 0.5 %collective-permute-start.22 = (bf16[320,2048]{1,0:T(8,128)(2,1)S(1)}, bf16[320,2048]{1,0:T(8,128)(2,1)S(1)}, u32[]{:S(2)}, u32[]{:S(2)}) collective-permute-start(bf16[320,2048]{1,0:T(8,128)(2,1)S(1)} %get-tuple-element.34.refs_9_.refs_6_), channel_id=1, source_target_pairs={{0,1},{1,0},{2,3},{3,2},{4,5},{5,4},{6,7},{7,6},{8,9},{9,8},{10,11... | collective-permute-start | bytes 3932168 | tf_op jit(solution)/shard_map/ppermute | solution.py:26
  15.5 0.6 %shard_map.142 = (bf16[256,1024]{1,0:T(8,128)(2,1)S(1)}, f32[256,128]{1,0:T(8,128)S(1)}, bf16[152,128]{1,0:T(8,128)(2,1)S(1)}, bf16[256,128]{1,0:T(8,128)(2,1)S(1)}) custom-call(bf16[256,256]{1,0:T(8,128)(2,1)S(1)} %collective-permute-done.refs_0_, bf16[256,256]{1,0:T(8,128)(2,1)S(1)} %collective-permute-done.2.refs_1_, ...), custom_call_target="tpu_custom_call" | custom-call | flops 268435456 | bytes 1048576 | tf_op jit(solution)/shard_map/pallas_call | solution.py:59
  16.1 3.9 %collective-permute-start.10 = (bf16[152,128]{1,0:T(8,128)(2,1)S(1)}, bf16[152,128]{1,0:T(8,128)(2,1)S(1)}, u32[]{:S(2)}, u32[]{:S(2)}) collective-permute-start(bf16[152,128]{1,0:T(8,128)(2,1)S(1)} %get-tuple-element.33.refs_9_), channel_id=1, source_target_pairs={{0,24},{8,16},{16,8},{24,0},{1,25},{9,17},{17,9},{25,1},{2,26},{10... | collective-permute-start | bytes 116744 | tf_op jit(solution)/shard_map/ppermute | solution.py:26
  20.0 0.6 %collective-permute-start.8 = (bf16[152,128]{1,0:T(8,128)(2,1)S(1)}, bf16[152,128]{1,0:T(8,128)(2,1)S(1)}, u32[]{:S(2)}, u32[]{:S(2)}) collective-permute-start(bf16[152,128]{1,0:T(8,128)(2,1)S(1)} %get-tuple-element.33.refs_9_), channel_id=1, source_target_pairs={{0,8},{8,0},{16,24},{24,16},{1,9},{9,1},{17,25},{25,17},{2,10},{10... | collective-permute-start | bytes 116744 | tf_op jit(solution)/shard_map/ppermute | solution.py:26
  20.6 2.6 %collective-permute-start.20 = (bf16[144,128]{1,0:T(8,128)(2,1)S(1)}, bf16[144,128]{1,0:T(8,128)(2,1)S(1)}, u32[]{:S(2)}, u32[]{:S(2)}) collective-permute-start(bf16[144,128]{1,0:T(8,128)(2,1)S(1)} %get-tuple-element.51.refs_4_), channel_id=1, source_target_pairs={{0,6},{1,7},{2,4},{3,5},{4,2},{5,3},{6,0},{7,1},{8,14},{9,15},{10,... | collective-permute-start | bytes 110600 | tf_op jit(solution)/shard_map/ppermute | solution.py:26
  23.2 0.5 %collective-permute-start.19 = (bf16[144,128]{1,0:T(8,128)(2,1)S(1)}, bf16[144,128]{1,0:T(8,128)(2,1)S(1)}, u32[]{:S(2)}, u32[]{:S(2)}) collective-permute-start(bf16[144,128]{1,0:T(8,128)(2,1)S(1)} %get-tuple-element.51.refs_4_), channel_id=1, source_target_pairs={{0,4},{1,5},{2,6},{3,7},{4,0},{5,1},{6,2},{7,3},{8,12},{9,13},{10,... | collective-permute-start | bytes 110600 | tf_op jit(solution)/shard_map/ppermute | solution.py:26
  23.7 1.1 %collective-permute-done.9.refs_11_ = bf16[152,128]{1,0:T(8,128)(2,1)S(1)} collective-permute-done((bf16[152,128]{1,0:T(8,128)(2,1)S(1)}, bf16[152,128]{1,0:T(8,128)(2,1)S(1)}, u32[]{:S(2)}, u32[]{:S(2)}) %collective-permute-start.9) | collective-permute-done | bytes 38944 | tf_op jit(solution)/shard_map/ppermute | solution.py:26
  24.8 1.5 %collective-permute-start.18 = (bf16[144,128]{1,0:T(8,128)(2,1)S(1)}, bf16[144,128]{1,0:T(8,128)(2,1)S(1)}, u32[]{:S(2)}, u32[]{:S(2)}) collective-permute-start(bf16[144,128]{1,0:T(8,128)(2,1)S(1)} %get-tuple-element.51.refs_4_), channel_id=1, source_target_pairs={{0,2},{1,3},{2,0},{3,1},{4,6},{5,7},{6,4},{7,5},{8,10},{9,11},{10,... | collective-permute-start | bytes 110600 | tf_op jit(solution)/shard_map/ppermute | solution.py:26
  26.4 1.6 %collective-permute-start.16 = (bf16[3,144,128]{2,1,0:T(8,128)(2,1)S(1)}, bf16[3,144,128]{2,1,0:T(8,128)(2,1)S(1)}, u32[]{:S(2)}, u32[]{:S(2)}) collective-permute-start(bf16[3,144,128]{2,1,0:T(8,128)(2,1)S(1)} %pad_maximum_fusion.1.refs_0_), channel_id=1, source_target_pairs={{0,6},{1,7},{2,4},{3,5},{4,2},{5,3},{6,0},{7,1},{8,14},{9,15},{10,... | collective-permute-start | bytes 331784 | tf_op jit(solution)/shard_map/ppermute | solution.py:26
  27.9 0.9 %shard_map.143 = (bf16[128,384]{1,0:T(8,128)(2,1)S(1)}, bf16[128,384]{1,0:T(8,128)(2,1)S(1)}) custom-call(bf16[256,1024]{1,0:T(8,128)(2,1)S(1)} %get-tuple-element.35.refs_0_, bf16[256,1024]{1,0:T(8,128)(2,1)S(1)} %get-tuple-element.36.refs_1_, f32[256,128]{1,0:T(8,128)S(1)} %get-tuple-element.37.refs_2_, bf16[256,2048]{1,0:T(8,128)(2,1)S(1)} %get-tuple-element.38.refs_3_, ...), custom_call_target="tpu_custom_call" | custom-call | flops 402653184 | bytes 2097152 | tf_op jit(solution)/shard_map/pallas_call | solution.py:59
  28.9 0.6 %collective-permute-start.14 = (bf16[3,144,128]{2,1,0:T(8,128)(2,1)S(1)}, bf16[3,144,128]{2,1,0:T(8,128)(2,1)S(1)}, u32[]{:S(2)}, u32[]{:S(2)}) collective-permute-start(bf16[3,144,128]{2,1,0:T(8,128)(2,1)S(1)} %pad_maximum_fusion.1.refs_0_), channel_id=1, source_target_pairs={{0,4},{1,5},{2,6},{3,7},{4,0},{5,1},{6,2},{7,3},{8,12},{9,13},{10,... | collective-permute-start | bytes 331784 | tf_op jit(solution)/shard_map/ppermute | solution.py:26
  29.4 1.5 %collective-permute-start.12 = (bf16[3,144,128]{2,1,0:T(8,128)(2,1)S(1)}, bf16[3,144,128]{2,1,0:T(8,128)(2,1)S(1)}, u32[]{:S(2)}, u32[]{:S(2)}) collective-permute-start(bf16[3,144,128]{2,1,0:T(8,128)(2,1)S(1)} %pad_maximum_fusion.1.refs_0_), channel_id=1, source_target_pairs={{0,2},{1,3},{2,0},{3,1},{4,6},{5,7},{6,4},{7,5},{8,10},{9,11},{10,... | collective-permute-start | bytes 331784 | tf_op jit(solution)/shard_map/ppermute | solution.py:26
  31.0 1.3 %collective-permute-done.23.refs_12_.refs_9_ = bf16[128,384]{1,0:T(8,128)(2,1)S(1)} collective-permute-done((bf16[128,384]{1,0:T(8,128)(2,1)S(1)}, bf16[128,384]{1,0:T(8,128)(2,1)S(1)}, u32[]{:S(2)}, u32[]{:S(2)}) %collective-permute-start.23) | collective-permute-done | bytes 98336 | tf_op jit(solution)/shard_map/ppermute | solution.py:26
  32.4 0.6 %collective-permute-done.16.refs_3_ = bf16[3,144,128]{2,1,0:T(8,128)(2,1)S(1)} collective-permute-done((bf16[3,144,128]{2,1,0:T(8,128)(2,1)S(1)}, bf16[3,144,128]{2,1,0:T(8,128)(2,1)S(1)}, u32[]{:S(2)}, u32[]{:S(2)}) %collective-permute-start.16) | collective-permute-done | bytes 110624 | tf_op jit(solution)/shard_map/ppermute | solution.py:26
  33.0 0.9 %collective-permute-done.14.refs_2_ = bf16[3,144,128]{2,1,0:T(8,128)(2,1)S(1)} collective-permute-done((bf16[3,144,128]{2,1,0:T(8,128)(2,1)S(1)}, bf16[3,144,128]{2,1,0:T(8,128)(2,1)S(1)}, u32[]{:S(2)}, u32[]{:S(2)}) %collective-permute-start.14) | collective-permute-done | bytes 110624 | tf_op jit(solution)/shard_map/ppermute | solution.py:26
  34.7 1.1 %shard_map.144 = (f32[8,256]{1,0:T(8,128)S(1)}, f32[128,256]{1,0:T(8,128)S(1)}) custom-call(bf16[3,144,128]{2,1,0:T(8,128)(2,1)S(1)} %pad_maximum_fusion.1.refs_0_, bf16[3,144,128]{2,1,0:T(8,128)(2,1)S(1)} %collective-permute-done.12.refs_1_, bf16[3,144,128]{2,1,0:T(8,128)(2,1)S(1)} %collective-permute-done.14.refs_2_, ...), custom_call_target="tpu_custom_call" | custom-call | flops 536870912 | bytes 4194304 | tf_op jit(solution)/shard_map/pallas_call | solution.py:59
  35.9 1.6 %shard_map.145 = (f32[32,2048]{1,0:T(8,128)S(1)}, bf16[32,2048]{1,0:T(8,128)(2,1)S(1)}, bf16[32,2048]{1,0:T(8,128)(2,1)S(1)}, bf16[32,2048]{1,0:T(8,128)(2,1)S(1...) custom-call(bf16[3,144,128]{2,1,0:T(8,128)(2,1)S(1)} %collective-permute-done.11.refs_0_, ...), custom_call_target="tpu_custom_call" | custom-call | flops 536870912 | bytes 4194304 | tf_op jit(solution)/shard_map/pallas_call | solution.py:59
  37.5 2.5 %collective-permute-start.24 = (bf16[32,2048]{1,0:T(8,128)(2,1)S(1)}, bf16[32,2048]{1,0:T(8,128)(2,1)S(1)}, u32[]{:S(2)}, u32[]{:S(2)}) collective-permute-start(bf16[32,2048]{1,0:T(8,128)(2,1)S(1)} %get-tuple-element.45), channel_id=1, source_target_pairs={{0,6},{1,7},{2,4},{3,5},{4,2},{5,3},{6,0},{7,1},{8,14},{9,15},{10,... | collective-permute-start | bytes 393224 | tf_op jit(solution)/shard_map/ppermute | solution.py:26
  40.0 0.5 %collective-permute-start.25 = (bf16[32,2048]{1,0:T(8,128)(2,1)S(1)}, bf16[32,2048]{1,0:T(8,128)(2,1)S(1)}, u32[]{:S(2)}, u32[]{:S(2)}) collective-permute-start(bf16[32,2048]{1,0:T(8,128)(2,1)S(1)} %get-tuple-element.46), channel_id=1, source_target_pairs={{0,4},{1,5},{2,6},{3,7},{4,0},{5,1},{6,2},{7,3},{8,12},{9,13},{10,... | collective-permute-start | bytes 393224 | tf_op jit(solution)/shard_map/ppermute | solution.py:26
  40.5 0.5 %collective-permute-start.26 = (bf16[32,2048]{1,0:T(8,128)(2,1)S(1)}, bf16[32,2048]{1,0:T(8,128)(2,1)S(1)}, u32[]{:S(2)}, u32[]{:S(2)}) collective-permute-start(bf16[32,2048]{1,0:T(8,128)(2,1)S(1)} %get-tuple-element.47), channel_id=1, source_target_pairs={{0,2},{1,3},{2,0},{3,1},{4,6},{5,7},{6,4},{7,5},{8,10},{9,11},{10,... | collective-permute-start | bytes 393224 | tf_op jit(solution)/shard_map/ppermute | solution.py:26
  41.1 1.2 %collective-permute-done.27.got_ref = f32[1,128]{1,0:T(1,128)S(1)} collective-permute-done((f32[1,128]{1,0:T(1,128)S(1)}, f32[1,128]{1,0:T(1,128)S(1)}, u32[]{:S(2)}, u32[]{:S(2)}) %collective-permute-start.27) | collective-permute-done | bytes 544 | tf_op jit(solution)/shard_map/ppermute | solution.py:26
  42.2 0.6 %shard_map.146 = f32[1,256]{1,0:T(1,128)} custom-call(f32[1,128]{1,0:T(1,128)S(1)} %get-tuple-element.48.own_ref, f32[1,128]{1,0:T(1,128)S(1)} %collective-permute-done.27.got_ref), custom_call_target="tpu_custom_call" | custom-call | flops 4194304 | bytes 4096 | tf_op jit(solution)/shard_map/pallas_call | solution.py:59
  42.9 1.7 %collective-permute-done.24 = bf16[32,2048]{1,0:T(8,128)(2,1)S(1)} collective-permute-done((bf16[32,2048]{1,0:T(8,128)(2,1)S(1)}, bf16[32,2048]{1,0:T(8,128)(2,1)S(1)}, u32[]{:S(2)}, u32[]{:S(2)}) %collective-permute-start.24) | collective-permute-done | bytes 131104 | tf_op jit(solution)/shard_map/ppermute | solution.py:26
  44.6 2.3 %collective-permute-done.25 = bf16[32,2048]{1,0:T(8,128)(2,1)S(1)} collective-permute-done((bf16[32,2048]{1,0:T(8,128)(2,1)S(1)}, bf16[32,2048]{1,0:T(8,128)(2,1)S(1)}, u32[]{:S(2)}, u32[]{:S(2)}) %collective-permute-start.25) | collective-permute-done | bytes 131104 | tf_op jit(solution)/shard_map/ppermute | solution.py:26
  46.9 0.7 %add_convert_fusion = bf16[32,2048]{1,0:T(8,128)(2,1)} fusion(bf16[32,2048]{1,0:T(8,128)(2,1)S(1)} %collective-permute-done.26, bf16[32,2048]{1,0:T(8,128)(2,1)S(1)} %collective-permute-done.25, f32[32,2048]{1,0:T(8,128)S(1)} %get-tuple-element.44, bf16[32,2048]{1,0:T(8,128)(2,1)S(1)} %collective-permute-done.24), kind=kLoop, calls=%fused_computation | loop fusion | flops 458752 | bytes 786432 | tf_op jit(solution)/shard_map/convert_element_type | solution.py:526
  (48 shorter events, 1.6 us)
Async XLA Ops:
  0.6 11.4 %collective-permute-start.7 = (bf16[64,2048]{1,0:T(8,128)(2,1)}, bf16[64,2048]{1,0:T(8,128)(2,1)S(1)}, u32[]{:S(2)}, u32[]{:S(2)}) collective-permute-start(bf16[64,2048]{1,0:T(8,128)(2,1)} %bitcast.24), channel_id=1, source_target_pairs={{0,1},{1,0},{2,3},{3,2},{4,5},{5,4},{6,7},{7,6},{8,9},{9,8},{10,11... | collective-permute-start | bytes 786440 | tf_op jit(solution)/shard_map/ppermute | solution.py:26
  1.2 6.9 %collective-permute-start.3 = (bf16[256,256]{1,0:T(8,128)(2,1)}, bf16[256,256]{1,0:T(8,128)(2,1)S(1)}, u32[]{:S(2)}, u32[]{:S(2)}) collective-permute-start(bf16[256,256]{1,0:T(8,128)(2,1)} %refs_0_.1), channel_id=1, source_target_pairs={{0,4},{1,5},{2,6},{3,7},{4,0},{5,1},{6,2},{7,3},{8,12},{9,13},{10,... | collective-permute-start | bytes 393224 | tf_op jit(solution)/shard_map/ppermute | solution.py:26
  3.8 6.6 %collective-permute-start.1 = (bf16[256,256]{1,0:T(8,128)(2,1)}, bf16[256,256]{1,0:T(8,128)(2,1)S(1)}, u32[]{:S(2)}, u32[]{:S(2)}) collective-permute-start(bf16[256,256]{1,0:T(8,128)(2,1)} %refs_0_.1), channel_id=1, source_target_pairs={{0,2},{1,3},{2,0},{3,1},{4,6},{5,7},{6,4},{7,5},{8,10},{9,11},{10,... | collective-permute-start | bytes 393224 | tf_op jit(solution)/shard_map/ppermute | solution.py:26
  5.3 6.8 %collective-permute-start.5 = (bf16[256,256]{1,0:T(8,128)(2,1)}, bf16[256,256]{1,0:T(8,128)(2,1)S(1)}, u32[]{:S(2)}, u32[]{:S(2)}) collective-permute-start(bf16[256,256]{1,0:T(8,128)(2,1)} %refs_0_.1), channel_id=1, source_target_pairs={{0,6},{1,7},{2,4},{3,5},{4,2},{5,3},{6,0},{7,1},{8,14},{9,15},{10,... | collective-permute-start | bytes 393224 | tf_op jit(solution)/shard_map/ppermute | solution.py:26
  5.3 10.1 %collective-permute-start = (bf16[256,256]{1,0:T(8,128)(2,1)}, bf16[256,256]{1,0:T(8,128)(2,1)S(1)}, u32[]{:S(2)}, u32[]{:S(2)}) collective-permute-start(bf16[256,256]{1,0:T(8,128)(2,1)} %refs_0_.1), channel_id=1, source_target_pairs={{0,1},{1,0},{2,3},{3,2},{4,5},{5,4},{6,7},{7,6},{8,9},{9,8},{10,11... | collective-permute-start | bytes 393224 | tf_op jit(solution)/shard_map/ppermute | solution.py:26
  8.1 7.4 %collective-permute-start.4 = (bf16[256,256]{1,0:T(8,128)(2,1)S(1)}, bf16[256,256]{1,0:T(8,128)(2,1)S(1)}, u32[]{:S(2)}, u32[]{:S(2)}) collective-permute-start(bf16[256,256]{1,0:T(8,128)(2,1)S(1)} %collective-permute-done.3.refs_2_), channel_id=1, source_target_pairs={{0,1},{1,0},{2,3},{3,2},{4,5},{5,4},{6,7},{7,6},{8,9},{9,8},{10,11... | collective-permute-start | bytes 393224 | tf_op jit(solution)/shard_map/ppermute | solution.py:26
  10.4 5.1 %collective-permute-start.2 = (bf16[256,256]{1,0:T(8,128)(2,1)S(1)}, bf16[256,256]{1,0:T(8,128)(2,1)S(1)}, u32[]{:S(2)}, u32[]{:S(2)}) collective-permute-start(bf16[256,256]{1,0:T(8,128)(2,1)S(1)} %collective-permute-done.1.refs_1_), channel_id=1, source_target_pairs={{0,1},{1,0},{2,3},{3,2},{4,5},{5,4},{6,7},{7,6},{8,9},{9,8},{10,11... | collective-permute-start | bytes 393224 | tf_op jit(solution)/shard_map/ppermute | solution.py:26
  12.1 3.4 %collective-permute-start.6 = (bf16[256,256]{1,0:T(8,128)(2,1)S(1)}, bf16[256,256]{1,0:T(8,128)(2,1)S(1)}, u32[]{:S(2)}, u32[]{:S(2)}) collective-permute-start(bf16[256,256]{1,0:T(8,128)(2,1)S(1)} %collective-permute-done.5.refs_3_), channel_id=1, source_target_pairs={{0,1},{1,0},{2,3},{3,2},{4,5},{5,4},{6,7},{7,6},{8,9},{9,8},{10,11... | collective-permute-start | bytes 393224 | tf_op jit(solution)/shard_map/ppermute | solution.py:26
  12.1 2.9 %copy-start.1 = (bf16[256,256]{1,0:T(8,128)(2,1)S(1)}, bf16[256,256]{1,0:T(8,128)(2,1)}, u32[]{:S(2)}) copy-start(bf16[256,256]{1,0:T(8,128)(2,1)} %refs_0_.1) | copy-start | bytes 393220
  14.4 20.0 %collective-permute-start.22 = (bf16[320,2048]{1,0:T(8,128)(2,1)S(1)}, bf16[320,2048]{1,0:T(8,128)(2,1)S(1)}, u32[]{:S(2)}, u32[]{:S(2)}) collective-permute-start(bf16[320,2048]{1,0:T(8,128)(2,1)S(1)} %get-tuple-element.34.refs_9_.refs_6_), channel_id=1, source_target_pairs={{0,1},{1,0},{2,3},{3,2},{4,5},{5,4},{6,7},{7,6},{8,9},{9,8},{10,11... | collective-permute-start | bytes 3932168 | tf_op jit(solution)/shard_map/ppermute | solution.py:26
  15.5 12.5 %copy-start = (bf16[2048,128]{1,0:T(8,128)(2,1)S(1)}, bf16[2048,128]{1,0:T(8,128)(2,1)}, u32[]{:S(2)}) copy-start(bf16[2048,128]{1,0:T(8,128)(2,1)} %refs_4_.1) | copy-start | bytes 1572868
  15.5 12.5 %copy-start.4 = (bf16[3,128]{1,0:T(4,128)(2,1)S(1)}, bf16[3,128]{1,0:T(4,128)(2,1)}, u32[]{:S(2)}) copy-start(bf16[3,128]{1,0:T(4,128)(2,1)} %refs_8_.1) | copy-start | bytes 2308
  16.1 7.1 %collective-permute-start.10 = (bf16[152,128]{1,0:T(8,128)(2,1)S(1)}, bf16[152,128]{1,0:T(8,128)(2,1)S(1)}, u32[]{:S(2)}, u32[]{:S(2)}) collective-permute-start(bf16[152,128]{1,0:T(8,128)(2,1)S(1)} %get-tuple-element.33.refs_9_), channel_id=1, source_target_pairs={{0,24},{8,16},{16,8},{24,0},{1,25},{9,17},{17,9},{25,1},{2,26},{10... | collective-permute-start | bytes 116744 | tf_op jit(solution)/shard_map/ppermute | solution.py:26
  20.0 4.9 %collective-permute-start.9 = (bf16[152,128]{1,0:T(8,128)(2,1)S(1)}, bf16[152,128]{1,0:T(8,128)(2,1)S(1)}, u32[]{:S(2)}, u32[]{:S(2)}) collective-permute-start(bf16[152,128]{1,0:T(8,128)(2,1)S(1)} %get-tuple-element.33.refs_9_), channel_id=1, source_target_pairs={{0,16},{8,24},{16,0},{24,8},{1,17},{9,25},{17,1},{25,9},{2,18},{10... | collective-permute-start | bytes 116744 | tf_op jit(solution)/shard_map/ppermute | solution.py:26
  20.0 6.4 %collective-permute-start.8 = (bf16[152,128]{1,0:T(8,128)(2,1)S(1)}, bf16[152,128]{1,0:T(8,128)(2,1)S(1)}, u32[]{:S(2)}, u32[]{:S(2)}) collective-permute-start(bf16[152,128]{1,0:T(8,128)(2,1)S(1)} %get-tuple-element.33.refs_9_), channel_id=1, source_target_pairs={{0,8},{8,0},{16,24},{24,16},{1,9},{9,1},{17,25},{25,17},{2,10},{10... | collective-permute-start | bytes 116744 | tf_op jit(solution)/shard_map/ppermute | solution.py:26
  20.6 8.2 %collective-permute-start.20 = (bf16[144,128]{1,0:T(8,128)(2,1)S(1)}, bf16[144,128]{1,0:T(8,128)(2,1)S(1)}, u32[]{:S(2)}, u32[]{:S(2)}) collective-permute-start(bf16[144,128]{1,0:T(8,128)(2,1)S(1)} %get-tuple-element.51.refs_4_), channel_id=1, source_target_pairs={{0,6},{1,7},{2,4},{3,5},{4,2},{5,3},{6,0},{7,1},{8,14},{9,15},{10,... | collective-permute-start | bytes 110600 | tf_op jit(solution)/shard_map/ppermute | solution.py:26
  23.2 6.2 %collective-permute-start.19 = (bf16[144,128]{1,0:T(8,128)(2,1)S(1)}, bf16[144,128]{1,0:T(8,128)(2,1)S(1)}, u32[]{:S(2)}, u32[]{:S(2)}) collective-permute-start(bf16[144,128]{1,0:T(8,128)(2,1)S(1)} %get-tuple-element.51.refs_4_), channel_id=1, source_target_pairs={{0,4},{1,5},{2,6},{3,7},{4,0},{5,1},{6,2},{7,3},{8,12},{9,13},{10,... | collective-permute-start | bytes 110600 | tf_op jit(solution)/shard_map/ppermute | solution.py:26
  24.8 6.1 %collective-permute-start.18 = (bf16[144,128]{1,0:T(8,128)(2,1)S(1)}, bf16[144,128]{1,0:T(8,128)(2,1)S(1)}, u32[]{:S(2)}, u32[]{:S(2)}) collective-permute-start(bf16[144,128]{1,0:T(8,128)(2,1)S(1)} %get-tuple-element.51.refs_4_), channel_id=1, source_target_pairs={{0,2},{1,3},{2,0},{3,1},{4,6},{5,7},{6,4},{7,5},{8,10},{9,11},{10,... | collective-permute-start | bytes 110600 | tf_op jit(solution)/shard_map/ppermute | solution.py:26
  26.4 6.6 %collective-permute-start.16 = (bf16[3,144,128]{2,1,0:T(8,128)(2,1)S(1)}, bf16[3,144,128]{2,1,0:T(8,128)(2,1)S(1)}, u32[]{:S(2)}, u32[]{:S(2)}) collective-permute-start(bf16[3,144,128]{2,1,0:T(8,128)(2,1)S(1)} %pad_maximum_fusion.1.refs_0_), channel_id=1, source_target_pairs={{0,6},{1,7},{2,4},{3,5},{4,2},{5,3},{6,0},{7,1},{8,14},{9,15},{10,... | collective-permute-start | bytes 331784 | tf_op jit(solution)/shard_map/ppermute | solution.py:26
  27.9 6.7 %copy-start.3 = (f32[512]{0:T(512)S(1)}, f32[512]{0:T(512)}, u32[]{:S(2)}) copy-start(f32[512]{0:T(512)} %param.18) | copy-start | bytes 6148
  28.9 5.1 %collective-permute-start.14 = (bf16[3,144,128]{2,1,0:T(8,128)(2,1)S(1)}, bf16[3,144,128]{2,1,0:T(8,128)(2,1)S(1)}, u32[]{:S(2)}, u32[]{:S(2)}) collective-permute-start(bf16[3,144,128]{2,1,0:T(8,128)(2,1)S(1)} %pad_maximum_fusion.1.refs_0_), channel_id=1, source_target_pairs={{0,4},{1,5},{2,6},{3,7},{4,0},{5,1},{6,2},{7,3},{8,12},{9,13},{10,... | collective-permute-start | bytes 331784 | tf_op jit(solution)/shard_map/ppermute | solution.py:26
  29.4 4.7 %collective-permute-start.12 = (bf16[3,144,128]{2,1,0:T(8,128)(2,1)S(1)}, bf16[3,144,128]{2,1,0:T(8,128)(2,1)S(1)}, u32[]{:S(2)}, u32[]{:S(2)}) collective-permute-start(bf16[3,144,128]{2,1,0:T(8,128)(2,1)S(1)} %pad_maximum_fusion.1.refs_0_), channel_id=1, source_target_pairs={{0,2},{1,3},{2,0},{3,1},{4,6},{5,7},{6,4},{7,5},{8,10},{9,11},{10,... | collective-permute-start | bytes 331784 | tf_op jit(solution)/shard_map/ppermute | solution.py:26
  30.9 1.3 %collective-permute-start.23 = (bf16[128,384]{1,0:T(8,128)(2,1)S(1)}, bf16[128,384]{1,0:T(8,128)(2,1)S(1)}, u32[]{:S(2)}, u32[]{:S(2)}) collective-permute-start(bf16[128,384]{1,0:T(8,128)(2,1)S(1)} %get-tuple-element.41), channel_id=1, source_target_pairs={{0,1},{1,0},{2,3},{3,2},{4,5},{5,4},{6,7},{7,6},{8,9},{9,8},{10,11... | collective-permute-start | bytes 294920 | tf_op jit(solution)/shard_map/ppermute | solution.py:26
  32.2 3.6 %collective-permute-start.21 = (bf16[4,144,128]{2,1,0:T(8,128)(2,1)S(1)}, bf16[4,144,128]{2,1,0:T(8,128)(2,1)S(1)}, u32[]{:S(2)}, u32[]{:S(2)}) collective-permute-start(bf16[4,144,128]{2,1,0:T(8,128)(2,1)S(1)} %pad_maximum_fusion), channel_id=1, source_target_pairs={{0,1},{1,0},{2,3},{3,2},{4,5},{5,4},{6,7},{7,6},{8,9},{9,8},{10,11... | collective-permute-start | bytes 442376 | tf_op jit(solution)/shard_map/ppermute | solution.py:26
  33.0 2.8 %collective-permute-start.11 = (bf16[3,144,128]{2,1,0:T(8,128)(2,1)S(1)}, bf16[3,144,128]{2,1,0:T(8,128)(2,1)S(1)}, u32[]{:S(2)}, u32[]{:S(2)}) collective-permute-start(bf16[3,144,128]{2,1,0:T(8,128)(2,1)S(1)} %pad_maximum_fusion.1.refs_0_), channel_id=1, source_target_pairs={{0,1},{1,0},{2,3},{3,2},{4,5},{5,4},{6,7},{7,6},{8,9},{9,8},{10,11... | collective-permute-start | bytes 331784 | tf_op jit(solution)/shard_map/ppermute | solution.py:26
  33.9 1.9 %collective-permute-start.17 = (bf16[3,144,128]{2,1,0:T(8,128)(2,1)S(1)}, bf16[3,144,128]{2,1,0:T(8,128)(2,1)S(1)}, u32[]{:S(2)}, u32[]{:S(2)}) collective-permute-start(bf16[3,144,128]{2,1,0:T(8,128)(2,1)S(1)} %collective-permute-done.16.refs_3_), channel_id=1, source_target_pairs={{0,1},{1,0},{2,3},{3,2},{4,5},{5,4},{6,7},{7,6},{8,9},{9,8},{10,11... | collective-permute-start | bytes 331784 | tf_op jit(solution)/shard_map/ppermute | solution.py:26
  34.2 1.7 %collective-permute-start.15 = (bf16[3,144,128]{2,1,0:T(8,128)(2,1)S(1)}, bf16[3,144,128]{2,1,0:T(8,128)(2,1)S(1)}, u32[]{:S(2)}, u32[]{:S(2)}) collective-permute-start(bf16[3,144,128]{2,1,0:T(8,128)(2,1)S(1)} %collective-permute-done.14.refs_2_), channel_id=1, source_target_pairs={{0,1},{1,0},{2,3},{3,2},{4,5},{5,4},{6,7},{7,6},{8,9},{9,8},{10,11... | collective-permute-start | bytes 331784 | tf_op jit(solution)/shard_map/ppermute | solution.py:26
  34.4 1.4 %collective-permute-start.13 = (bf16[3,144,128]{2,1,0:T(8,128)(2,1)S(1)}, bf16[3,144,128]{2,1,0:T(8,128)(2,1)S(1)}, u32[]{:S(2)}, u32[]{:S(2)}) collective-permute-start(bf16[3,144,128]{2,1,0:T(8,128)(2,1)S(1)} %collective-permute-done.12.refs_1_), channel_id=1, source_target_pairs={{0,1},{1,0},{2,3},{3,2},{4,5},{5,4},{6,7},{7,6},{8,9},{9,8},{10,11... | collective-permute-start | bytes 331784 | tf_op jit(solution)/shard_map/ppermute | solution.py:26
  37.5 7.1 %collective-permute-start.24 = (bf16[32,2048]{1,0:T(8,128)(2,1)S(1)}, bf16[32,2048]{1,0:T(8,128)(2,1)S(1)}, u32[]{:S(2)}, u32[]{:S(2)}) collective-permute-start(bf16[32,2048]{1,0:T(8,128)(2,1)S(1)} %get-tuple-element.45), channel_id=1, source_target_pairs={{0,6},{1,7},{2,4},{3,5},{4,2},{5,3},{6,0},{7,1},{8,14},{9,15},{10,... | collective-permute-start | bytes 393224 | tf_op jit(solution)/shard_map/ppermute | solution.py:26
  40.0 6.9 %collective-permute-start.25 = (bf16[32,2048]{1,0:T(8,128)(2,1)S(1)}, bf16[32,2048]{1,0:T(8,128)(2,1)S(1)}, u32[]{:S(2)}, u32[]{:S(2)}) collective-permute-start(bf16[32,2048]{1,0:T(8,128)(2,1)S(1)} %get-tuple-element.46), channel_id=1, source_target_pairs={{0,4},{1,5},{2,6},{3,7},{4,0},{5,1},{6,2},{7,3},{8,12},{9,13},{10,... | collective-permute-start | bytes 393224 | tf_op jit(solution)/shard_map/ppermute | solution.py:26
  40.5 6.4 %collective-permute-start.26 = (bf16[32,2048]{1,0:T(8,128)(2,1)S(1)}, bf16[32,2048]{1,0:T(8,128)(2,1)S(1)}, u32[]{:S(2)}, u32[]{:S(2)}) collective-permute-start(bf16[32,2048]{1,0:T(8,128)(2,1)S(1)} %get-tuple-element.47), channel_id=1, source_target_pairs={{0,2},{1,3},{2,0},{3,1},{4,6},{5,7},{6,4},{7,5},{8,10},{9,11},{10,... | collective-permute-start | bytes 393224 | tf_op jit(solution)/shard_map/ppermute | solution.py:26
  41.1 1.2 %collective-permute-start.27 = (f32[1,128]{1,0:T(1,128)S(1)}, f32[1,128]{1,0:T(1,128)S(1)}, u32[]{:S(2)}, u32[]{:S(2)}) collective-permute-start(f32[1,128]{1,0:T(1,128)S(1)} %get-tuple-element.49), channel_id=1, source_target_pairs={{0,1},{1,0},{2,3},{3,2},{4,5},{5,4},{6,7},{7,6},{8,9},{9,8},{10,11... | collective-permute-start | bytes 1544 | tf_op jit(solution)/shard_map/ppermute | solution.py:26
  (1 other events, 2.9 us)

commit v5 on v4

--- a/solution.py
+++ b/solution.py
@@ -84,7 +84,7 @@
 
 def prepare(
     latent_ref, rope_ref, query_ref, pre_ref, value_ref, attend_ref, conv_ref, expand_ref, partner_ref,
-    key_w_ref, query_w_ref, mix_w_ref, own_w_ref, cos_ref, sin_ref, sems,
+    key_w_ref, query_w_ref, mix_w_ref, own_w_ref, cos_ref, sin_ref, expand_in, sems,
 ):
     core = lax.axis_index("tp") % 2
     mine = pl.ds(pl.multiple_of(core * ROPE, ROPE), ROPE)
@@ -99,11 +99,7 @@
         (attend_ref, own_w_ref.at[:VDIM]),
         (conv_ref, own_w_ref.at[VDIM : 2 * VDIM]),
     ]
-    wide = NOPE + VDIM
-    high = own_w_ref.shape[0] - 2 * VDIM
-    for k in range(own_w_ref.shape[1] // wide):
-        target = own_w_ref.at[2 * VDIM :, k * wide : (k + 1) * wide]
-        moves.append((expand_ref.at[k * high : (k + 1) * high], target))
+    moves.append((expand_ref, expand_in))
     copies = [pltpu.make_async_copy(source, target, sems.at[i]) for i, (source, target) in enumerate(moves)]
     for copy in copies:
         copy.start()
@@ -128,6 +124,10 @@
         sin_ref[rows, :] = jnp.where(by_row, row_sin[g : g + 1], col_sin)
     for copy in copies:
         copy.wait()
+    high, deep = own_w_ref.shape[0] - 2 * VDIM, expand_in.shape[0]
+    turned = jnp.transpose(expand_in[...].astype(F32)).astype(BF16)
+    for k in range(own_w_ref.shape[1] // deep):
+        own_w_ref[2 * VDIM :, k * deep : (k + 1) * deep] = turned[k * high : (k + 1) * high]
 
 
 def dot_nt(left, right):
@@ -274,14 +274,15 @@
         zeros = jnp.zeros_like(rope)
         sides = (jnp.where(low, rope, zeros), jnp.where(low, zeros, rope))
         queries.append([jnp.concatenate([nope, side], axis=1) for side in sides])
-    wide = NOPE + VDIM
-    starts = range(0, own_w_ref.shape[1], wide)
-
-    def expansion(ref, begin, size):
-        return jnp.concatenate([ref[2 * VDIM :, k + begin : k + begin + size] for k in starts], axis=0)
-
-    key_w = jnp.concatenate([expansion(ref, 0, NOPE) for ref in (own_w_ref, other_w_ref)], axis=1)
-    value_w = jnp.concatenate([expansion(ref, NOPE, VDIM) for ref in (own_w_ref, other_w_ref)], axis=1)
+    deep = pairs * LANES
+    blocks = range(own_w_ref.shape[1] // deep)
+
+    def expansion(part):
+        rows = [ref[2 * VDIM :, k * deep : (k + 1) * deep] for ref in (own_w_ref, other_w_ref) for k in part]
+        return jnp.concatenate(rows, axis=0)
+
+    key_w = expansion(blocks[: len(blocks) // 2])
+    value_w = expansion(blocks[len(blocks) // 2 :])
     views = [(chip ^ i, chip_slots) for i, chip_slots in enumerate(slots)]
 
     def rows_of(chip_slots, slot, first, start, count):
@@ -307,10 +308,8 @@
                     base = (side * chunk + slot) * group
                     latent_ref[base : base + group, columns] = scaled[side * group : (side + 1) * group]
         latent = latent_ref[...]
-        keys = jnp.dot(latent, key_w, preferred_element_type=F32).astype(BF16)
-        values = lax.dot_general(
-            value_w, latent, (((0,), (1,)), ((), ())), preferred_element_type=F32
-        ).astype(BF16)
+        keys = dot_nt(latent, key_w).astype(BF16)
+        values = dot_nt(value_w, latent).astype(BF16)
         rope = rope_ref[...]
         count = chunk * group
         spans = [slice(i * count, (i + 1) * count) for i in range(2)]
@@ -434,7 +433,7 @@
             ((tokens, LANES), F32),
         ],
         16 << 20,
-        scratch=[pltpu.SemaphoreType.DMA((9 + features // (NOPE + VDIM),))],
+        scratch=[pltpu.VMEM(expand_weight.shape, BF16), pltpu.SemaphoreType.DMA((10,))],
         flops=1 << 28,
         nbytes=1 << 23,
         in_hbm=range(8),

time: 47.8 us -> 47.9 us (level)
  no operation moved by 1% of the time
where the time goes in v5:
time: 47.9 us; the launch traced here: 47.8 us
  starting transfers between devices  22.2 us (46%)
  waiting for transfers between devices  16.2 us (34%)
  Pallas kernels  7.75 us (16%)
  between operations  0.82 us (2%)
  other arithmetic  0.75 us (2%)
    ppermute x28, starting transfers between devices, swap(): return lax.ppermute(array, axis, [(i, i ^ mask) for i in range(peers)])  22.2 us
    ppermute x28, waiting for transfers between devices, swap(): return lax.ppermute(array, axis, [(i, i ^ mask) for i in range(peers)])  16.2 us
    pallas_call x7, Pallas kernels, call(): pl.pallas_call(body, out_shape=[jax.ShapeDtypeStruct(shape, dtype) for sh...  7.75 us
  transfers between devices with their start and end apart: 28, of which 11 were waited for; matrix products, arithmetic and copies ran while one was open for 0% of the time, Pallas kernels for 13%

profile of v5, /device:TPU:0, one launch (start us, length us, event | category | flops | bytes accessed | tf_op | source)
XLA Modules:
  0.0 47.8 jit_solution(1915688772564516445)
XLA Ops:
  0.6 0.6 %collective-permute-start.7 = (bf16[64,2048]{1,0:T(8,128)(2,1)}, bf16[64,2048]{1,0:T(8,128)(2,1)S(1)}, u32[]{:S(2)}, u32[]{:S(2)}) collective-permute-start(bf16[64,2048]{1,0:T(8,128)(2,1)} %bitcast.24), channel_id=1, source_target_pairs={{0,1},{1,0},{2,3},{3,2},{4,5},{5,4},{6,7},{7,6},{8,9},{9,8},{10,11... | collective-permute-start | bytes 786440 | tf_op jit(solution)/shard_map/ppermute | solution.py:26
  1.2 2.6 %collective-permute-start.3 = (bf16[256,256]{1,0:T(8,128)(2,1)}, bf16[256,256]{1,0:T(8,128)(2,1)S(1)}, u32[]{:S(2)}, u32[]{:S(2)}) collective-permute-start(bf16[256,256]{1,0:T(8,128)(2,1)} %refs_0_.1), channel_id=1, source_target_pairs={{0,4},{1,5},{2,6},{3,7},{4,0},{5,1},{6,2},{7,3},{8,12},{9,13},{10,... | collective-permute-start | bytes 393224 | tf_op jit(solution)/shard_map/ppermute | solution.py:26
  3.8 1.5 %collective-permute-start.1 = (bf16[256,256]{1,0:T(8,128)(2,1)}, bf16[256,256]{1,0:T(8,128)(2,1)S(1)}, u32[]{:S(2)}, u32[]{:S(2)}) collective-permute-start(bf16[256,256]{1,0:T(8,128)(2,1)} %refs_0_.1), channel_id=1, source_target_pairs={{0,2},{1,3},{2,0},{3,1},{4,6},{5,7},{6,4},{7,5},{8,10},{9,11},{10,... | collective-permute-start | bytes 393224 | tf_op jit(solution)/shard_map/ppermute | solution.py:26
  5.3 2.8 %collective-permute-done.3.refs_2_ = bf16[256,256]{1,0:T(8,128)(2,1)S(1)} collective-permute-done((bf16[256,256]{1,0:T(8,128)(2,1)}, bf16[256,256]{1,0:T(8,128)(2,1)S(1)}, u32[]{:S(2)}, u32[]{:S(2)}) %collective-permute-start.3) | collective-permute-done | bytes 131104 | tf_op jit(solution)/shard_map/ppermute | solution.py:26
  8.1 2.3 %collective-permute-done.1.refs_1_ = bf16[256,256]{1,0:T(8,128)(2,1)S(1)} collective-permute-done((bf16[256,256]{1,0:T(8,128)(2,1)}, bf16[256,256]{1,0:T(8,128)(2,1)S(1)}, u32[]{:S(2)}, u32[]{:S(2)}) %collective-permute-start.1) | collective-permute-done | bytes 131104 | tf_op jit(solution)/shard_map/ppermute | solution.py:26
  10.4 1.7 %collective-permute-done.5.refs_3_ = bf16[256,256]{1,0:T(8,128)(2,1)S(1)} collective-permute-done((bf16[256,256]{1,0:T(8,128)(2,1)}, bf16[256,256]{1,0:T(8,128)(2,1)S(1)}, u32[]{:S(2)}, u32[]{:S(2)}) %collective-permute-start.5) | collective-permute-done | bytes 131104 | tf_op jit(solution)/shard_map/ppermute | solution.py:26
  12.1 2.4 %shard_map.140 = (bf16[256,2048]{1,0:T(8,128)(2,1)S(1)}, bf16[256,2048]{1,0:T(8,128)(2,1)S(1)}, bf16[2048,256]{1,0:T(8,128)(2,1)S(1)}, bf16[320,2048]{1,0:T(8,12...) custom-call(bf16[64,2048]{1,0:T(8,128)(2,1)} %bitcast.25, bf16[64,2048]{1,0:T(8,128)(2,1)} %bitcast.26, ...), custom_call_target="tpu_custom_call" | custom-call | flops 268435456 | bytes 8388608 | tf_op jit(solution)/shard_map/pallas_call | solution.py:59
  14.5 0.5 %collective-permute-start.22 = (bf16[320,2048]{1,0:T(8,128)(2,1)S(1)}, bf16[320,2048]{1,0:T(8,128)(2,1)S(1)}, u32[]{:S(2)}, u32[]{:S(2)}) collective-permute-start(bf16[320,2048]{1,0:T(8,128)(2,1)S(1)} %get-tuple-element.34.refs_9_.refs_6_), channel_id=1, source_target_pairs={{0,1},{1,0},{2,3},{3,2},{4,5},{5,4},{6,7},{7,6},{8,9},{9,8},{10,11... | collective-permute-start | bytes 3932168 | tf_op jit(solution)/shard_map/ppermute | solution.py:26
  15.6 0.6 %shard_map.142 = (bf16[256,1024]{1,0:T(8,128)(2,1)S(1)}, f32[256,128]{1,0:T(8,128)S(1)}, bf16[152,128]{1,0:T(8,128)(2,1)S(1)}, bf16[256,128]{1,0:T(8,128)(2,1)S(1)}) custom-call(bf16[256,256]{1,0:T(8,128)(2,1)S(1)} %collective-permute-done.refs_0_, bf16[256,256]{1,0:T(8,128)(2,1)S(1)} %collective-permute-done.2.refs_1_, ...), custom_call_target="tpu_custom_call" | custom-call | flops 268435456 | bytes 1048576 | tf_op jit(solution)/shard_map/pallas_call | solution.py:59
  16.2 3.9 %collective-permute-start.10 = (bf16[152,128]{1,0:T(8,128)(2,1)S(1)}, bf16[152,128]{1,0:T(8,128)(2,1)S(1)}, u32[]{:S(2)}, u32[]{:S(2)}) collective-permute-start(bf16[152,128]{1,0:T(8,128)(2,1)S(1)} %get-tuple-element.33.refs_9_), channel_id=1, source_target_pairs={{0,24},{8,16},{16,8},{24,0},{1,25},{9,17},{17,9},{25,1},{2,26},{10... | collective-permute-start | bytes 116744 | tf_op jit(solution)/shard_map/ppermute | solution.py:26
  20.1 0.6 %collective-permute-start.8 = (bf16[152,128]{1,0:T(8,128)(2,1)S(1)}, bf16[152,128]{1,0:T(8,128)(2,1)S(1)}, u32[]{:S(2)}, u32[]{:S(2)}) collective-permute-start(bf16[152,128]{1,0:T(8,128)(2,1)S(1)} %get-tuple-element.33.refs_9_), channel_id=1, source_target_pairs={{0,8},{8,0},{16,24},{24,16},{1,9},{9,1},{17,25},{25,17},{2,10},{10... | collective-permute-start | bytes 116744 | tf_op jit(solution)/shard_map/ppermute | solution.py:26
  20.7 2.6 %collective-permute-start.20 = (bf16[144,128]{1,0:T(8,128)(2,1)S(1)}, bf16[144,128]{1,0:T(8,128)(2,1)S(1)}, u32[]{:S(2)}, u32[]{:S(2)}) collective-permute-start(bf16[144,128]{1,0:T(8,128)(2,1)S(1)} %get-tuple-element.51.refs_4_), channel_id=1, source_target_pairs={{0,6},{1,7},{2,4},{3,5},{4,2},{5,3},{6,0},{7,1},{8,14},{9,15},{10,... | collective-permute-start | bytes 110600 | tf_op jit(solution)/shard_map/ppermute | solution.py:26
  23.3 0.5 %collective-permute-start.19 = (bf16[144,128]{1,0:T(8,128)(2,1)S(1)}, bf16[144,128]{1,0:T(8,128)(2,1)S(1)}, u32[]{:S(2)}, u32[]{:S(2)}) collective-permute-start(bf16[144,128]{1,0:T(8,128)(2,1)S(1)} %get-tuple-element.51.refs_4_), channel_id=1, source_target_pairs={{0,4},{1,5},{2,6},{3,7},{4,0},{5,1},{6,2},{7,3},{8,12},{9,13},{10,... | collective-permute-start | bytes 110600 | tf_op jit(solution)/shard_map/ppermute | solution.py:26
  23.9 1.1 %collective-permute-done.9.refs_11_ = bf16[152,128]{1,0:T(8,128)(2,1)S(1)} collective-permute-done((bf16[152,128]{1,0:T(8,128)(2,1)S(1)}, bf16[152,128]{1,0:T(8,128)(2,1)S(1)}, u32[]{:S(2)}, u32[]{:S(2)}) %collective-permute-start.9) | collective-permute-done | bytes 38944 | tf_op jit(solution)/shard_map/ppermute | solution.py:26
  25.0 1.5 %collective-permute-start.18 = (bf16[144,128]{1,0:T(8,128)(2,1)S(1)}, bf16[144,128]{1,0:T(8,128)(2,1)S(1)}, u32[]{:S(2)}, u32[]{:S(2)}) collective-permute-start(bf16[144,128]{1,0:T(8,128)(2,1)S(1)} %get-tuple-element.51.refs_4_), channel_id=1, source_target_pairs={{0,2},{1,3},{2,0},{3,1},{4,6},{5,7},{6,4},{7,5},{8,10},{9,11},{10,... | collective-permute-start | bytes 110600 | tf_op jit(solution)/shard_map/ppermute | solution.py:26
  26.5 1.6 %collective-permute-start.16 = (bf16[3,144,128]{2,1,0:T(8,128)(2,1)S(1)}, bf16[3,144,128]{2,1,0:T(8,128)(2,1)S(1)}, u32[]{:S(2)}, u32[]{:S(2)}) collective-permute-start(bf16[3,144,128]{2,1,0:T(8,128)(2,1)S(1)} %pad_maximum_fusion.1.refs_0_), channel_id=1, source_target_pairs={{0,6},{1,7},{2,4},{3,5},{4,2},{5,3},{6,0},{7,1},{8,14},{9,15},{10,... | collective-permute-start | bytes 331784 | tf_op jit(solution)/shard_map/ppermute | solution.py:26
  28.1 0.9 %shard_map.143 = (bf16[128,384]{1,0:T(8,128)(2,1)S(1)}, bf16[128,384]{1,0:T(8,128)(2,1)S(1)}) custom-call(bf16[256,1024]{1,0:T(8,128)(2,1)S(1)} %get-tuple-element.35.refs_0_, bf16[256,1024]{1,0:T(8,128)(2,1)S(1)} %get-tuple-element.36.refs_1_, f32[256,128]{1,0:T(8,128)S(1)} %get-tuple-element.37.refs_2_, bf16[256,2048]{1,0:T(8,128)(2,1)S(1)} %get-tuple-element.38.refs_3_, ...), custom_call_target="tpu_custom_call" | custom-call | flops 402653184 | bytes 2097152 | tf_op jit(solution)/shard_map/pallas_call | solution.py:59
  29.0 0.6 %collective-permute-start.14 = (bf16[3,144,128]{2,1,0:T(8,128)(2,1)S(1)}, bf16[3,144,128]{2,1,0:T(8,128)(2,1)S(1)}, u32[]{:S(2)}, u32[]{:S(2)}) collective-permute-start(bf16[3,144,128]{2,1,0:T(8,128)(2,1)S(1)} %pad_maximum_fusion.1.refs_0_), channel_id=1, source_target_pairs={{0,4},{1,5},{2,6},{3,7},{4,0},{5,1},{6,2},{7,3},{8,12},{9,13},{10,... | collective-permute-start | bytes 331784 | tf_op jit(solution)/shard_map/ppermute | solution.py:26
  29.6 1.5 %collective-permute-start.12 = (bf16[3,144,128]{2,1,0:T(8,128)(2,1)S(1)}, bf16[3,144,128]{2,1,0:T(8,128)(2,1)S(1)}, u32[]{:S(2)}, u32[]{:S(2)}) collective-permute-start(bf16[3,144,128]{2,1,0:T(8,128)(2,1)S(1)} %pad_maximum_fusion.1.refs_0_), channel_id=1, source_target_pairs={{0,2},{1,3},{2,0},{3,1},{4,6},{5,7},{6,4},{7,5},{8,10},{9,11},{10,... | collective-permute-start | bytes 331784 | tf_op jit(solution)/shard_map/ppermute | solution.py:26
  31.1 1.3 %collective-permute-done.23.refs_12_.refs_9_ = bf16[128,384]{1,0:T(8,128)(2,1)S(1)} collective-permute-done((bf16[128,384]{1,0:T(8,128)(2,1)S(1)}, bf16[128,384]{1,0:T(8,128)(2,1)S(1)}, u32[]{:S(2)}, u32[]{:S(2)}) %collective-permute-start.23) | collective-permute-done | bytes 98336 | tf_op jit(solution)/shard_map/ppermute | solution.py:26
  32.5 0.6 %collective-permute-done.16.refs_3_ = bf16[3,144,128]{2,1,0:T(8,128)(2,1)S(1)} collective-permute-done((bf16[3,144,128]{2,1,0:T(8,128)(2,1)S(1)}, bf16[3,144,128]{2,1,0:T(8,128)(2,1)S(1)}, u32[]{:S(2)}, u32[]{:S(2)}) %collective-permute-start.16) | collective-permute-done | bytes 110624 | tf_op jit(solution)/shard_map/ppermute | solution.py:26
  33.1 0.9 %collective-permute-done.14.refs_2_ = bf16[3,144,128]{2,1,0:T(8,128)(2,1)S(1)} collective-permute-done((bf16[3,144,128]{2,1,0:T(8,128)(2,1)S(1)}, bf16[3,144,128]{2,1,0:T(8,128)(2,1)S(1)}, u32[]{:S(2)}, u32[]{:S(2)}) %collective-permute-start.14) | collective-permute-done | bytes 110624 | tf_op jit(solution)/shard_map/ppermute | solution.py:26
  34.8 1.1 %shard_map.144 = (f32[8,256]{1,0:T(8,128)S(1)}, f32[128,256]{1,0:T(8,128)S(1)}) custom-call(bf16[3,144,128]{2,1,0:T(8,128)(2,1)S(1)} %pad_maximum_fusion.1.refs_0_, bf16[3,144,128]{2,1,0:T(8,128)(2,1)S(1)} %collective-permute-done.12.refs_1_, bf16[3,144,128]{2,1,0:T(8,128)(2,1)S(1)} %collective-permute-done.14.refs_2_, ...), custom_call_target="tpu_custom_call" | custom-call | flops 536870912 | bytes 4194304 | tf_op jit(solution)/shard_map/pallas_call | solution.py:59
  36.0 1.6 %shard_map.145 = (f32[32,2048]{1,0:T(8,128)S(1)}, bf16[32,2048]{1,0:T(8,128)(2,1)S(1)}, bf16[32,2048]{1,0:T(8,128)(2,1)S(1)}, bf16[32,2048]{1,0:T(8,128)(2,1)S(1...) custom-call(bf16[3,144,128]{2,1,0:T(8,128)(2,1)S(1)} %collective-permute-done.11.refs_0_, ...), custom_call_target="tpu_custom_call" | custom-call | flops 536870912 | bytes 4194304 | tf_op jit(solution)/shard_map/pallas_call | solution.py:59
  37.6 2.5 %collective-permute-start.24 = (bf16[32,2048]{1,0:T(8,128)(2,1)S(1)}, bf16[32,2048]{1,0:T(8,128)(2,1)S(1)}, u32[]{:S(2)}, u32[]{:S(2)}) collective-permute-start(bf16[32,2048]{1,0:T(8,128)(2,1)S(1)} %get-tuple-element.45), channel_id=1, source_target_pairs={{0,6},{1,7},{2,4},{3,5},{4,2},{5,3},{6,0},{7,1},{8,14},{9,15},{10,... | collective-permute-start | bytes 393224 | tf_op jit(solution)/shard_map/ppermute | solution.py:26
  40.1 0.5 %collective-permute-start.25 = (bf16[32,2048]{1,0:T(8,128)(2,1)S(1)}, bf16[32,2048]{1,0:T(8,128)(2,1)S(1)}, u32[]{:S(2)}, u32[]{:S(2)}) collective-permute-start(bf16[32,2048]{1,0:T(8,128)(2,1)S(1)} %get-tuple-element.46), channel_id=1, source_target_pairs={{0,4},{1,5},{2,6},{3,7},{4,0},{5,1},{6,2},{7,3},{8,12},{9,13},{10,... | collective-permute-start | bytes 393224 | tf_op jit(solution)/shard_map/ppermute | solution.py:26
  40.6 0.5 %collective-permute-start.26 = (bf16[32,2048]{1,0:T(8,128)(2,1)S(1)}, bf16[32,2048]{1,0:T(8,128)(2,1)S(1)}, u32[]{:S(2)}, u32[]{:S(2)}) collective-permute-start(bf16[32,2048]{1,0:T(8,128)(2,1)S(1)} %get-tuple-element.47), channel_id=1, source_target_pairs={{0,2},{1,3},{2,0},{3,1},{4,6},{5,7},{6,4},{7,5},{8,10},{9,11},{10,... | collective-permute-start | bytes 393224 | tf_op jit(solution)/shard_map/ppermute | solution.py:26
  41.2 1.2 %collective-permute-done.27.got_ref = f32[1,128]{1,0:T(1,128)S(1)} collective-permute-done((f32[1,128]{1,0:T(1,128)S(1)}, f32[1,128]{1,0:T(1,128)S(1)}, u32[]{:S(2)}, u32[]{:S(2)}) %collective-permute-start.27) | collective-permute-done | bytes 544 | tf_op jit(solution)/shard_map/ppermute | solution.py:26
  42.3 0.6 %shard_map.146 = f32[1,256]{1,0:T(1,128)} custom-call(f32[1,128]{1,0:T(1,128)S(1)} %get-tuple-element.48.own_ref, f32[1,128]{1,0:T(1,128)S(1)} %collective-permute-done.27.got_ref), custom_call_target="tpu_custom_call" | custom-call | flops 4194304 | bytes 4096 | tf_op jit(solution)/shard_map/pallas_call | solution.py:59
  43.0 1.7 %collective-permute-done.24 = bf16[32,2048]{1,0:T(8,128)(2,1)S(1)} collective-permute-done((bf16[32,2048]{1,0:T(8,128)(2,1)S(1)}, bf16[32,2048]{1,0:T(8,128)(2,1)S(1)}, u32[]{:S(2)}, u32[]{:S(2)}) %collective-permute-start.24) | collective-permute-done | bytes 131104 | tf_op jit(solution)/shard_map/ppermute | solution.py:26
  44.7 2.3 %collective-permute-done.25 = bf16[32,2048]{1,0:T(8,128)(2,1)S(1)} collective-permute-done((bf16[32,2048]{1,0:T(8,128)(2,1)S(1)}, bf16[32,2048]{1,0:T(8,128)(2,1)S(1)}, u32[]{:S(2)}, u32[]{:S(2)}) %collective-permute-start.25) | collective-permute-done | bytes 131104 | tf_op jit(solution)/shard_map/ppermute | solution.py:26
  47.0 0.7 %add_convert_fusion = bf16[32,2048]{1,0:T(8,128)(2,1)} fusion(bf16[32,2048]{1,0:T(8,128)(2,1)S(1)} %collective-permute-done.26, bf16[32,2048]{1,0:T(8,128)(2,1)S(1)} %collective-permute-done.25, f32[32,2048]{1,0:T(8,128)S(1)} %get-tuple-element.44, bf16[32,2048]{1,0:T(8,128)(2,1)S(1)} %collective-permute-done.24), kind=kLoop, calls=%fused_computation | loop fusion | flops 458752 | bytes 786432 | tf_op jit(solution)/shard_map/convert_element_type | solution.py:525
  (48 shorter events, 1.6 us)
Async XLA Ops:
  0.6 11.4 %collective-permute-start.7 = (bf16[64,2048]{1,0:T(8,128)(2,1)}, bf16[64,2048]{1,0:T(8,128)(2,1)S(1)}, u32[]{:S(2)}, u32[]{:S(2)}) collective-permute-start(bf16[64,2048]{1,0:T(8,128)(2,1)} %bitcast.24), channel_id=1, source_target_pairs={{0,1},{1,0},{2,3},{3,2},{4,5},{5,4},{6,7},{7,6},{8,9},{9,8},{10,11... | collective-permute-start | bytes 786440 | tf_op jit(solution)/shard_map/ppermute | solution.py:26
  1.2 6.9 %collective-permute-start.3 = (bf16[256,256]{1,0:T(8,128)(2,1)}, bf16[256,256]{1,0:T(8,128)(2,1)S(1)}, u32[]{:S(2)}, u32[]{:S(2)}) collective-permute-start(bf16[256,256]{1,0:T(8,128)(2,1)} %refs_0_.1), channel_id=1, source_target_pairs={{0,4},{1,5},{2,6},{3,7},{4,0},{5,1},{6,2},{7,3},{8,12},{9,13},{10,... | collective-permute-start | bytes 393224 | tf_op jit(solution)/shard_map/ppermute | solution.py:26
  3.8 6.6 %collective-permute-start.1 = (bf16[256,256]{1,0:T(8,128)(2,1)}, bf16[256,256]{1,0:T(8,128)(2,1)S(1)}, u32[]{:S(2)}, u32[]{:S(2)}) collective-permute-start(bf16[256,256]{1,0:T(8,128)(2,1)} %refs_0_.1), channel_id=1, source_target_pairs={{0,2},{1,3},{2,0},{3,1},{4,6},{5,7},{6,4},{7,5},{8,10},{9,11},{10,... | collective-permute-start | bytes 393224 | tf_op jit(solution)/shard_map/ppermute | solution.py:26
  5.3 6.8 %collective-permute-start.5 = (bf16[256,256]{1,0:T(8,128)(2,1)}, bf16[256,256]{1,0:T(8,128)(2,1)S(1)}, u32[]{:S(2)}, u32[]{:S(2)}) collective-permute-start(bf16[256,256]{1,0:T(8,128)(2,1)} %refs_0_.1), channel_id=1, source_target_pairs={{0,6},{1,7},{2,4},{3,5},{4,2},{5,3},{6,0},{7,1},{8,14},{9,15},{10,... | collective-permute-start | bytes 393224 | tf_op jit(solution)/shard_map/ppermute | solution.py:26
  5.3 10.2 %collective-permute-start = (bf16[256,256]{1,0:T(8,128)(2,1)}, bf16[256,256]{1,0:T(8,128)(2,1)S(1)}, u32[]{:S(2)}, u32[]{:S(2)}) collective-permute-start(bf16[256,256]{1,0:T(8,128)(2,1)} %refs_0_.1), channel_id=1, source_target_pairs={{0,1},{1,0},{2,3},{3,2},{4,5},{5,4},{6,7},{7,6},{8,9},{9,8},{10,11... | collective-permute-start | bytes 393224 | tf_op jit(solution)/shard_map/ppermute | solution.py:26
  8.1 7.5 %collective-permute-start.4 = (bf16[256,256]{1,0:T(8,128)(2,1)S(1)}, bf16[256,256]{1,0:T(8,128)(2,1)S(1)}, u32[]{:S(2)}, u32[]{:S(2)}) collective-permute-start(bf16[256,256]{1,0:T(8,128)(2,1)S(1)} %collective-permute-done.3.refs_2_), channel_id=1, source_target_pairs={{0,1},{1,0},{2,3},{3,2},{4,5},{5,4},{6,7},{7,6},{8,9},{9,8},{10,11... | collective-permute-start | bytes 393224 | tf_op jit(solution)/shard_map/ppermute | solution.py:26
  10.4 5.2 %collective-permute-start.2 = (bf16[256,256]{1,0:T(8,128)(2,1)S(1)}, bf16[256,256]{1,0:T(8,128)(2,1)S(1)}, u32[]{:S(2)}, u32[]{:S(2)}) collective-permute-start(bf16[256,256]{1,0:T(8,128)(2,1)S(1)} %collective-permute-done.1.refs_1_), channel_id=1, source_target_pairs={{0,1},{1,0},{2,3},{3,2},{4,5},{5,4},{6,7},{7,6},{8,9},{9,8},{10,11... | collective-permute-start | bytes 393224 | tf_op jit(solution)/shard_map/ppermute | solution.py:26
  12.1 3.5 %collective-permute-start.6 = (bf16[256,256]{1,0:T(8,128)(2,1)S(1)}, bf16[256,256]{1,0:T(8,128)(2,1)S(1)}, u32[]{:S(2)}, u32[]{:S(2)}) collective-permute-start(bf16[256,256]{1,0:T(8,128)(2,1)S(1)} %collective-permute-done.5.refs_3_), channel_id=1, source_target_pairs={{0,1},{1,0},{2,3},{3,2},{4,5},{5,4},{6,7},{7,6},{8,9},{9,8},{10,11... | collective-permute-start | bytes 393224 | tf_op jit(solution)/shard_map/ppermute | solution.py:26
  12.1 3.0 %copy-start.1 = (bf16[256,256]{1,0:T(8,128)(2,1)S(1)}, bf16[256,256]{1,0:T(8,128)(2,1)}, u32[]{:S(2)}) copy-start(bf16[256,256]{1,0:T(8,128)(2,1)} %refs_0_.1) | copy-start | bytes 393220
  14.5 20.0 %collective-permute-start.22 = (bf16[320,2048]{1,0:T(8,128)(2,1)S(1)}, bf16[320,2048]{1,0:T(8,128)(2,1)S(1)}, u32[]{:S(2)}, u32[]{:S(2)}) collective-permute-start(bf16[320,2048]{1,0:T(8,128)(2,1)S(1)} %get-tuple-element.34.refs_9_.refs_6_), channel_id=1, source_target_pairs={{0,1},{1,0},{2,3},{3,2},{4,5},{5,4},{6,7},{7,6},{8,9},{9,8},{10,11... | collective-permute-start | bytes 3932168 | tf_op jit(solution)/shard_map/ppermute | solution.py:26
  15.6 12.5 %copy-start = (bf16[2048,128]{1,0:T(8,128)(2,1)S(1)}, bf16[2048,128]{1,0:T(8,128)(2,1)}, u32[]{:S(2)}) copy-start(bf16[2048,128]{1,0:T(8,128)(2,1)} %refs_4_.1) | copy-start | bytes 1572868
  15.6 12.5 %copy-start.4 = (bf16[3,128]{1,0:T(4,128)(2,1)S(1)}, bf16[3,128]{1,0:T(4,128)(2,1)}, u32[]{:S(2)}) copy-start(bf16[3,128]{1,0:T(4,128)(2,1)} %refs_8_.1) | copy-start | bytes 2308
  16.2 7.1 %collective-permute-start.10 = (bf16[152,128]{1,0:T(8,128)(2,1)S(1)}, bf16[152,128]{1,0:T(8,128)(2,1)S(1)}, u32[]{:S(2)}, u32[]{:S(2)}) collective-permute-start(bf16[152,128]{1,0:T(8,128)(2,1)S(1)} %get-tuple-element.33.refs_9_), channel_id=1, source_target_pairs={{0,24},{8,16},{16,8},{24,0},{1,25},{9,17},{17,9},{25,1},{2,26},{10... | collective-permute-start | bytes 116744 | tf_op jit(solution)/shard_map/ppermute | solution.py:26
  20.1 4.9 %collective-permute-start.9 = (bf16[152,128]{1,0:T(8,128)(2,1)S(1)}, bf16[152,128]{1,0:T(8,128)(2,1)S(1)}, u32[]{:S(2)}, u32[]{:S(2)}) collective-permute-start(bf16[152,128]{1,0:T(8,128)(2,1)S(1)} %get-tuple-element.33.refs_9_), channel_id=1, source_target_pairs={{0,16},{8,24},{16,0},{24,8},{1,17},{9,25},{17,1},{25,9},{2,18},{10... | collective-permute-start | bytes 116744 | tf_op jit(solution)/shard_map/ppermute | solution.py:26
  20.1 6.4 %collective-permute-start.8 = (bf16[152,128]{1,0:T(8,128)(2,1)S(1)}, bf16[152,128]{1,0:T(8,128)(2,1)S(1)}, u32[]{:S(2)}, u32[]{:S(2)}) collective-permute-start(bf16[152,128]{1,0:T(8,128)(2,1)S(1)} %get-tuple-element.33.refs_9_), channel_id=1, source_target_pairs={{0,8},{8,0},{16,24},{24,16},{1,9},{9,1},{17,25},{25,17},{2,10},{10... | collective-permute-start | bytes 116744 | tf_op jit(solution)/shard_map/ppermute | solution.py:26
  20.7 8.2 %collective-permute-start.20 = (bf16[144,128]{1,0:T(8,128)(2,1)S(1)}, bf16[144,128]{1,0:T(8,128)(2,1)S(1)}, u32[]{:S(2)}, u32[]{:S(2)}) collective-permute-start(bf16[144,128]{1,0:T(8,128)(2,1)S(1)} %get-tuple-element.51.refs_4_), channel_id=1, source_target_pairs={{0,6},{1,7},{2,4},{3,5},{4,2},{5,3},{6,0},{7,1},{8,14},{9,15},{10,... | collective-permute-start | bytes 110600 | tf_op jit(solution)/shard_map/ppermute | solution.py:26
  23.3 6.2 %collective-permute-start.19 = (bf16[144,128]{1,0:T(8,128)(2,1)S(1)}, bf16[144,128]{1,0:T(8,128)(2,1)S(1)}, u32[]{:S(2)}, u32[]{:S(2)}) collective-permute-start(bf16[144,128]{1,0:T(8,128)(2,1)S(1)} %get-tuple-element.51.refs_4_), channel_id=1, source_target_pairs={{0,4},{1,5},{2,6},{3,7},{4,0},{5,1},{6,2},{7,3},{8,12},{9,13},{10,... | collective-permute-start | bytes 110600 | tf_op jit(solution)/shard_map/ppermute | solution.py:26
  25.0 6.1 %collective-permute-start.18 = (bf16[144,128]{1,0:T(8,128)(2,1)S(1)}, bf16[144,128]{1,0:T(8,128)(2,1)S(1)}, u32[]{:S(2)}, u32[]{:S(2)}) collective-permute-start(bf16[144,128]{1,0:T(8,128)(2,1)S(1)} %get-tuple-element.51.refs_4_), channel_id=1, source_target_pairs={{0,2},{1,3},{2,0},{3,1},{4,6},{5,7},{6,4},{7,5},{8,10},{9,11},{10,... | collective-permute-start | bytes 110600 | tf_op jit(solution)/shard_map/ppermute | solution.py:26
  26.5 6.6 %collective-permute-start.16 = (bf16[3,144,128]{2,1,0:T(8,128)(2,1)S(1)}, bf16[3,144,128]{2,1,0:T(8,128)(2,1)S(1)}, u32[]{:S(2)}, u32[]{:S(2)}) collective-permute-start(bf16[3,144,128]{2,1,0:T(8,128)(2,1)S(1)} %pad_maximum_fusion.1.refs_0_), channel_id=1, source_target_pairs={{0,6},{1,7},{2,4},{3,5},{4,2},{5,3},{6,0},{7,1},{8,14},{9,15},{10,... | collective-permute-start | bytes 331784 | tf_op jit(solution)/shard_map/ppermute | solution.py:26
  28.1 6.8 %copy-start.3 = (f32[512]{0:T(512)S(1)}, f32[512]{0:T(512)}, u32[]{:S(2)}) copy-start(f32[512]{0:T(512)} %param.18) | copy-start | bytes 6148
  29.0 5.1 %collective-permute-start.14 = (bf16[3,144,128]{2,1,0:T(8,128)(2,1)S(1)}, bf16[3,144,128]{2,1,0:T(8,128)(2,1)S(1)}, u32[]{:S(2)}, u32[]{:S(2)}) collective-permute-start(bf16[3,144,128]{2,1,0:T(8,128)(2,1)S(1)} %pad_maximum_fusion.1.refs_0_), channel_id=1, source_target_pairs={{0,4},{1,5},{2,6},{3,7},{4,0},{5,1},{6,2},{7,3},{8,12},{9,13},{10,... | collective-permute-start | bytes 331784 | tf_op jit(solution)/shard_map/ppermute | solution.py:26
  29.6 4.7 %collective-permute-start.12 = (bf16[3,144,128]{2,1,0:T(8,128)(2,1)S(1)}, bf16[3,144,128]{2,1,0:T(8,128)(2,1)S(1)}, u32[]{:S(2)}, u32[]{:S(2)}) collective-permute-start(bf16[3,144,128]{2,1,0:T(8,128)(2,1)S(1)} %pad_maximum_fusion.1.refs_0_), channel_id=1, source_target_pairs={{0,2},{1,3},{2,0},{3,1},{4,6},{5,7},{6,4},{7,5},{8,10},{9,11},{10,... | collective-permute-start | bytes 331784 | tf_op jit(solution)/shard_map/ppermute | solution.py:26
  31.1 1.3 %collective-permute-start.23 = (bf16[128,384]{1,0:T(8,128)(2,1)S(1)}, bf16[128,384]{1,0:T(8,128)(2,1)S(1)}, u32[]{:S(2)}, u32[]{:S(2)}) collective-permute-start(bf16[128,384]{1,0:T(8,128)(2,1)S(1)} %get-tuple-element.41), channel_id=1, source_target_pairs={{0,1},{1,0},{2,3},{3,2},{4,5},{5,4},{6,7},{7,6},{8,9},{9,8},{10,11... | collective-permute-start | bytes 294920 | tf_op jit(solution)/shard_map/ppermute | solution.py:26
  32.4 3.6 %collective-permute-start.21 = (bf16[4,144,128]{2,1,0:T(8,128)(2,1)S(1)}, bf16[4,144,128]{2,1,0:T(8,128)(2,1)S(1)}, u32[]{:S(2)}, u32[]{:S(2)}) collective-permute-start(bf16[4,144,128]{2,1,0:T(8,128)(2,1)S(1)} %pad_maximum_fusion), channel_id=1, source_target_pairs={{0,1},{1,0},{2,3},{3,2},{4,5},{5,4},{6,7},{7,6},{8,9},{9,8},{10,11... | collective-permute-start | bytes 442376 | tf_op jit(solution)/shard_map/ppermute | solution.py:26
  33.1 2.8 %collective-permute-start.11 = (bf16[3,144,128]{2,1,0:T(8,128)(2,1)S(1)}, bf16[3,144,128]{2,1,0:T(8,128)(2,1)S(1)}, u32[]{:S(2)}, u32[]{:S(2)}) collective-permute-start(bf16[3,144,128]{2,1,0:T(8,128)(2,1)S(1)} %pad_maximum_fusion.1.refs_0_), channel_id=1, source_target_pairs={{0,1},{1,0},{2,3},{3,2},{4,5},{5,4},{6,7},{7,6},{8,9},{9,8},{10,11... | collective-permute-start | bytes 331784 | tf_op jit(solution)/shard_map/ppermute | solution.py:26
  34.0 1.9 %collective-permute-start.17 = (bf16[3,144,128]{2,1,0:T(8,128)(2,1)S(1)}, bf16[3,144,128]{2,1,0:T(8,128)(2,1)S(1)}, u32[]{:S(2)}, u32[]{:S(2)}) collective-permute-start(bf16[3,144,128]{2,1,0:T(8,128)(2,1)S(1)} %collective-permute-done.16.refs_3_), channel_id=1, source_target_pairs={{0,1},{1,0},{2,3},{3,2},{4,5},{5,4},{6,7},{7,6},{8,9},{9,8},{10,11... | collective-permute-start | bytes 331784 | tf_op jit(solution)/shard_map/ppermute | solution.py:26
  34.3 1.7 %collective-permute-start.15 = (bf16[3,144,128]{2,1,0:T(8,128)(2,1)S(1)}, bf16[3,144,128]{2,1,0:T(8,128)(2,1)S(1)}, u32[]{:S(2)}, u32[]{:S(2)}) collective-permute-start(bf16[3,144,128]{2,1,0:T(8,128)(2,1)S(1)} %collective-permute-done.14.refs_2_), channel_id=1, source_target_pairs={{0,1},{1,0},{2,3},{3,2},{4,5},{5,4},{6,7},{7,6},{8,9},{9,8},{10,11... | collective-permute-start | bytes 331784 | tf_op jit(solution)/shard_map/ppermute | solution.py:26
  34.6 1.4 %collective-permute-start.13 = (bf16[3,144,128]{2,1,0:T(8,128)(2,1)S(1)}, bf16[3,144,128]{2,1,0:T(8,128)(2,1)S(1)}, u32[]{:S(2)}, u32[]{:S(2)}) collective-permute-start(bf16[3,144,128]{2,1,0:T(8,128)(2,1)S(1)} %collective-permute-done.12.refs_1_), channel_id=1, source_target_pairs={{0,1},{1,0},{2,3},{3,2},{4,5},{5,4},{6,7},{7,6},{8,9},{9,8},{10,11... | collective-permute-start | bytes 331784 | tf_op jit(solution)/shard_map/ppermute | solution.py:26
  37.6 7.1 %collective-permute-start.24 = (bf16[32,2048]{1,0:T(8,128)(2,1)S(1)}, bf16[32,2048]{1,0:T(8,128)(2,1)S(1)}, u32[]{:S(2)}, u32[]{:S(2)}) collective-permute-start(bf16[32,2048]{1,0:T(8,128)(2,1)S(1)} %get-tuple-element.45), channel_id=1, source_target_pairs={{0,6},{1,7},{2,4},{3,5},{4,2},{5,3},{6,0},{7,1},{8,14},{9,15},{10,... | collective-permute-start | bytes 393224 | tf_op jit(solution)/shard_map/ppermute | solution.py:26
  40.1 6.9 %collective-permute-start.25 = (bf16[32,2048]{1,0:T(8,128)(2,1)S(1)}, bf16[32,2048]{1,0:T(8,128)(2,1)S(1)}, u32[]{:S(2)}, u32[]{:S(2)}) collective-permute-start(bf16[32,2048]{1,0:T(8,128)(2,1)S(1)} %get-tuple-element.46), channel_id=1, source_target_pairs={{0,4},{1,5},{2,6},{3,7},{4,0},{5,1},{6,2},{7,3},{8,12},{9,13},{10,... | collective-permute-start | bytes 393224 | tf_op jit(solution)/shard_map/ppermute | solution.py:26
  40.6 6.4 %collective-permute-start.26 = (bf16[32,2048]{1,0:T(8,128)(2,1)S(1)}, bf16[32,2048]{1,0:T(8,128)(2,1)S(1)}, u32[]{:S(2)}, u32[]{:S(2)}) collective-permute-start(bf16[32,2048]{1,0:T(8,128)(2,1)S(1)} %get-tuple-element.47), channel_id=1, source_target_pairs={{0,2},{1,3},{2,0},{3,1},{4,6},{5,7},{6,4},{7,5},{8,10},{9,11},{10,... | collective-permute-start | bytes 393224 | tf_op jit(solution)/shard_map/ppermute | solution.py:26
  41.2 1.2 %collective-permute-start.27 = (f32[1,128]{1,0:T(1,128)S(1)}, f32[1,128]{1,0:T(1,128)S(1)}, u32[]{:S(2)}, u32[]{:S(2)}) collective-permute-start(f32[1,128]{1,0:T(1,128)S(1)} %get-tuple-element.49), channel_id=1, source_target_pairs={{0,1},{1,0},{2,3},{3,2},{4,5},{5,4},{6,7},{7,6},{8,9},{9,8},{10,11... | collective-permute-start | bytes 1544 | tf_op jit(solution)/shard_map/ppermute | solution.py:26
  (1 other events, 3.0 us)
